TPU v7x, 32 devices: a whole 2x2x4 slice. The times are simulated.
32 devices in a mesh: grp: 2 (over y), sp: 4 (over z), dp: 4 (over x, core).
Axes of the slice: x: 2, y: 2, z: 4, core: 2. Of those that a mesh axis runs over, the one named last changes fastest.
Arguments:
- gate_input: bfloat16 [8, 1536, 2048], P(('grp', 'dp'), 'sp'), parts along dimension 0, may hold values from -6 to 6
- value_input: bfloat16 [8, 1536, 2048], P(('grp', 'dp'), 'sp'), parts along dimension 0, may hold values from -6 to 6
- norm_gain: bfloat16 [2048], replicated, may hold values from 0.099609375 to 1.8984375
- norm_bias: bfloat16 [2048], replicated, may hold values from -2.5 to 2.5
- mix_weight: bfloat16 [16, 1024, 1024], P('sp', 'dp'), may hold values from -0.1875 to 0.1875
- mix_bias: bfloat16 [16, 1024], P('sp'), may hold values from 0.099609375 to 1.8984375
Outputs:
- gated: bfloat16 [8, 1536, 2048], P(('grp', 'dp'), 'sp'), parts along dimension 0
There are 2 independent parts, one for each index of `grp`. A program takes and returns all parts, laid end to end along the dimension named above; an argument that names none is the same for every part. Nothing has to cross between parts.
All inputs are finite; a program needn't handle non-finite values.
Results may differ from a plain program's by a relative error of at most 0.0053.
Values may be sent and summed in bfloat16 or wider, within the bound.
No kernel may reach another device: no remote copies, remote signals or barrier semaphores. Data moves between devices by JAX's collectives and lax.ppermute only.
A program may use at most 64 MiB of HBM per device.

v0:
```python
import jax
import jax.numpy as jnp
from jax import lax
from jax.sharding import PartitionSpec as P

GD = 128
BLK = 1024


def mix_groups(normed_ex, mix_weight, mix_bias):
    seqs, length, local_width = normed_ex.shape
    groups_here = mix_weight.shape[0]
    nblocks = -(-length // BLK)
    padded = jnp.pad(normed_ex, ((0, 0), (0, nblocks * BLK - length), (0, 0)))
    blocks = padded.reshape(seqs * nblocks, BLK, groups_here, GD)
    piece = lax.all_gather(mix_weight, "dp", axis=1, tiled=True)
    count = piece.shape[1]
    rows = lax.iota(jnp.int32, count)
    cols = lax.iota(jnp.int32, BLK)
    keep = cols[None, :] <= rows[:, None]
    masked = jnp.where(keep[None], piece, jnp.zeros_like(piece))
    term = jnp.einsum("gts,bsgc->btgc", masked, blocks, preferred_element_type=jnp.float32)
    bias_rows = mix_bias.astype(jnp.float32)
    mixed = term + bias_rows.T[None, :, :, None]
    mixed = mixed.reshape(seqs, nblocks * BLK, local_width)[:, :length]
    return mixed.astype(jnp.bfloat16)


def body(gate_input, value_input, norm_gain, norm_bias, mix_weight, mix_bias):
    act = jax.nn.gelu(value_input.astype(jnp.float32))
    mean = jnp.mean(act, axis=-1, keepdims=True)
    var = jnp.mean(jnp.square(act - mean), axis=-1, keepdims=True)
    normed = (
        (act - mean) * lax.rsqrt(var + 1e-06) * norm_gain.astype(jnp.float32)
        + norm_bias.astype(jnp.float32)
    ).astype(jnp.bfloat16)
    normed_ex = lax.all_to_all(normed, "sp", split_axis=2, concat_axis=1, tiled=True)
    mixed = mix_groups(normed_ex, mix_weight, mix_bias)
    returned = lax.all_to_all(mixed, "sp", split_axis=1, concat_axis=2, tiled=True)
    gated = jax.nn.gelu(gate_input.astype(jnp.float32)) * returned.astype(jnp.float32)
    return gated.astype(jnp.bfloat16)


def solution(mesh):
    placed = (
        P(("grp", "dp"), "sp", None),
        P(("grp", "dp"), "sp", None),
        P(),
        P(),
        P("sp", "dp", None),
        P("sp", None),
    )
    return jax.shard_map(
        body, mesh=mesh, in_specs=placed, out_specs=P(("grp", "dp"), "sp", None), check_vma=False
    )
```

profile of v0, /device:TPU:0, one launch (start us, length us, event | category | flops | bytes accessed | tf_op | source)
XLA Modules:
  0.0 239.9 jit_solution(9603832664579578522)
XLA Ops:
  6.5 0.0 copy-start
  6.5 0.0 copy-start.4
  6.5 0.0 copy-start.5
  6.5 0.0 all-gather.2.cloned.1.call-start
  6.5 0.7 all-gather.2.cloned.1.call-update
  7.3 0.7 copy-done
  7.9 0.9 copy.17
  8.8 0.0 copy-done.4
  8.8 0.0 copy-done.5
  8.8 1.1 fusion.23
  10.0 1.3 multiply_reduce_fusion
  11.3 1.5 add_convert_fusion
  12.9 30.1 %copy.35 = bf16[1,384,2048]{1,0,2:T(2,128)(2,1)S(1)} copy(bf16[1,384,2048]{1,2,0:T(8,128)(2,1)S(1)} %add_convert_fusion) | data formatting | bytes 3145728 | tf_op jit(solution)/shard_map/convert_element_type | solution.py:36
  43.0 0.5 broadcast.85
  43.5 34.4 %reduce.2 = bf16[2048,384]{1,0:T(8,128)(2,1)} reduce(bf16[2048,1,384]{2,1,0:T(2,128)(2,1)S(1)} %bitcast.31, bf16[]{:T(256)} %broadcast.85), dimensions={1}, to_apply=%bitcast.30.reduce_sub_computation | reduce | bytes 3145730
  77.9 0.0 copy-start.3
  77.9 3.7 %reshape.69 = bf16[4,2,98304]{2,1,0:T(2,128)(2,1)} reshape(bf16[2048,384]{1,0:T(8,128)(2,1)} %reduce.2) | data formatting | bytes 3145728
  81.7 6.3 %all-to-all-start = ((bf16[4,2,98304]{2,1,0:T(2,128)(2,1)}), bf16[4,2,98304]{2,1,0:T(2,128)(2,1)}, u32[]{:S(2)}, u32[]{:S(2)}) async-start(bf16[4,2,98304]{2,1,0:T(2,128)(2,1)} %reshape.69), calls=%async_computation | async-start | bytes 3145728 | tf_op jit(solution)/shard_map/all_to_all | solution.py:37
  88.0 1.3 iota_compare_fusion
  89.3 0.0 copy-done.3
  89.3 35.8 %all-to-all-done = bf16[4,2,98304]{2,1,0:T(2,128)(2,1)} async-done(((bf16[4,2,98304]{2,1,0:T(2,128)(2,1)}), bf16[4,2,98304]{2,1,0:T(2,128)(2,1)}, u32[]{:S(2)}, u32[]{:S(2)}) %all-to-all-start) | async-done | bytes 1572896 | tf_op jit(solution)/shard_map/all_to_all | solution.py:37
  125.1 3.1 %reshape.70 = bf16[2048,1,384]{2,1,0:T(2,128)(2,1)S(1)} reshape(bf16[4,2,98304]{2,1,0:T(2,128)(2,1)} %all-to-all-done) | data formatting | bytes 3145728
  128.2 1.4 copy.27
  129.6 2.6 %copy.19 = bf16[1,4,384,512]{3,2,1,0:T(8,128)(2,1)} copy(bf16[1,4,384,512]{2,3,1,0:T(8,128)(2,1)} %bitcast.36) | data formatting | bytes 3145728 | tf_op jit(solution)/shard_map/all_to_all | solution.py:37
  132.2 0.0 copy-start.2
  132.2 1.6 pad.4
  133.8 2.1 reshape.64
  135.9 0.0 all-gather.2.cloned.1.call-done
  135.9 0.0 copy-done.2
  135.9 8.1 %fusion.4 = bf16[2,1024,4,128]{1,3,0,2:T(8,128)(2,1)} fusion(f32[1024,4]{0,1:T(4,128)S(1)} %convert_bitcast_fusion.1, bf16[4,1024,1024]{2,1,0:T(8,128)(2,1)} %all-gather.2.cloned.1.call-done, pred[1024,1024]{1,0:T(8,128)(4,1)S(1)} %copy-done.2, bf16[2,1024,4,128]{3,2,1,0:T(4,128)(2,1)} %reshape.64), kind=kOutput, calls=%fused_computation.13 | convolution fusion | flops 2153775104 | bytes 13647872 | tf_op jit(solution)/shard_map/gts,bsgc->btgc/dot_general | solution.py:22
  144.0 3.1 %copy.21 = bf16[2,1024,4,128]{3,2,1,0:T(4,128)(2,1)S(1)} copy(bf16[2,1024,4,128]{1,3,0,2:T(8,128)(2,1)} %fusion.4) | data formatting | bytes 4194304 | tf_op jit(solution)/shard_map/convert.5
  147.2 2.2 reshape.65
  149.4 0.0 slice-start
  149.4 1.4 slice-done
  150.8 11.7 %copy.34 = bf16[1,1536,512]{2,0,1:T(2,128)(2,1)S(1)} copy(bf16[1,1536,512]{2,1,0:T(8,128)(2,1)S(1)} %slice-done) | data formatting | bytes 3145728 | tf_op jit(solution)/shard_map/slice | solution.py:25
  162.5 11.1 %reduce.3 = bf16[1536,512]{1,0:T(8,128)(2,1)} reduce(bf16[1536,1,512]{2,1,0:T(2,128)(2,1)S(1)} %bitcast.32, bf16[]{:T(256)} %broadcast.85), dimensions={1}, to_apply=%bitcast.29.reduce_sub_computation | reduce | bytes 3145730
  173.5 0.0 copy-start.1
  173.5 4.3 %reshape.71 = bf16[4,2,98304]{2,1,0:T(2,128)(2,1)} reshape(bf16[1536,512]{1,0:T(8,128)(2,1)} %reduce.3) | data formatting | bytes 3145728
  177.8 4.3 %all-to-all-start.1 = ((bf16[4,2,98304]{2,1,0:T(2,128)(2,1)}), bf16[4,2,98304]{2,1,0:T(2,128)(2,1)}, u32[]{:S(2)}, u32[]{:S(2)}) async-start(bf16[4,2,98304]{2,1,0:T(2,128)(2,1)} %reshape.71), calls=%async_computation.1 | async-start | bytes 3145728 | tf_op jit(solution)/shard_map/all_to_all | solution.py:39
  182.1 0.0 copy-done.1
  182.2 1.6 copy.16
  183.7 35.0 %all-to-all-done.1 = bf16[4,2,98304]{2,1,0:T(2,128)(2,1)} async-done(((bf16[4,2,98304]{2,1,0:T(2,128)(2,1)}), bf16[4,2,98304]{2,1,0:T(2,128)(2,1)}, u32[]{:S(2)}, u32[]{:S(2)}) %all-to-all-start.1) | async-done | bytes 1572896 | tf_op jit(solution)/shard_map/all_to_all | solution.py:39
  218.7 3.1 %reshape.72 = bf16[1536,1,512]{2,1,0:T(2,128)(2,1)S(1)} reshape(bf16[4,2,98304]{2,1,0:T(2,128)(2,1)} %all-to-all-done.1) | data formatting | bytes 3145728
  221.8 0.4 copy.23
  222.2 2.1 convert_bitcast_fusion
  224.3 2.4 copy.24
  226.7 3.8 %fusion.12 = bf16[1,384,2048]{1,2,0:T(8,128)(2,1)} fusion(bf16[1,384,2048]{1,2,0:T(8,128)(2,1)} %copy.16, f32[1,384,4,512]{1,3,2,0:T(8,128)S(1)} %copy.24), kind=kLoop, calls=%fused_computation.22 | loop fusion | flops 8650752 | bytes 6291456 | tf_op jit(solution)/shard_map/convert_element_type | solution.py:41
  230.5 2.6 %copy.25 = bf16[1,384,2048]{2,1,0:T(8,128)(2,1)} copy(bf16[1,384,2048]{1,2,0:T(8,128)(2,1)} %fusion.12) | data formatting | bytes 3145728 | tf_op jit(solution)/shard_map/convert_element_type | solution.py:41
  (5 shorter events, 0.0 us)
Async XLA Ops:
  6.5 1.4 copy-start
  6.5 2.3 copy-start.4
  6.5 2.3 copy-start.5
  6.5 129.4 %all-gather.2.cloned.1.call-start = ((), (), s32[]{:S(2)}) async-start(), calls=%async_computation.2 | async-start | bytes 10485760 | tf_op jit(solution)/shard_map/all_gather | solution.py:16
  77.9 11.4 %copy-start.3 = (bf16[4,1024]{1,0:T(4,128)(2,1)S(1)}, bf16[4,1024]{1,0:T(4,128)(2,1)}, u32[]{:S(2)}) copy-start(bf16[4,1024]{1,0:T(4,128)(2,1)} %param.11) | copy-start | bytes 24580
  81.7 43.4 %all-to-all-start = ((bf16[4,2,98304]{2,1,0:T(2,128)(2,1)}), bf16[4,2,98304]{2,1,0:T(2,128)(2,1)}, u32[]{:S(2)}, u32[]{:S(2)}) async-start(bf16[4,2,98304]{2,1,0:T(2,128)(2,1)} %reshape.69), calls=%async_computation | async-start | bytes 3145728 | tf_op jit(solution)/shard_map/all_to_all | solution.py:37
  132.2 3.7 %copy-start.2 = (pred[1024,1024]{1,0:T(8,128)(4,1)S(1)}, pred[1024,1024]{1,0:T(8,128)(4,1)}, u32[]{:S(2)}) copy-start(pred[1024,1024]{1,0:T(8,128)(4,1)} %iota_compare_fusion) | copy-start | bytes 3145732
  149.4 1.4 slice-start
  173.5 8.6 %copy-start.1 = (bf16[1,384,2048]{2,1,0:T(8,128)(2,1)S(1)}, bf16[1,384,2048]{2,1,0:T(8,128)(2,1)}, u32[]{:S(2)}) copy-start(bf16[1,384,2048]{2,1,0:T(8,128)(2,1)} %param.6) | copy-start | bytes 4718596
  177.8 40.9 %all-to-all-start.1 = ((bf16[4,2,98304]{2,1,0:T(2,128)(2,1)}), bf16[4,2,98304]{2,1,0:T(2,128)(2,1)}, u32[]{:S(2)}, u32[]{:S(2)}) async-start(bf16[4,2,98304]{2,1,0:T(2,128)(2,1)} %reshape.71), calls=%async_computation.1 | async-start | bytes 3145728 | tf_op jit(solution)/shard_map/all_to_all | solution.py:39
Sparse Core Ops, SparseCore 0:
  8.9 60.9 all-gather.1
where the time goes:
time: 241 us; the launch traced here: 240 us
  local copies, waits for them, and re-layouts  79.4 us (33%)
  waiting for transfers between devices  71.5 us (30%)
  other arithmetic  56.7 us (24%)
  between operations  13.5 us (6%)
  starting transfers between devices  10.7 us (4%)
  matrix products  8.09 us (3%)
    unnamed x2, other arithmetic  45.5 us
    all_to_all x1, waiting for transfers between devices, body(): lax.all_to_all(normed, 'sp', split_axis=2, concat_axis=1, tiled=True)  35.8 us
    all_to_all x1, waiting for transfers between devices, body(): lax.all_to_all(mixed, 'sp', split_axis=1, concat_axis=2, tiled=True)  35 us
    convert_element_type x1, local copies, waits for them, and re-layouts, body(): normed = ((act - mean) * lax.rsqrt(var + 1e-06) * norm_gain.astype(jnp.fl...  30.1 us
    unnamed x20, local copies, waits for them, and re-layouts  19.2 us
    slice x3, local copies, waits for them, and re-layouts, mix_groups(): mixed = mixed.reshape(seqs, nblocks * BLK, local_width)[:, :length]  13.1 us
    dot_general x1, matrix products, mix_groups(): jnp.einsum('gts,bsgc->btgc', masked, blocks, preferred_element_type=jnp.f...  8.09 us
    all_to_all x1, starting transfers between devices, body(): lax.all_to_all(normed, 'sp', split_axis=2, concat_axis=1, tiled=True)  6.35 us
  transfers between devices with their start and end apart: 3, of which 2 were waited for; matrix products, arithmetic and copies ran while one was open for 36% of the time, Pallas kernels for 0%

commit v1 on v0

v1 whole, which is shorter than its diff:
```python
import functools

import jax
import jax.numpy as jnp
from jax import lax
from jax.experimental import pallas as pl
from jax.experimental.pallas import tpu as pltpu
from jax.sharding import PartitionSpec as P


GD = 128
BLK = 1024
TILE = 256


VMEM = pl.BlockSpec(memory_space=pltpu.VMEM)
SMEM = pl.BlockSpec(memory_space=pltpu.SMEM)


def gelu(x):
    half = 0.5 * x
    return half + half * jnp.tanh(x * (0.7978845608028654 + 0.035677408136300125 * (x * x)))


def norm_kernel(shards, chunks, width, rows_step, at_ref, x_ref, gain_ref, bias_ref, *refs):
    outs, held = refs[:-1], refs[-1]
    here = at_ref[0]
    span = chunks * width
    gain = gain_ref[...].astype(jnp.float32)
    bias = bias_ref[...].astype(jnp.float32)

    def step(i, carry):
        rows = pl.ds(pl.multiple_of(i * rows_step, rows_step), rows_step)
        act = gelu(x_ref[rows, :].astype(jnp.float32))
        centred = act - jnp.mean(act, axis=-1, keepdims=True)
        var = jnp.mean(jnp.square(centred), axis=-1, keepdims=True)
        held[rows, :] = (centred * lax.rsqrt(var + 1e-06) * gain + bias).astype(jnp.bfloat16)
        return carry

    steps = x_ref.shape[0] // rows_step
    lax.fori_loop(0, steps, step, 0, unroll=4 if steps % 4 == 0 else 1)
    for c in range(chunks):
        for s in range(shards):
            owner = lax.rem(here + s, shards)
            start = pl.multiple_of(owner * span + c * width, GD)
            outs[c * shards + s][...] = held[:, pl.ds(start, width)]


def mix_kernel(shards, length, first, layout, at_ref, *refs):
    pieces, refs = refs[:shards], refs[shards:]
    weights, refs = refs[:len(layout)], refs[len(layout):]
    bias_ref, outs, (values, mixed) = refs[0], refs[1:1 + shards], refs[1 + shards:]
    here, row = at_ref[0], at_ref[1]
    rows = pieces[0].shape[0]
    groups = pieces[0].shape[1] // GD
    nblocks = -(-length // BLK)
    for s in range(shards):
        origin = lax.rem(here + shards - s, shards)
        mixed[pl.ds(pl.multiple_of(origin * rows, rows), rows), :] = pieces[s][...]
    for g in range(groups):
        for b in range(nblocks):
            count = min(BLK, length - b * BLK)
            lanes = pl.ds(b * GD, GD)
            values[g, pl.ds(0, count), lanes] = mixed[pl.ds(b * BLK, count), pl.ds(g * GD, GD)]
            if count < BLK:
                values[g, pl.ds(count, BLK - count), lanes] = jnp.zeros((BLK - count, GD), jnp.bfloat16)
    tiles = {}
    for ref, (flip, first_row, low) in zip(weights, layout):
        tiles.setdefault((flip, first_row), []).append((ref, low))
    for (flip, first_row), parts in tiles.items():
        at_row = row ^ flip if first_row is None else first_row
        top = pl.multiple_of(at_row * TILE, TILE)
        for g in range(groups):
            total = None
            for ref, low in parts:
                if first_row is None:
                    part = ref[g]
                else:
                    part = ref[g, pl.ds(first_row * TILE, TILE), :]
                cols = lax.broadcasted_iota(jnp.int32, part.shape, 1) + low
                keep = cols <= lax.broadcasted_iota(jnp.int32, part.shape, 0) + top
                part = jnp.where(keep, part, jnp.zeros_like(part))
                term = jnp.dot(part, values[g, pl.ds(low, part.shape[1]), :], preferred_element_type=jnp.float32)
                total = term if total is None else total + term
            total = total + bias_ref[pl.ds(top, TILE), pl.ds(first + g, 1)]
            for b in range(nblocks):
                mixed[pl.ds(b * BLK + top, TILE), pl.ds(g * GD, GD)] = total[:, b * GD:(b + 1) * GD].astype(jnp.bfloat16)
    for s in range(shards):
        target = lax.rem(here + s, shards)
        outs[s][...] = mixed[pl.ds(pl.multiple_of(target * rows, rows), rows), :]


def gate_kernel(shards, at_ref, gate_ref, *refs):
    pieces, out_ref = refs[:shards], refs[-1]
    for s in range(shards):

        @pl.when(pl.program_id(0) == s)
        def _():
            gate = gelu(gate_ref[...].astype(jnp.float32))
            out_ref[...] = (gate * pieces[s][...].astype(jnp.float32)).astype(jnp.bfloat16)


def shift_pairs(count, by):
    return [(i, (i + by) % count) for i in range(count)]


def flip_pairs(count, by):
    return [(i, i ^ by) for i in range(count)]


def exchange_rows(parts, ndp):
    got = []
    whole = parts[0]
    got.append((whole, 0, None, 0))
    got.append((lax.ppermute(whole, "dp", flip_pairs(ndp, 1)), 1, None, 0))
    for low, least, part in parts[1:]:
        far = lax.ppermute(part, "dp", [p for p in flip_pairs(ndp, 2) if p[0] >= least])
        got.append((far, 2, None, low))
        got.append((lax.ppermute(far, "dp", flip_pairs(ndp, 1)), 3, None, low))
    return got


def gathered_rows(weight):
    whole = lax.all_gather(weight, "dp", axis=1, tiled=True)
    return [(whole, 0, i, 0) for i in range(BLK // TILE)]


def compute(nsp, ndp, exchange, gate, value, gain, bias, mix_weight, bias_rows):
    rows, width = value.shape
    groups = mix_weight.shape[0]
    length = rows * nsp
    chunks = 2 if groups % 2 == 0 else 1
    per = groups // chunks
    rows_step = 16
    nblocks = -(-length // BLK)
    at = jnp.stack([lax.axis_index("sp").astype(jnp.int32), lax.axis_index("dp").astype(jnp.int32)])
    piece = jax.ShapeDtypeStruct((rows, per * GD), jnp.bfloat16)

    weights = []
    for c in range(chunks):
        own = lax.slice_in_dim(mix_weight, c * per, (c + 1) * per, axis=0)
        if exchange:
            cuts = [(0, 2 * TILE, 0), (2 * TILE, TILE, 2), (3 * TILE, TILE, 3)]
            parts = [(low, least, lax.slice_in_dim(own, low, low + count, axis=2)) for low, count, least in cuts]
            weights.append(exchange_rows([own] + parts, ndp))
        else:
            weights.append(gathered_rows(own))

    sent = pl.pallas_call(
        functools.partial(norm_kernel, nsp, chunks, per * GD, rows_step),
        out_shape=[piece] * (nsp * chunks),
        in_specs=[SMEM, VMEM, VMEM, VMEM],
        out_specs=[VMEM] * (nsp * chunks),
        scratch_shapes=[pltpu.VMEM((rows, width), jnp.bfloat16)],
        cost_estimate=pl.CostEstimate(flops=30 * rows * width, bytes_accessed=4 * rows * width, transcendentals=rows * width),
        name="norm",
    )(at, value, gain, bias)
    out = None
    got = []
    for c in range(chunks):
        mine = sent[c * nsp:(c + 1) * nsp]
        got.append([mine[0]] + [lax.ppermute(mine[s], "sp", shift_pairs(nsp, s)) for s in range(1, nsp)])
    for c in range(chunks):
        layout = [(flip, fixed, low) for _, flip, fixed, low in weights[c]]
        outs = pl.pallas_call(
            functools.partial(mix_kernel, nsp, length, c * per, layout),
            out_shape=[piece] * nsp,
            in_specs=[SMEM] + [VMEM] * (nsp + len(layout) + 1),
            out_specs=[VMEM] * nsp,
            scratch_shapes=[
                pltpu.VMEM((per, BLK, nblocks * GD), jnp.bfloat16),
                pltpu.VMEM((nblocks * BLK, per * GD), jnp.bfloat16),
            ],
            cost_estimate=pl.CostEstimate(flops=2 * per * BLK * length * GD, bytes_accessed=per * BLK * BLK, transcendentals=0),
        )(at, *got[c], *[w[0] for w in weights[c]], bias_rows)
        back = [outs[0]] + [lax.ppermute(outs[s], "sp", shift_pairs(nsp, s)) for s in range(1, nsp)]

        def block(s, at_ref, c=c):
            return 0, lax.rem(at_ref[0] + nsp - s, nsp) * chunks + c

        wide = pl.BlockSpec((rows, per * GD), block)
        extra = [] if out is None else [out]
        out = pl.pallas_call(
            functools.partial(gate_kernel, nsp),
            out_shape=jax.ShapeDtypeStruct((rows, width), jnp.bfloat16),
            grid_spec=pltpu.PrefetchScalarGridSpec(
                num_scalar_prefetch=1,
                grid=(nsp,),
                in_specs=[wide] + [VMEM] * nsp + [pl.BlockSpec(memory_space=pl.ANY)] * len(extra),
                out_specs=wide,
            ),
            input_output_aliases={nsp + 2: 0} if extra else {},
            cost_estimate=pl.CostEstimate(flops=12 * rows * width // chunks, bytes_accessed=6 * rows * width // chunks, transcendentals=rows * width // chunks),
        )(at, gate, *back, *extra)
    return out


def body(nsp, ndp, exchange, gate_input, value_input, norm_gain, norm_bias, mix_weight, mix_bias):
    seqs, _, width = value_input.shape
    gain = norm_gain.reshape(1, width)
    bias = norm_bias.reshape(1, width)
    bias_rows = mix_bias.astype(jnp.float32).T
    return jnp.stack([
        compute(nsp, ndp, exchange, gate_input[q], value_input[q], gain, bias, mix_weight, bias_rows)
        for q in range(seqs)
    ])


def solution(mesh):
    nsp, ndp = mesh.shape["sp"], mesh.shape["dp"]
    exchange = ndp == BLK // TILE == 4
    placed = (
        P(("grp", "dp"), "sp", None),
        P(("grp", "dp"), "sp", None),
        P(),
        P(),
        P("sp", "dp", None),
        P("sp", None),
    )
    return jax.shard_map(
        functools.partial(body, nsp, ndp, exchange),
        mesh=mesh,
        in_specs=placed,
        out_specs=P(("grp", "dp"), "sp", None),
        check_vma=False,
    )
```

time: 241 us -> 123 us (0.51)
  local copies, waits for them, and re-layouts: 79.4 us -> 8.64 us
  other arithmetic: 56.7 us -> 0.59 us
  starting transfers between devices: 10.7 us -> 40.8 us
  waiting for transfers between devices: 71.5 us -> 45.6 us
  Pallas kernels: 0 us -> 24.8 us
  between operations: 13.5 us -> 0.25 us
  matrix products: 8.09 us -> 0 us
    all_to_all x2 -> x0, waiting for transfers between devices: 70.8 us -> none  [the longest x1 35.8 us: body(): lax.all_to_all(normed, 'sp', split_axis=2, concat_axis=1, tiled=True)]
    ppermute x0 -> x26, waiting for transfers between devices: none -> 45.6 us  [the longest x6 18.3 us: exchange_rows(): lax.ppermute(part, 'dp', [p for p in flip_pairs(ndp, 2) if p[0] >= least])]
    unnamed x2 -> x0, other arithmetic: 45.5 us -> none
    ppermute x0 -> x26, starting transfers between devices: none -> 40.8 us  [the longest x6 22.1 us: compute(): lax.ppermute(mine[s], 'sp', shift_pairs(nsp, s))]
    convert_element_type x3 -> x0, local copies, waits for them, and re-layouts: 35 us -> none  [the longest x1 30.1 us: body(): normed = ((act - mean) * lax.rsqrt(var + 1e-06) * norm_gain.astype(jnp.fl...]
    pallas_call x0 -> x5, Pallas kernels: none -> 24.8 us  [the longest x2 10.6 us: compute(): pl.pallas_call(functools.partial(mix_kernel, nsp, length, c * per, layout...]
    unnamed x20 -> x50, local copies, waits for them, and re-layouts: 19.2 us -> 3.42 us
    slice x3, local copies, waits for them, and re-layouts: 13.1 us -> 1.54 us  [the longest x2 1.37 us: compute(): lax.slice_in_dim(own, low, low + count, axis=2)]
  transfers between devices with their start and end apart: 3 -> 26, of which waited for: 2 -> 8; matrix products, arithmetic and copies ran while one was open for 36% -> 2% of each run, Pallas kernels for 0% -> 13%
where the time goes in v1:
time: 123 us; the launch traced here: 121 us
  waiting for transfers between devices  45.6 us (37%)
  starting transfers between devices  40.8 us (33%)
  Pallas kernels  24.8 us (20%)
  local copies, waits for them, and re-layouts  8.64 us (7%)
    ppermute x6, starting transfers between devices, compute(): lax.ppermute(mine[s], 'sp', shift_pairs(nsp, s))  22.1 us
    ppermute x6, waiting for transfers between devices, exchange_rows(): lax.ppermute(part, 'dp', [p for p in flip_pairs(ndp, 2) if p[0] >= least])  18.3 us
    ppermute x6, waiting for transfers between devices, compute(): lax.ppermute(outs[s], 'sp', shift_pairs(nsp, s))  13.2 us
    ppermute x6, waiting for transfers between devices, compute(): lax.ppermute(mine[s], 'sp', shift_pairs(nsp, s))  13 us
    pallas_call x2, Pallas kernels, compute(): pl.pallas_call(functools.partial(mix_kernel, nsp, length, c * per, layout...  10.6 us
    ppermute x6, starting transfers between devices, compute(): lax.ppermute(outs[s], 'sp', shift_pairs(nsp, s))  9.65 us
    pallas_call x2, Pallas kernels, compute(): pl.pallas_call(functools.partial(gate_kernel, nsp), out_shape=jax.ShapeDt...  9.21 us
    ppermute x6, starting transfers between devices, exchange_rows(): lax.ppermute(part, 'dp', [p for p in flip_pairs(ndp, 2) if p[0] >= least])  6.3 us
  transfers between devices with their start and end apart: 26, of which 8 were waited for; matrix products, arithmetic and copies ran while one was open for 2% of the time, Pallas kernels for 13%

profile of v1, /device:TPU:0, one launch (start us, length us, event | category | flops | bytes accessed | tf_op | source)
XLA Modules:
  0.0 120.8 jit_solution(15071391200819096529)
XLA Ops:
  0.0 1.4 %reshape.6.gain_ref = bf16[1,2048]{1,0:T(2,128)(2,1)} reshape(bf16[2048]{0:T(1024)(128)(2,1)} %param.8) | data formatting | bytes 8192 | tf_op jit(solution)/shard_map/reshape | solution.py:200
  1.4 1.3 %reshape.7.bias_ref = bf16[1,2048]{1,0:T(2,128)(2,1)} reshape(bf16[2048]{0:T(1024)(128)(2,1)} %param.9) | data formatting | bytes 8192 | tf_op jit(solution)/shard_map/reshape | solution.py:201
  2.7 0.6 pad_add_fusion.at_ref
  3.3 5.1 %norm.1 = (bf16[384,256]{1,0:T(8,128)(2,1)}, bf16[384,256]{1,0:T(8,128)(2,1)}, bf16[384,256]{1,0:T(8,128)(2,1)}, bf16[384,256]{1,0:T(8,128)(2,1)}, bf16[384,256]...) custom-call(s32[2]{0:T(128)} %pad_add_fusion.at_ref, ...), custom_call_target="tpu_custom_call" | custom-call | flops 23592960 | bytes 3145728 | tf_op jit(solution)/shard_map/norm/pallas_call | solution.py:149
  8.4 3.1 %collective-permute-start.13 = (bf16[384,256]{1,0:T(8,128)(2,1)}, bf16[384,256]{1,0:T(8,128)(2,1)S(1)}, u32[]{:S(2)}, u32[]{:S(2)}) collective-permute-start(bf16[384,256]{1,0:T(8,128)(2,1)} %get-tuple-element.30), channel_id=1, source_target_pairs={{0,4},{4,8},{8,12},{12,0},{1,5},{5,9},{9,13},{13,1},{2,6},{6,10},{... | collective-permute-start | bytes 589832 | tf_op jit(solution)/shard_map/ppermute | solution.py:162
  11.4 2.6 %collective-permute-start.14 = (bf16[384,256]{1,0:T(8,128)(2,1)}, bf16[384,256]{1,0:T(8,128)(2,1)S(1)}, u32[]{:S(2)}, u32[]{:S(2)}) collective-permute-start(bf16[384,256]{1,0:T(8,128)(2,1)} %get-tuple-element.31), channel_id=1, source_target_pairs={{0,8},{4,12},{8,0},{12,4},{1,9},{5,13},{9,1},{13,5},{2,10},{6,14},... | collective-permute-start | bytes 589832 | tf_op jit(solution)/shard_map/ppermute | solution.py:162
  14.0 1.3 %collective-permute-start.15 = (bf16[384,256]{1,0:T(8,128)(2,1)}, bf16[384,256]{1,0:T(8,128)(2,1)S(1)}, u32[]{:S(2)}, u32[]{:S(2)}) collective-permute-start(bf16[384,256]{1,0:T(8,128)(2,1)} %get-tuple-element.32), channel_id=1, source_target_pairs={{0,12},{4,0},{8,4},{12,8},{1,13},{5,1},{9,5},{13,9},{2,14},{6,2},{... | collective-permute-start | bytes 589832 | tf_op jit(solution)/shard_map/ppermute | solution.py:162
  15.4 1.3 %fusion = (bf16[2,256,256]{2,1,0:T(8,128)(2,1)S(1)}, bf16[2,256,256]{2,1,0:T(8,128)(2,1)S(1)}, bf16[2,256,256]{2,1,0:T(8,128)(2,1)S(1)}, bf16[2,256,256]{2,1,0:T(8,128)(2,1)S(1)}) fusion(bf16[4,256,1024]{2,1,0:T(8,128)(2,1)} %param.10), kind=kLoop, calls=%fused_computation.1 | loop fusion | bytes 2097152 | tf_op jit(solution)/shard_map/slice | solution.py:144
  16.6 1.3 %collective-permute-start.19 = (bf16[2,256,256]{2,1,0:T(8,128)(2,1)S(1)}, bf16[2,256,256]{2,1,0:T(8,128)(2,1)S(1)}, u32[]{:S(2)}, u32[]{:S(2)}) collective-permute-start(bf16[2,256,256]{2,1,0:T(8,128)(2,1)S(1)} %get-tuple-element.40), channel_id=1, source_target_pairs={{2,0},{3,1},{6,4},{7,5},{10,8},{11,9},{14,12},{15,13},{18,16},{19,... | collective-permute-start | bytes 786440 | tf_op jit(solution)/shard_map/ppermute | solution.py:117
  17.9 0.7 collective-permute-start
  18.7 0.2 fusion.2
  18.9 0.0 copy-start.1
  18.9 0.0 copy-start.22
  18.9 0.6 collective-permute-done.13.refs_1_
  19.5 9.4 %collective-permute-start.1 = (bf16[384,256]{1,0:T(8,128)(2,1)S(1)}, bf16[384,256]{1,0:T(8,128)(2,1)S(1)}, u32[]{:S(2)}, u32[]{:S(2)}) collective-permute-start(bf16[384,256]{1,0:T(8,128)(2,1)S(1)} %copy-done.23), channel_id=1, source_target_pairs={{0,8},{4,12},{8,0},{12,4},{1,9},{5,13},{9,1},{13,5},{2,10},{6,14},... | collective-permute-start | bytes 589832 | tf_op jit(solution)/shard_map/ppermute | solution.py:162
  28.9 0.1 fusion.1
  29.0 0.0 collective-permute-done.14.refs_2_
  29.0 0.7 collective-permute-start.21
  29.7 0.1 collective-permute-start.16
  29.8 2.4 %collective-permute-done.refs_1_ = bf16[384,256]{1,0:T(8,128)(2,1)S(1)} collective-permute-done((bf16[384,256]{1,0:T(8,128)(2,1)S(1)}, bf16[384,256]{1,0:T(8,128)(2,1)S(1)}, u32[]{:S(2)}, u32[]{:S(2)}) %collective-permute-start) | collective-permute-done | bytes 196640 | tf_op jit(solution)/shard_map/ppermute | solution.py:162
  32.2 1.7 %collective-permute-start.17 = (bf16[2,256,512]{2,1,0:T(8,128)(2,1)S(1)}, bf16[2,256,512]{2,1,0:T(8,128)(2,1)S(1)}, u32[]{:S(2)}, u32[]{:S(2)}) collective-permute-start(bf16[2,256,512]{2,1,0:T(8,128)(2,1)S(1)} %get-tuple-element.41), channel_id=1, source_target_pairs={{0,2},{1,3},{2,0},{3,1},{4,6},{5,7},{6,4},{7,5},{8,10},{9,11},{10,... | collective-permute-start | bytes 1572872 | tf_op jit(solution)/shard_map/ppermute | solution.py:117
  33.9 10.0 %collective-permute-done.1.refs_2_ = bf16[384,256]{1,0:T(8,128)(2,1)S(1)} collective-permute-done((bf16[384,256]{1,0:T(8,128)(2,1)S(1)}, bf16[384,256]{1,0:T(8,128)(2,1)S(1)}, u32[]{:S(2)}, u32[]{:S(2)}) %collective-permute-start.1) | collective-permute-done | bytes 196640 | tf_op jit(solution)/shard_map/ppermute | solution.py:162
  43.9 1.3 %collective-permute-start.6 = (bf16[2,256,256]{2,1,0:T(8,128)(2,1)S(1)}, bf16[2,256,256]{2,1,0:T(8,128)(2,1)}, u32[]{:S(2)}, u32[]{:S(2)}) collective-permute-start(bf16[2,256,256]{2,1,0:T(8,128)(2,1)S(1)} %get-tuple-element.39), channel_id=1, source_target_pairs={{2,0},{3,1},{6,4},{7,5},{10,8},{11,9},{14,12},{15,13},{18,16},{19,... | collective-permute-start | bytes 786440 | tf_op jit(solution)/shard_map/ppermute | solution.py:117
  45.2 1.4 %collective-permute-start.8 = (bf16[2,256,256]{2,1,0:T(8,128)(2,1)S(1)}, bf16[2,256,256]{2,1,0:T(8,128)(2,1)}, u32[]{:S(2)}, u32[]{:S(2)}) collective-permute-start(bf16[2,256,256]{2,1,0:T(8,128)(2,1)S(1)} %get-tuple-element.38), channel_id=1, source_target_pairs={{3,1},{7,5},{11,9},{15,13},{19,17},{23,21},{27,25},{31,29}} | collective-permute-start | bytes 786440 | tf_op jit(solution)/shard_map/ppermute | solution.py:117
  46.5 0.0 collective-permute-done.21.refs_10_
  46.5 0.0 collective-permute-start.3
  46.6 8.4 %collective-permute-done.6.refs_8_ = bf16[2,256,256]{2,1,0:T(8,128)(2,1)} collective-permute-done((bf16[2,256,256]{2,1,0:T(8,128)(2,1)S(1)}, bf16[2,256,256]{2,1,0:T(8,128)(2,1)}, u32[]{:S(2)}, u32[]{:S(2)}) %collective-permute-start.6) | collective-permute-done | bytes 262176 | tf_op jit(solution)/shard_map/ppermute | solution.py:117
  55.0 0.0 collective-permute-start.4
  55.0 0.0 collective-permute-done.8.refs_10_
  55.0 1.7 %collective-permute-start.20 = (bf16[2,256,256]{2,1,0:T(8,128)(2,1)S(1)}, bf16[2,256,256]{2,1,0:T(8,128)(2,1)S(1)}, u32[]{:S(2)}, u32[]{:S(2)}) collective-permute-start(bf16[2,256,256]{2,1,0:T(8,128)(2,1)S(1)} %collective-permute-done.19.refs_8_), channel_id=1, source_target_pairs={{0,1},{1,0},{2,3},{3,2},{4,5},{5,4},{6,7},{7,6},{8,9},{9,8},{10,11... | collective-permute-start | bytes 786440 | tf_op jit(solution)/shard_map/ppermute | solution.py:119
  56.7 0.1 collective-permute-start.18
  56.8 1.1 collective-permute-done.20.refs_9_
  57.9 0.4 collective-permute-start.22
  58.2 9.9 %collective-permute-done.4.refs_6_ = bf16[2,256,512]{2,1,0:T(8,128)(2,1)} collective-permute-done((bf16[2,256,512]{2,1,0:T(8,128)(2,1)S(1)}, bf16[2,256,512]{2,1,0:T(8,128)(2,1)}, u32[]{:S(2)}, u32[]{:S(2)}) %collective-permute-start.4) | collective-permute-done | bytes 524320 | tf_op jit(solution)/shard_map/ppermute | solution.py:117
  68.1 0.0 collective-permute-start.5
  68.1 0.0 collective-permute-done.22.refs_11_
  68.1 5.0 %collective-permute-start.2 = (bf16[384,256]{1,0:T(8,128)(2,1)}, bf16[384,256]{1,0:T(8,128)(2,1)}, u32[]{:S(2)}, u32[]{:S(2)}) collective-permute-start(bf16[384,256]{1,0:T(8,128)(2,1)} %get-tuple-element.24), channel_id=1, source_target_pairs={{0,12},{4,0},{8,4},{12,8},{1,13},{5,1},{9,5},{13,9},{2,14},{6,2},{... | collective-permute-start | bytes 589832 | tf_op jit(solution)/shard_map/ppermute | solution.py:162
  73.2 0.0 collective-permute-done.16.refs_5_
  73.2 0.2 collective-permute-start.7
  73.4 0.0 collective-permute-done.18.refs_7_
  73.5 0.8 copy-done.6
  74.3 0.3 collective-permute-start.9
  74.6 1.0 copy.8
  75.6 5.3 %shard_map.65 = (bf16[384,256]{1,0:T(8,128)(2,1)}, bf16[384,256]{1,0:T(8,128)(2,1)}, bf16[384,256]{1,0:T(8,128)(2,1)}, bf16[384,256]{1,0:T(8,128)(2,1)}) custom-call(s32[2]{0:T(128)} %pad_add_fusion.at_ref, bf16[384,256]{1,0:T(8,128)(2,1)} %get-tuple-element.29.refs_0_, bf16[384,256]{1,0:T(8,128)(2,1)} %copy-done.13, bf16[384,256]{1,0:T(8,128)(2,1)} %copy-done.14, ...), custom_call_target="tpu_custom_call" | custom-call | flops 805306368 | bytes 2097152 | tf_op jit(solution)/shard_map/pallas_call | solution.py:165
  80.9 0.0 collective-permute-done.2.refs_3_
  80.9 1.9 %collective-permute-start.23 = (bf16[384,256]{1,0:T(8,128)(2,1)}, bf16[384,256]{1,0:T(8,128)(2,1)S(1)}, u32[]{:S(2)}, u32[]{:S(2)}) collective-permute-start(bf16[384,256]{1,0:T(8,128)(2,1)} %get-tuple-element.34), channel_id=1, source_target_pairs={{0,4},{4,8},{8,12},{12,0},{1,5},{5,9},{9,13},{13,1},{2,6},{6,10},{... | collective-permute-start | bytes 589832 | tf_op jit(solution)/shard_map/ppermute | solution.py:176
  82.8 1.0 collective-permute-start.24
  83.8 2.8 %collective-permute-start.25 = (bf16[384,256]{1,0:T(8,128)(2,1)}, bf16[384,256]{1,0:T(8,128)(2,1)S(1)}, u32[]{:S(2)}, u32[]{:S(2)}) collective-permute-start(bf16[384,256]{1,0:T(8,128)(2,1)} %get-tuple-element.36), channel_id=1, source_target_pairs={{0,12},{4,0},{8,4},{12,8},{1,13},{5,1},{9,5},{13,9},{2,14},{6,2},{... | collective-permute-start | bytes 589832 | tf_op jit(solution)/shard_map/ppermute | solution.py:176
  86.7 0.0 collective-permute-done.3.refs_5_
  86.7 0.0 collective-permute-done.5.refs_7_
  86.7 1.0 copy-done.3
  87.7 5.3 %shard_map.64 = (bf16[384,256]{1,0:T(8,128)(2,1)}, bf16[384,256]{1,0:T(8,128)(2,1)}, bf16[384,256]{1,0:T(8,128)(2,1)}, bf16[384,256]{1,0:T(8,128)(2,1)}) custom-call(s32[2]{0:T(128)} %pad_add_fusion.at_ref, bf16[384,256]{1,0:T(8,128)(2,1)} %get-tuple-element.21.refs_0_, bf16[384,256]{1,0:T(8,128)(2,1)} %copy-done.11, bf16[384,256]{1,0:T(8,128)(2,1)} %copy-done.12, ...), custom_call_target="tpu_custom_call" | custom-call | flops 805306368 | bytes 2097152 | tf_op jit(solution)/shard_map/pallas_call | solution.py:165
  93.0 1.1 collective-permute-start.11
  94.0 0.0 collective-permute-done.23.refs_1_
  94.0 2.8 %collective-permute-start.12 = (bf16[384,256]{1,0:T(8,128)(2,1)}, bf16[384,256]{1,0:T(8,128)(2,1)S(1)}, u32[]{:S(2)}, u32[]{:S(2)}) collective-permute-start(bf16[384,256]{1,0:T(8,128)(2,1)} %get-tuple-element.28), channel_id=1, source_target_pairs={{0,12},{4,0},{8,4},{12,8},{1,13},{5,1},{9,5},{13,9},{2,14},{6,2},{... | collective-permute-start | bytes 589832 | tf_op jit(solution)/shard_map/ppermute | solution.py:176
  96.8 9.4 %collective-permute-done.24.refs_2_ = bf16[384,256]{1,0:T(8,128)(2,1)S(1)} collective-permute-done((bf16[384,256]{1,0:T(8,128)(2,1)}, bf16[384,256]{1,0:T(8,128)(2,1)S(1)}, u32[]{:S(2)}, u32[]{:S(2)}) %collective-permute-start.24) | collective-permute-done | bytes 196640 | tf_op jit(solution)/shard_map/ppermute | solution.py:176
  106.3 0.0 collective-permute-done.25.refs_3_
  106.3 0.7 copy-done.17
  107.0 0.1 copy-done.18
  107.0 4.6 %shard_map.66.refs_4_ = bf16[384,2048]{1,0:T(8,128)(2,1)} custom-call(s32[2]{0:T(128)} %pad_add_fusion.at_ref, bf16[384,2048]{1,0:T(8,128)(2,1)} %bitcast.6, bf16[384,256]{1,0:T(8,128)(2,1)} %get-tuple-element.33.refs_0_, bf16[384,256]{1,0:T(8,128)(2,1)} %copy-done.16, bf16[384,256]{1,0:T(8,128)(2,1)} %copy-done.17, bf16[384,256]{1,0:T(8,128)(2,1)} %copy-done.18), custom_call_target="tpu_custom_call" | custom-call | flops 4718592 | bytes 2359296 | tf_op jit(solution)/shard_map/pallas_call | solution.py:183
  111.7 3.7 %collective-permute-done.11.refs_2_ = bf16[384,256]{1,0:T(8,128)(2,1)S(1)} collective-permute-done((bf16[384,256]{1,0:T(8,128)(2,1)}, bf16[384,256]{1,0:T(8,128)(2,1)S(1)}, u32[]{:S(2)}, u32[]{:S(2)}) %collective-permute-start.11) | collective-permute-done | bytes 196640 | tf_op jit(solution)/shard_map/ppermute | solution.py:176
  115.4 0.7 copy-done.20
  116.1 0.1 copy-done.21
  116.2 4.6 %shard_map.67 = bf16[384,2048]{1,0:T(8,128)(2,1)} custom-call(s32[2]{0:T(128)} %pad_add_fusion.at_ref, bf16[384,2048]{1,0:T(8,128)(2,1)} %bitcast.7, bf16[384,256]{1,0:T(8,128)(2,1)} %get-tuple-element.25.refs_0_, bf16[384,256]{1,0:T(8,128)(2,1)} %copy-done.19, bf16[384,256]{1,0:T(8,128)(2,1)} %copy-done.20, ...), custom_call_target="tpu_custom_call", output_to_operand_aliasing={{}: (6, {})} | custom-call | flops 4718592 | bytes 2359296 | tf_op jit(solution)/shard_map/pallas_call | solution.py:183
  (50 shorter events, 0.1 us)
Async XLA Ops:
  0.0 18.7 %copy-start = (bf16[4,256,1024]{2,1,0:T(8,128)(2,1)S(1)}, bf16[4,256,1024]{2,1,0:T(8,128)(2,1)}, u32[]{:S(2)}) copy-start(bf16[4,256,1024]{2,1,0:T(8,128)(2,1)} %param.10) | copy-start | bytes 6291460
  8.4 9.6 %copy-start.24 = (bf16[384,256]{1,0:T(8,128)(2,1)S(1)}, bf16[384,256]{1,0:T(8,128)(2,1)}, u32[]{:S(2)}) copy-start(bf16[384,256]{1,0:T(8,128)(2,1)} %get-tuple-element.22) | copy-start | bytes 589828
  8.4 11.2 %collective-permute-start.13 = (bf16[384,256]{1,0:T(8,128)(2,1)}, bf16[384,256]{1,0:T(8,128)(2,1)S(1)}, u32[]{:S(2)}, u32[]{:S(2)}) collective-permute-start(bf16[384,256]{1,0:T(8,128)(2,1)} %get-tuple-element.30), channel_id=1, source_target_pairs={{0,4},{4,8},{8,12},{12,0},{1,5},{5,9},{9,13},{13,1},{2,6},{6,10},{... | collective-permute-start | bytes 589832 | tf_op jit(solution)/shard_map/ppermute | solution.py:162
  11.4 17.6 %collective-permute-start.14 = (bf16[384,256]{1,0:T(8,128)(2,1)}, bf16[384,256]{1,0:T(8,128)(2,1)S(1)}, u32[]{:S(2)}, u32[]{:S(2)}) collective-permute-start(bf16[384,256]{1,0:T(8,128)(2,1)} %get-tuple-element.31), channel_id=1, source_target_pairs={{0,8},{4,12},{8,0},{12,4},{1,9},{5,13},{9,1},{13,5},{2,10},{6,14},... | collective-permute-start | bytes 589832 | tf_op jit(solution)/shard_map/ppermute | solution.py:162
  14.0 15.7 %collective-permute-start.15 = (bf16[384,256]{1,0:T(8,128)(2,1)}, bf16[384,256]{1,0:T(8,128)(2,1)S(1)}, u32[]{:S(2)}, u32[]{:S(2)}) collective-permute-start(bf16[384,256]{1,0:T(8,128)(2,1)} %get-tuple-element.32), channel_id=1, source_target_pairs={{0,12},{4,0},{8,4},{12,8},{1,13},{5,1},{9,5},{13,9},{2,14},{6,2},{... | collective-permute-start | bytes 589832 | tf_op jit(solution)/shard_map/ppermute | solution.py:162
  16.6 28.5 %collective-permute-start.19 = (bf16[2,256,256]{2,1,0:T(8,128)(2,1)S(1)}, bf16[2,256,256]{2,1,0:T(8,128)(2,1)S(1)}, u32[]{:S(2)}, u32[]{:S(2)}) collective-permute-start(bf16[2,256,256]{2,1,0:T(8,128)(2,1)S(1)} %get-tuple-element.40), channel_id=1, source_target_pairs={{2,0},{3,1},{6,4},{7,5},{10,8},{11,9},{14,12},{15,13},{18,16},{19,... | collective-permute-start | bytes 786440 | tf_op jit(solution)/shard_map/ppermute | solution.py:117
  17.9 1.6 %copy-start.23 = (bf16[384,256]{1,0:T(8,128)(2,1)S(1)}, bf16[384,256]{1,0:T(8,128)(2,1)}, u32[]{:S(2)}) copy-start(bf16[384,256]{1,0:T(8,128)(2,1)} %get-tuple-element.23) | copy-start | bytes 589828
  17.9 14.3 %collective-permute-start = (bf16[384,256]{1,0:T(8,128)(2,1)S(1)}, bf16[384,256]{1,0:T(8,128)(2,1)S(1)}, u32[]{:S(2)}, u32[]{:S(2)}) collective-permute-start(bf16[384,256]{1,0:T(8,128)(2,1)S(1)} %copy-done.24), channel_id=1, source_target_pairs={{0,4},{4,8},{8,12},{12,0},{1,5},{5,9},{9,13},{13,1},{2,6},{6,10},{... | collective-permute-start | bytes 589832 | tf_op jit(solution)/shard_map/ppermute | solution.py:162
  18.9 27.7 %copy-start.2 = (bf16[2,256,1024]{2,1,0:T(8,128)(2,1)}, bf16[2,256,1024]{2,1,0:T(8,128)(2,1)S(1)}, u32[]{:S(2)}) copy-start(bf16[2,256,1024]{2,1,0:T(8,128)(2,1)S(1)} %get-tuple-element.43.refs_4_) | copy-start | bytes 3145732
  18.9 62.0 %copy-start.1 = (bf16[2,256,1024]{2,1,0:T(8,128)(2,1)}, bf16[2,256,1024]{2,1,0:T(8,128)(2,1)S(1)}, u32[]{:S(2)}) copy-start(bf16[2,256,1024]{2,1,0:T(8,128)(2,1)S(1)} %get-tuple-element.44.refs_4_) | copy-start | bytes 3145732
  18.9 55.7 %copy-start.22 = (bf16[4,1024]{1,0:T(4,128)(2,1)S(1)}, bf16[4,1024]{1,0:T(4,128)(2,1)}, u32[]{:S(2)}) copy-start(bf16[4,1024]{1,0:T(4,128)(2,1)} %param.11) | copy-start | bytes 24580
  19.5 53.9 %copy-start.13 = (bf16[384,256]{1,0:T(8,128)(2,1)}, bf16[384,256]{1,0:T(8,128)(2,1)S(1)}, u32[]{:S(2)}) copy-start(bf16[384,256]{1,0:T(8,128)(2,1)S(1)} %collective-permute-done.13.refs_1_) | copy-start | bytes 589828
  19.5 24.3 %collective-permute-start.1 = (bf16[384,256]{1,0:T(8,128)(2,1)S(1)}, bf16[384,256]{1,0:T(8,128)(2,1)S(1)}, u32[]{:S(2)}, u32[]{:S(2)}) collective-permute-start(bf16[384,256]{1,0:T(8,128)(2,1)S(1)} %copy-done.23), channel_id=1, source_target_pairs={{0,8},{4,12},{8,0},{12,4},{1,9},{5,13},{9,1},{13,5},{2,10},{6,14},... | collective-permute-start | bytes 589832 | tf_op jit(solution)/shard_map/ppermute | solution.py:162
  29.0 44.4 %copy-start.14 = (bf16[384,256]{1,0:T(8,128)(2,1)}, bf16[384,256]{1,0:T(8,128)(2,1)S(1)}, u32[]{:S(2)}) copy-start(bf16[384,256]{1,0:T(8,128)(2,1)S(1)} %collective-permute-done.14.refs_2_) | copy-start | bytes 589828
  29.0 17.5 %collective-permute-start.21 = (bf16[2,256,256]{2,1,0:T(8,128)(2,1)S(1)}, bf16[2,256,256]{2,1,0:T(8,128)(2,1)S(1)}, u32[]{:S(2)}, u32[]{:S(2)}) collective-permute-start(bf16[2,256,256]{2,1,0:T(8,128)(2,1)S(1)} %get-tuple-element.37), channel_id=1, source_target_pairs={{3,1},{7,5},{11,9},{15,13},{19,17},{23,21},{27,25},{31,29}} | collective-permute-start | bytes 786440 | tf_op jit(solution)/shard_map/ppermute | solution.py:117
  29.7 43.7 %copy-start.15 = (bf16[384,256]{1,0:T(8,128)(2,1)}, bf16[384,256]{1,0:T(8,128)(2,1)S(1)}, u32[]{:S(2)}) copy-start(bf16[384,256]{1,0:T(8,128)(2,1)S(1)} %collective-permute-done.15.refs_3_) | copy-start | bytes 589828
  29.7 43.4 %collective-permute-start.16 = (bf16[2,256,1024]{2,1,0:T(8,128)(2,1)S(1)}, bf16[2,256,1024]{2,1,0:T(8,128)(2,1)S(1)}, u32[]{:S(2)}, u32[]{:S(2)}) collective-permute-start(bf16[2,256,1024]{2,1,0:T(8,128)(2,1)S(1)} %get-tuple-element.43.refs_4_), channel_id=1, source_target_pairs={{0,1},{1,0},{2,3},{3,2},{4,5},{5,4},{6,7},{7,6},{8,9},{9,8},{10,11... | collective-permute-start | bytes 3145736 | tf_op jit(solution)/shard_map/ppermute | solution.py:115
  32.2 41.2 %copy-start.11 = (bf16[384,256]{1,0:T(8,128)(2,1)}, bf16[384,256]{1,0:T(8,128)(2,1)S(1)}, u32[]{:S(2)}) copy-start(bf16[384,256]{1,0:T(8,128)(2,1)S(1)} %collective-permute-done.refs_1_) | copy-start | bytes 589828
  32.2 24.5 %collective-permute-start.17 = (bf16[2,256,512]{2,1,0:T(8,128)(2,1)S(1)}, bf16[2,256,512]{2,1,0:T(8,128)(2,1)S(1)}, u32[]{:S(2)}, u32[]{:S(2)}) collective-permute-start(bf16[2,256,512]{2,1,0:T(8,128)(2,1)S(1)} %get-tuple-element.41), channel_id=1, source_target_pairs={{0,2},{1,3},{2,0},{3,1},{4,6},{5,7},{6,4},{7,5},{8,10},{9,11},{10,... | collective-permute-start | bytes 1572872 | tf_op jit(solution)/shard_map/ppermute | solution.py:117
  43.9 11.2 %copy-start.12 = (bf16[384,256]{1,0:T(8,128)(2,1)}, bf16[384,256]{1,0:T(8,128)(2,1)S(1)}, u32[]{:S(2)}) copy-start(bf16[384,256]{1,0:T(8,128)(2,1)S(1)} %collective-permute-done.1.refs_2_) | copy-start | bytes 589828
  43.9 11.2 %collective-permute-start.6 = (bf16[2,256,256]{2,1,0:T(8,128)(2,1)S(1)}, bf16[2,256,256]{2,1,0:T(8,128)(2,1)}, u32[]{:S(2)}, u32[]{:S(2)}) collective-permute-start(bf16[2,256,256]{2,1,0:T(8,128)(2,1)S(1)} %get-tuple-element.39), channel_id=1, source_target_pairs={{2,0},{3,1},{6,4},{7,5},{10,8},{11,9},{14,12},{15,13},{18,16},{19,... | collective-permute-start | bytes 786440 | tf_op jit(solution)/shard_map/ppermute | solution.py:117
  45.2 30.4 %copy-start.7 = (bf16[2,256,256]{2,1,0:T(8,128)(2,1)}, bf16[2,256,256]{2,1,0:T(8,128)(2,1)S(1)}, u32[]{:S(2)}) copy-start(bf16[2,256,256]{2,1,0:T(8,128)(2,1)S(1)} %collective-permute-done.19.refs_8_) | copy-start | bytes 786436
  45.2 9.9 %collective-permute-start.8 = (bf16[2,256,256]{2,1,0:T(8,128)(2,1)S(1)}, bf16[2,256,256]{2,1,0:T(8,128)(2,1)}, u32[]{:S(2)}, u32[]{:S(2)}) collective-permute-start(bf16[2,256,256]{2,1,0:T(8,128)(2,1)S(1)} %get-tuple-element.38), channel_id=1, source_target_pairs={{3,1},{7,5},{11,9},{15,13},{19,17},{23,21},{27,25},{31,29}} | collective-permute-start | bytes 786440 | tf_op jit(solution)/shard_map/ppermute | solution.py:117
  46.5 26.9 %copy-start.8 = (bf16[2,256,256]{2,1,0:T(8,128)(2,1)}, bf16[2,256,256]{2,1,0:T(8,128)(2,1)S(1)}, u32[]{:S(2)}) copy-start(bf16[2,256,256]{2,1,0:T(8,128)(2,1)S(1)} %collective-permute-done.21.refs_10_) | copy-start | bytes 786436
  46.5 40.1 %collective-permute-start.3 = (bf16[2,256,1024]{2,1,0:T(8,128)(2,1)S(1)}, bf16[2,256,1024]{2,1,0:T(8,128)(2,1)S(1)}, u32[]{:S(2)}, u32[]{:S(2)}) collective-permute-start(bf16[2,256,1024]{2,1,0:T(8,128)(2,1)S(1)} %get-tuple-element.44.refs_4_), channel_id=1, source_target_pairs={{0,1},{1,0},{2,3},{3,2},{4,5},{5,4},{6,7},{7,6},{8,9},{9,8},{10,11... | collective-permute-start | bytes 3145736 | tf_op jit(solution)/shard_map/ppermute | solution.py:115
  55.0 13.1 %collective-permute-start.4 = (bf16[2,256,512]{2,1,0:T(8,128)(2,1)S(1)}, bf16[2,256,512]{2,1,0:T(8,128)(2,1)}, u32[]{:S(2)}, u32[]{:S(2)}) collective-permute-start(bf16[2,256,512]{2,1,0:T(8,128)(2,1)S(1)} %get-tuple-element.42), channel_id=1, source_target_pairs={{0,2},{1,3},{2,0},{3,1},{4,6},{5,7},{6,4},{7,5},{8,10},{9,11},{10,... | collective-permute-start | bytes 1572872 | tf_op jit(solution)/shard_map/ppermute | solution.py:117
  55.0 2.8 %collective-permute-start.20 = (bf16[2,256,256]{2,1,0:T(8,128)(2,1)S(1)}, bf16[2,256,256]{2,1,0:T(8,128)(2,1)S(1)}, u32[]{:S(2)}, u32[]{:S(2)}) collective-permute-start(bf16[2,256,256]{2,1,0:T(8,128)(2,1)S(1)} %collective-permute-done.19.refs_8_), channel_id=1, source_target_pairs={{0,1},{1,0},{2,3},{3,2},{4,5},{5,4},{6,7},{7,6},{8,9},{9,8},{10,11... | collective-permute-start | bytes 786440 | tf_op jit(solution)/shard_map/ppermute | solution.py:119
  56.7 16.4 %copy-start.5 = (bf16[2,256,512]{2,1,0:T(8,128)(2,1)}, bf16[2,256,512]{2,1,0:T(8,128)(2,1)S(1)}, u32[]{:S(2)}) copy-start(bf16[2,256,512]{2,1,0:T(8,128)(2,1)S(1)} %collective-permute-done.17.refs_6_) | copy-start | bytes 1572868
  56.7 16.7 %collective-permute-start.18 = (bf16[2,256,512]{2,1,0:T(8,128)(2,1)S(1)}, bf16[2,256,512]{2,1,0:T(8,128)(2,1)S(1)}, u32[]{:S(2)}, u32[]{:S(2)}) collective-permute-start(bf16[2,256,512]{2,1,0:T(8,128)(2,1)S(1)} %collective-permute-done.17.refs_6_), channel_id=1, source_target_pairs={{0,1},{1,0},{2,3},{3,2},{4,5},{5,4},{6,7},{7,6},{8,9},{9,8},{10,11... | collective-permute-start | bytes 1572872 | tf_op jit(solution)/shard_map/ppermute | solution.py:119
  57.9 15.6 %copy-start.9 = (bf16[2,256,256]{2,1,0:T(8,128)(2,1)}, bf16[2,256,256]{2,1,0:T(8,128)(2,1)S(1)}, u32[]{:S(2)}) copy-start(bf16[2,256,256]{2,1,0:T(8,128)(2,1)S(1)} %collective-permute-done.20.refs_9_) | copy-start | bytes 786436
  57.9 10.3 %collective-permute-start.22 = (bf16[2,256,256]{2,1,0:T(8,128)(2,1)S(1)}, bf16[2,256,256]{2,1,0:T(8,128)(2,1)S(1)}, u32[]{:S(2)}, u32[]{:S(2)}) collective-permute-start(bf16[2,256,256]{2,1,0:T(8,128)(2,1)S(1)} %collective-permute-done.21.refs_10_), channel_id=1, source_target_pairs={{0,1},{1,0},{2,3},{3,2},{4,5},{5,4},{6,7},{7,6},{8,9},{9,8},{10,11... | collective-permute-start | bytes 786440 | tf_op jit(solution)/shard_map/ppermute | solution.py:119
  68.1 18.6 %collective-permute-start.5 = (bf16[2,256,512]{2,1,0:T(8,128)(2,1)}, bf16[2,256,512]{2,1,0:T(8,128)(2,1)}, u32[]{:S(2)}, u32[]{:S(2)}) collective-permute-start(bf16[2,256,512]{2,1,0:T(8,128)(2,1)} %collective-permute-done.4.refs_6_), channel_id=1, source_target_pairs={{0,1},{1,0},{2,3},{3,2},{4,5},{5,4},{6,7},{7,6},{8,9},{9,8},{10,11... | collective-permute-start | bytes 1572872 | tf_op jit(solution)/shard_map/ppermute | solution.py:119
  68.1 5.3 %copy-start.10 = (bf16[2,256,256]{2,1,0:T(8,128)(2,1)}, bf16[2,256,256]{2,1,0:T(8,128)(2,1)S(1)}, u32[]{:S(2)}) copy-start(bf16[2,256,256]{2,1,0:T(8,128)(2,1)S(1)} %collective-permute-done.22.refs_11_) | copy-start | bytes 786436
  68.1 12.8 %collective-permute-start.2 = (bf16[384,256]{1,0:T(8,128)(2,1)}, bf16[384,256]{1,0:T(8,128)(2,1)}, u32[]{:S(2)}, u32[]{:S(2)}) collective-permute-start(bf16[384,256]{1,0:T(8,128)(2,1)} %get-tuple-element.24), channel_id=1, source_target_pairs={{0,12},{4,0},{8,4},{12,8},{1,13},{5,1},{9,5},{13,9},{2,14},{6,2},{... | collective-permute-start | bytes 589832 | tf_op jit(solution)/shard_map/ppermute | solution.py:162
  73.2 2.4 %copy-start.4 = (bf16[2,256,1024]{2,1,0:T(8,128)(2,1)}, bf16[2,256,1024]{2,1,0:T(8,128)(2,1)S(1)}, u32[]{:S(2)}) copy-start(bf16[2,256,1024]{2,1,0:T(8,128)(2,1)S(1)} %collective-permute-done.16.refs_5_) | copy-start | bytes 3145732
  73.2 9.6 %collective-permute-start.7 = (bf16[2,256,256]{2,1,0:T(8,128)(2,1)}, bf16[2,256,256]{2,1,0:T(8,128)(2,1)}, u32[]{:S(2)}, u32[]{:S(2)}) collective-permute-start(bf16[2,256,256]{2,1,0:T(8,128)(2,1)} %collective-permute-done.6.refs_8_), channel_id=1, source_target_pairs={{0,1},{1,0},{2,3},{3,2},{4,5},{5,4},{6,7},{7,6},{8,9},{9,8},{10,11... | collective-permute-start | bytes 786440 | tf_op jit(solution)/shard_map/ppermute | solution.py:119
  73.5 0.8 copy-start.6
  74.3 9.5 %collective-permute-start.9 = (bf16[2,256,256]{2,1,0:T(8,128)(2,1)}, bf16[2,256,256]{2,1,0:T(8,128)(2,1)}, u32[]{:S(2)}, u32[]{:S(2)}) collective-permute-start(bf16[2,256,256]{2,1,0:T(8,128)(2,1)} %collective-permute-done.8.refs_10_), channel_id=1, source_target_pairs={{0,1},{1,0},{2,3},{3,2},{4,5},{5,4},{6,7},{7,6},{8,9},{9,8},{10,11... | collective-permute-start | bytes 786440 | tf_op jit(solution)/shard_map/ppermute | solution.py:119
  80.9 13.1 %collective-permute-start.23 = (bf16[384,256]{1,0:T(8,128)(2,1)}, bf16[384,256]{1,0:T(8,128)(2,1)S(1)}, u32[]{:S(2)}, u32[]{:S(2)}) collective-permute-start(bf16[384,256]{1,0:T(8,128)(2,1)} %get-tuple-element.34), channel_id=1, source_target_pairs={{0,4},{4,8},{8,12},{12,0},{1,5},{5,9},{9,13},{13,1},{2,6},{6,10},{... | collective-permute-start | bytes 589832 | tf_op jit(solution)/shard_map/ppermute | solution.py:176
  82.8 23.5 %collective-permute-start.24 = (bf16[384,256]{1,0:T(8,128)(2,1)}, bf16[384,256]{1,0:T(8,128)(2,1)S(1)}, u32[]{:S(2)}, u32[]{:S(2)}) collective-permute-start(bf16[384,256]{1,0:T(8,128)(2,1)} %get-tuple-element.35), channel_id=1, source_target_pairs={{0,8},{4,12},{8,0},{12,4},{1,9},{5,13},{9,1},{13,5},{2,10},{6,14},... | collective-permute-start | bytes 589832 | tf_op jit(solution)/shard_map/ppermute | solution.py:176
  83.8 22.5 %collective-permute-start.25 = (bf16[384,256]{1,0:T(8,128)(2,1)}, bf16[384,256]{1,0:T(8,128)(2,1)S(1)}, u32[]{:S(2)}, u32[]{:S(2)}) collective-permute-start(bf16[384,256]{1,0:T(8,128)(2,1)} %get-tuple-element.36), channel_id=1, source_target_pairs={{0,12},{4,0},{8,4},{12,8},{1,13},{5,1},{9,5},{13,9},{2,14},{6,2},{... | collective-permute-start | bytes 589832 | tf_op jit(solution)/shard_map/ppermute | solution.py:176
  86.7 1.0 copy-start.3
  93.0 18.7 %collective-permute-start.10 = (bf16[384,256]{1,0:T(8,128)(2,1)}, bf16[384,256]{1,0:T(8,128)(2,1)S(1)}, u32[]{:S(2)}, u32[]{:S(2)}) collective-permute-start(bf16[384,256]{1,0:T(8,128)(2,1)} %get-tuple-element.26), channel_id=1, source_target_pairs={{0,4},{4,8},{8,12},{12,0},{1,5},{5,9},{9,13},{13,1},{2,6},{6,10},{... | collective-permute-start | bytes 589832 | tf_op jit(solution)/shard_map/ppermute | solution.py:176
  93.0 22.4 %collective-permute-start.11 = (bf16[384,256]{1,0:T(8,128)(2,1)}, bf16[384,256]{1,0:T(8,128)(2,1)S(1)}, u32[]{:S(2)}, u32[]{:S(2)}) collective-permute-start(bf16[384,256]{1,0:T(8,128)(2,1)} %get-tuple-element.27), channel_id=1, source_target_pairs={{0,8},{4,12},{8,0},{12,4},{1,9},{5,13},{9,1},{13,5},{2,10},{6,14},... | collective-permute-start | bytes 589832 | tf_op jit(solution)/shard_map/ppermute | solution.py:176
  94.0 12.3 %copy-start.16 = (bf16[384,256]{1,0:T(8,128)(2,1)}, bf16[384,256]{1,0:T(8,128)(2,1)S(1)}, u32[]{:S(2)}) copy-start(bf16[384,256]{1,0:T(8,128)(2,1)S(1)} %collective-permute-done.23.refs_1_) | copy-start | bytes 589828
  94.0 21.4 %collective-permute-start.12 = (bf16[384,256]{1,0:T(8,128)(2,1)}, bf16[384,256]{1,0:T(8,128)(2,1)S(1)}, u32[]{:S(2)}, u32[]{:S(2)}) collective-permute-start(bf16[384,256]{1,0:T(8,128)(2,1)} %get-tuple-element.28), channel_id=1, source_target_pairs={{0,12},{4,0},{8,4},{12,8},{1,13},{5,1},{9,5},{13,9},{2,14},{6,2},{... | collective-permute-start | bytes 589832 | tf_op jit(solution)/shard_map/ppermute | solution.py:176
  106.3 0.7 copy-start.17
  106.3 0.8 copy-start.18
  111.7 3.8 %copy-start.19 = (bf16[384,256]{1,0:T(8,128)(2,1)}, bf16[384,256]{1,0:T(8,128)(2,1)S(1)}, u32[]{:S(2)}) copy-start(bf16[384,256]{1,0:T(8,128)(2,1)S(1)} %collective-permute-done.10.refs_1_) | copy-start | bytes 589828
  115.4 0.7 copy-start.20
  115.4 0.8 copy-start.21

commit v2 on v1

v2 whole, which is shorter than its diff:
```python
import functools

import jax
import jax.numpy as jnp
from jax import lax
from jax.experimental import pallas as pl
from jax.experimental.pallas import tpu as pltpu
from jax.sharding import PartitionSpec as P


GD = 128
BLK = 1024
TILE = 256


VMEM = pl.BlockSpec(memory_space=pltpu.VMEM)
HBM = pl.BlockSpec(memory_space=pltpu.HBM)


def gelu(x):
    half = 0.5 * x
    return half + half * jnp.tanh(x * (0.7978845608028654 + 0.035677408136300125 * (x * x)))


def partner(here, step, shards):
    if shards & (shards - 1) == 0:
        return here ^ step, here ^ step
    return lax.rem(here + step, shards), lax.rem(here + shards - step, shards)


def swap_pairs(count, step):
    if count & (count - 1) == 0:
        return [(i, i ^ step) for i in range(count)]
    return [(i, (i + step) % count) for i in range(count)]


def steps_of(shards):
    return list(range(shards - 1, 0, -1))


def norm_kernel(shards, chunks, width, rows_step, cuts, value_ref, gain_ref, bias_ref, weight_ref, *refs):
    nouts = shards * chunks
    outs, parts = refs[:nouts], refs[nouts:nouts + len(cuts)]
    value, gain, bias, held, sems = refs[nouts + len(cuts):]
    here = lax.axis_index("sp")
    span = chunks * width
    rows = value.shape[0]
    loads = 3 if rows % (3 * rows_step) == 0 else 1
    block = rows // loads
    pairs = [(value_ref.at[pl.ds(0, block), :], value.at[pl.ds(0, block), :]), (gain_ref, gain), (bias_ref, bias)]
    pairs += [(value_ref.at[pl.ds(k * block, block), :], value.at[pl.ds(k * block, block), :]) for k in range(1, loads)]
    for part, (first, count, low, cols) in zip(parts, cuts):
        pairs.append((weight_ref.at[pl.ds(first, count), :, pl.ds(low, cols)], part))
    copies = [pltpu.make_async_copy(source, target, sems.at[k]) for k, (source, target) in enumerate(pairs)]
    for copy in copies:
        copy.start()
    for k in range(loads):
        if k == 0:
            for copy in copies[:3]:
                copy.wait()
            scale = gain[...].astype(jnp.float32).reshape(1, -1)
            offset = bias[...].astype(jnp.float32).reshape(1, -1)
        else:
            copies[2 + k].wait()

        def step(i, carry, k=k):
            at = pl.ds(pl.multiple_of(k * block + i * rows_step, rows_step), rows_step)
            act = gelu(value[at, :].astype(jnp.float32))
            centred = act - jnp.mean(act, axis=-1, keepdims=True)
            var = jnp.mean(jnp.square(centred), axis=-1, keepdims=True)
            held[at, :] = (centred * lax.rsqrt(var + 1e-06) * scale + offset).astype(jnp.bfloat16)
            return carry

        steps = block // rows_step
        lax.fori_loop(0, steps, step, 0, unroll=8 if steps % 8 == 0 else 1)
        at = pl.ds(k * block, block)
        for c in range(chunks):
            for s in range(shards):
                start = pl.multiple_of(partner(here, s, shards)[0] * span + c * width, GD)
                outs[c * shards + s][at, :] = held[at, pl.ds(start, width)]
    for copy in copies[2 + loads:]:
        copy.wait()


def mix_kernel(shards, length, first, layout, *refs):
    pieces, refs = refs[:shards], refs[shards:]
    weights, refs = refs[:len(layout)], refs[len(layout):]
    bias_ref, outs, (values, mixed) = refs[0], refs[1:1 + shards], refs[1 + shards:]
    here, row = lax.axis_index("sp"), lax.axis_index("dp")
    rows = pieces[0].shape[0]
    groups = pieces[0].shape[1] // GD
    nblocks = -(-length // BLK)
    for s in range(shards):
        origin = partner(here, s, shards)[1]
        mixed[pl.ds(pl.multiple_of(origin * rows, rows), rows), :] = pieces[s][...]
    for g in range(groups):
        for b in range(nblocks):
            count = min(BLK, length - b * BLK)
            lanes = pl.ds(b * GD, GD)
            values[g, pl.ds(0, count), lanes] = mixed[pl.ds(b * BLK, count), pl.ds(g * GD, GD)]
            if count < BLK:
                values[g, pl.ds(count, BLK - count), lanes] = jnp.zeros((BLK - count, GD), jnp.bfloat16)
    tiles = {}
    for ref, (flip, fixed, low, skip) in zip(weights, layout):
        tiles.setdefault((flip, fixed), []).append((ref, low, skip))
    for (flip, fixed), parts in tiles.items():
        at_row = row ^ flip if fixed is None else fixed
        top = pl.multiple_of(at_row * TILE, TILE)
        for g in range(groups):
            total = None
            for ref, low, skip in parts:
                part = ref[skip + g] if fixed is None else ref[skip + g, pl.ds(fixed * TILE, TILE), :]
                cols = lax.broadcasted_iota(jnp.int32, part.shape, 1) + low
                keep = cols <= lax.broadcasted_iota(jnp.int32, part.shape, 0) + top
                part = jnp.where(keep, part, jnp.zeros_like(part))
                term = jnp.dot(part, values[g, pl.ds(low, part.shape[1]), :], preferred_element_type=jnp.float32)
                total = term if total is None else total + term
            shift = bias_ref[pl.ds(first + g, 1), pl.ds(top, TILE)].astype(jnp.float32)
            shift = jnp.broadcast_to(shift, (GD, TILE)).T
            for b in range(nblocks):
                block = total[:, b * GD:(b + 1) * GD] + shift
                mixed[pl.ds(b * BLK + top, TILE), pl.ds(g * GD, GD)] = block.astype(jnp.bfloat16)
    for s in range(shards):
        target = partner(here, s, shards)[0]
        outs[s][...] = mixed[pl.ds(pl.multiple_of(target * rows, rows), rows), :]


def gate_kernel(shards, chunks, chunk, rows_step, gate_ref, *refs):
    pieces = refs[:shards]
    out_ref, held, sems = refs[-3:]
    here = lax.axis_index("sp")
    width = pieces[0].shape[1]
    copies = []
    for s in range(shards):
        start = (partner(here, s, shards)[1] * chunks + chunk) * width
        lanes = pl.ds(pl.multiple_of(start, GD), width)

        def step(i, carry, s=s, lanes=lanes):
            rows = pl.ds(pl.multiple_of(i * rows_step, rows_step), rows_step)
            gate = gelu(gate_ref[rows, lanes].astype(jnp.float32))
            held[s, rows, :] = (gate * pieces[s][rows, :].astype(jnp.float32)).astype(jnp.bfloat16)
            return carry

        lax.fori_loop(0, gate_ref.shape[0] // rows_step, step, 0, unroll=4)
        copies.append(pltpu.make_async_copy(held.at[s], out_ref.at[:, lanes], sems.at[s]))
        copies[-1].start()
    for copy in copies:
        copy.wait()


def exchange_rows(weight, parts, ndp, first):
    got = [(weight[0], 0, None, 0, first), (weight[1], 1, None, 0, first)]
    for low, least, part in parts:
        far = lax.ppermute(part, "dp", [p for p in swap_pairs(ndp, 2) if p[0] >= least])
        got.append((far, 2, None, low, 0))
        got.append((lax.ppermute(far, "dp", swap_pairs(ndp, 1)), 3, None, low, 0))
    return got


def compute(nsp, ndp, exchange, gate, value, gain, bias, mix_weight, mix_bias):
    rows, width = value.shape
    groups = mix_weight.shape[0]
    length = rows * nsp
    chunks = 2 if groups % 2 == 0 else 1
    per = groups // chunks
    nblocks = -(-length // BLK)
    piece = jax.ShapeDtypeStruct((rows, per * GD), jnp.bfloat16)
    small = pltpu.CompilerParams(vmem_limit_bytes=16 << 20)

    columns = [(0, 2 * TILE, 0), (2 * TILE, TILE, 2), (3 * TILE, TILE, 3)] if exchange else []
    cuts = [(c * per, per, low, cols) for c in range(chunks) for low, cols, _ in columns]
    made = pl.pallas_call(
        functools.partial(norm_kernel, nsp, chunks, per * GD, 16, cuts),
        out_shape=[piece] * (nsp * chunks)
        + [jax.ShapeDtypeStruct((n, mix_weight.shape[1], cols), jnp.bfloat16) for _, n, _, cols in cuts],
        in_specs=[HBM] * 4,
        out_specs=[VMEM] * (nsp * chunks + len(cuts)),
        scratch_shapes=[
            pltpu.VMEM((rows, width), jnp.bfloat16),
            pltpu.VMEM((width,), jnp.bfloat16),
            pltpu.VMEM((width,), jnp.bfloat16),
            pltpu.VMEM((rows, width), jnp.bfloat16),
            pltpu.SemaphoreType.DMA((5 + len(cuts),)),
        ],
        compiler_params=small,
        cost_estimate=pl.CostEstimate(flops=30 * rows * width, bytes_accessed=4 * rows * width, transcendentals=rows * width),
        name="norm",
    )(*[pltpu.with_memory_space_constraint(x, pltpu.HBM) for x in (value, gain, bias, mix_weight)])
    sent, parts = made[:nsp * chunks], made[nsp * chunks:]
    weights = []
    if exchange:
        other = lax.ppermute(mix_weight, "dp", swap_pairs(ndp, 1))
        for c in range(chunks):
            mine = parts[c * len(columns):(c + 1) * len(columns)]
            mine = [(low, least, part) for (low, _, least), part in zip(columns, mine)]
            weights.append(exchange_rows((mix_weight, other), mine, ndp, c * per))
    else:
        whole = lax.all_gather(mix_weight, "dp", axis=1, tiled=True)
        weights = [[(whole, 0, i, 0, c * per) for i in range(BLK // TILE)] for c in range(chunks)]
    out = None
    got = []
    for c in range(chunks):
        mine = sent[c * nsp:(c + 1) * nsp]
        far = {s: lax.ppermute(mine[s], "sp", swap_pairs(nsp, s)) for s in steps_of(nsp)}
        got.append([mine[0]] + [far[s] for s in range(1, nsp)])
    backs = []
    for c in range(chunks):
        layout = [w[1:] for w in weights[c]]
        outs = pl.pallas_call(
            functools.partial(mix_kernel, nsp, length, c * per, layout),
            out_shape=[piece] * nsp,
            in_specs=[VMEM] * (nsp + len(layout) + 1),
            out_specs=[VMEM] * nsp,
            scratch_shapes=[
                pltpu.VMEM((per, BLK, nblocks * GD), jnp.bfloat16),
                pltpu.VMEM((nblocks * BLK, per * GD), jnp.bfloat16),
            ],
            compiler_params=pltpu.CompilerParams(vmem_limit_bytes=24 << 20),
            cost_estimate=pl.CostEstimate(flops=2 * per * BLK * length * GD, bytes_accessed=per * BLK * BLK, transcendentals=0),
        )(*got[c], *[w[0] for w in weights[c]], mix_bias)
        far = {s: lax.ppermute(outs[s], "sp", swap_pairs(nsp, s)) for s in steps_of(nsp)}
        backs += [[outs[0]] + [far[s] for s in range(1, nsp)]]
    out = None
    for c in range(chunks):
        extra = [] if out is None else [out]
        out = pl.pallas_call(
            functools.partial(gate_kernel, nsp, chunks, c, 32),
            out_shape=jax.ShapeDtypeStruct((rows, width), jnp.bfloat16),
            in_specs=[VMEM] * (1 + nsp) + [HBM] * len(extra),
            out_specs=HBM,
            scratch_shapes=[pltpu.VMEM((nsp, rows, per * GD), jnp.bfloat16), pltpu.SemaphoreType.DMA((nsp,))],
            input_output_aliases={nsp + 1: 0} if extra else {},
            compiler_params=small,
            cost_estimate=pl.CostEstimate(flops=12 * rows * width // chunks, bytes_accessed=6 * rows * width // chunks, transcendentals=rows * width // chunks),
        )(gate, *backs[c], *extra)
    return out


def body(nsp, ndp, exchange, gate_input, value_input, norm_gain, norm_bias, mix_weight, mix_bias):
    outs = [
        compute(nsp, ndp, exchange, gate_input[q], value_input[q], norm_gain, norm_bias, mix_weight, mix_bias)
        for q in range(value_input.shape[0])
    ]
    return jnp.stack(outs)


def solution(mesh):
    nsp, ndp = mesh.shape["sp"], mesh.shape["dp"]
    exchange = ndp == BLK // TILE == 4
    placed = (
        P(("grp", "dp"), "sp", None),
        P(("grp", "dp"), "sp", None),
        P(),
        P(),
        P("sp", "dp", None),
        P("sp", None),
    )
    return jax.shard_map(
        functools.partial(body, nsp, ndp, exchange),
        mesh=mesh,
        in_specs=placed,
        out_specs=P(("grp", "dp"), "sp", None),
        check_vma=False,
    )
```

time: 123 us -> 111 us (0.902)
  waiting for transfers between devices: 45.6 us -> 67.9 us
  Pallas kernels: 24.8 us -> 9.64 us
  starting transfers between devices: 40.8 us -> 31.6 us
  local copies, waits for them, and re-layouts: 8.64 us -> 0.01 us
    ppermute x26 -> x25, waiting for transfers between devices: 45.6 us -> 67.9 us  [the longest x6 25 us: compute(): lax.ppermute(mine[s], 'sp', swap_pairs(nsp, s))]
    ppermute x26 -> x25, starting transfers between devices: 40.8 us -> 31.6 us  [the longest x6 11.5 us: compute(): lax.ppermute(outs[s], 'sp', swap_pairs(nsp, s))]
    pallas_call x3, Pallas kernels: 14.3 us -> 6.28 us  [the longest x1 3.4 us: compute(): pl.pallas_call(functools.partial(norm_kernel, nsp, chunks, per * GD, 16,...]
    pallas_call x2, Pallas kernels: 10.6 us -> 3.37 us  [compute(): pl.pallas_call(functools.partial(mix_kernel, nsp, length, c * per, layout...]
    unnamed x50 -> x6, local copies, waits for them, and re-layouts: 3.42 us -> 0.01 us
    reshape x2 -> x0, local copies, waits for them, and re-layouts: 2.72 us -> none  [the longest x1 1.43 us: body(): gain = norm_gain.reshape(1, width)]
    slice x3 -> x0, local copies, waits for them, and re-layouts: 1.54 us -> none  [the longest x2 1.37 us: compute(): lax.slice_in_dim(own, low, low + count, axis=2)]
  transfers between devices with their start and end apart: 26 -> 25, of which waited for: 8 -> 9; matrix products, arithmetic and copies ran while one was open for 2% -> 0% of each run, Pallas kernels for 13% -> 8%
where the time goes in v2:
time: 111 us; the launch traced here: 109 us
  waiting for transfers between devices  67.9 us (61%)
  starting transfers between devices  31.6 us (28%)
  Pallas kernels  9.64 us (9%)
    ppermute x6, waiting for transfers between devices, compute(): lax.ppermute(mine[s], 'sp', swap_pairs(nsp, s))  25 us
    ppermute x6, waiting for transfers between devices, exchange_rows(): lax.ppermute(part, 'dp', [p for p in swap_pairs(ndp, 2) if p[0] >= least])  21.1 us
    ppermute x6, waiting for transfers between devices, compute(): lax.ppermute(outs[s], 'sp', swap_pairs(nsp, s))  20.9 us
    ppermute x6, starting transfers between devices, compute(): lax.ppermute(outs[s], 'sp', swap_pairs(nsp, s))  11.5 us
    ppermute x6, starting transfers between devices, compute(): lax.ppermute(mine[s], 'sp', swap_pairs(nsp, s))  8.4 us
    ppermute x6, starting transfers between devices, exchange_rows(): lax.ppermute(part, 'dp', [p for p in swap_pairs(ndp, 2) if p[0] >= least])  8.13 us
    pallas_call x1, Pallas kernels, compute(): pl.pallas_call(functools.partial(norm_kernel, nsp, chunks, per * GD, 16,...  3.4 us
    pallas_call x2, Pallas kernels, compute(): pl.pallas_call(functools.partial(mix_kernel, nsp, length, c * per, layout...  3.37 us
  transfers between devices with their start and end apart: 25, of which 9 were waited for; matrix products, arithmetic and copies ran while one was open for 0% of the time, Pallas kernels for 8%

profile of v2, /device:TPU:0, one launch (start us, length us, event | category | flops | bytes accessed | tf_op | source)
XLA Modules:
  0.0 109.3 jit_solution(9291061027739854200)
XLA Ops:
  0.0 0.5 collective-permute-start.3
  0.5 0.0 copy-start
  0.5 0.0 copy-start.2
  0.5 3.4 %norm.1 = (bf16[384,256]{1,0:T(8,128)(2,1)S(1)}, bf16[384,256]{1,0:T(8,128)(2,1)S(1)}, bf16[384,256]{1,0:T(8,128)(2,1)S(1)}, bf16[384,256]{1,0:T(8,128)(2,1)S(1)...) custom-call(bf16[384,2048]{1,0:T(8,128)(2,1)} %bitcast.5, ...), custom_call_target="tpu_custom_call" | custom-call | flops 23592960 | bytes 3145728 | tf_op jit(solution)/shard_map/norm/pallas_call | solution.py:172
  3.9 2.6 %collective-permute-start.13 = (bf16[384,256]{1,0:T(8,128)(2,1)S(1)}, bf16[384,256]{1,0:T(8,128)(2,1)S(1)}, u32[]{:S(2)}, u32[]{:S(2)}) collective-permute-start(bf16[384,256]{1,0:T(8,128)(2,1)S(1)} %get-tuple-element.39), channel_id=1, source_target_pairs={{0,4},{4,0},{8,12},{12,8},{1,5},{5,1},{9,13},{13,9},{2,6},{6,2},{1... | collective-permute-start | bytes 589832 | tf_op jit(solution)/shard_map/ppermute | solution.py:204
  6.5 1.5 %collective-permute-start.16 = (bf16[2,256,512]{2,1,0:T(8,128)(2,1)S(1)}, bf16[2,256,512]{2,1,0:T(8,128)(2,1)S(1)}, u32[]{:S(2)}, u32[]{:S(2)}) collective-permute-start(bf16[2,256,512]{2,1,0:T(8,128)(2,1)S(1)} %get-tuple-element.42), channel_id=1, source_target_pairs={{0,2},{1,3},{2,0},{3,1},{4,6},{5,7},{6,4},{7,5},{8,10},{9,11},{10,... | collective-permute-start | bytes 1572872 | tf_op jit(solution)/shard_map/ppermute | solution.py:154
  8.0 2.6 %collective-permute-start.14 = (bf16[384,256]{1,0:T(8,128)(2,1)S(1)}, bf16[384,256]{1,0:T(8,128)(2,1)S(1)}, u32[]{:S(2)}, u32[]{:S(2)}) collective-permute-start(bf16[384,256]{1,0:T(8,128)(2,1)S(1)} %get-tuple-element.40), channel_id=1, source_target_pairs={{0,8},{4,12},{8,0},{12,4},{1,9},{5,13},{9,1},{13,5},{2,10},{6,14},... | collective-permute-start | bytes 589832 | tf_op jit(solution)/shard_map/ppermute | solution.py:204
  10.6 0.2 collective-permute-start.15
  10.8 4.2 %collective-permute-done.13.refs_1_ = bf16[384,256]{1,0:T(8,128)(2,1)S(1)} collective-permute-done((bf16[384,256]{1,0:T(8,128)(2,1)S(1)}, bf16[384,256]{1,0:T(8,128)(2,1)S(1)}, u32[]{:S(2)}, u32[]{:S(2)}) %collective-permute-start.13) | collective-permute-done | bytes 196640 | tf_op jit(solution)/shard_map/ppermute | solution.py:204
  15.0 0.0 collective-permute-start
  15.0 10.2 %collective-permute-done.14.refs_2_ = bf16[384,256]{1,0:T(8,128)(2,1)S(1)} collective-permute-done((bf16[384,256]{1,0:T(8,128)(2,1)S(1)}, bf16[384,256]{1,0:T(8,128)(2,1)S(1)}, u32[]{:S(2)}, u32[]{:S(2)}) %collective-permute-start.14) | collective-permute-done | bytes 196640 | tf_op jit(solution)/shard_map/ppermute | solution.py:204
  25.2 1.3 %collective-permute-start.18 = (bf16[2,256,256]{2,1,0:T(8,128)(2,1)S(1)}, bf16[2,256,256]{2,1,0:T(8,128)(2,1)S(1)}, u32[]{:S(2)}, u32[]{:S(2)}) collective-permute-start(bf16[2,256,256]{2,1,0:T(8,128)(2,1)S(1)} %get-tuple-element.43), channel_id=1, source_target_pairs={{2,0},{3,1},{6,4},{7,5},{10,8},{11,9},{14,12},{15,13},{18,16},{19,... | collective-permute-start | bytes 786440 | tf_op jit(solution)/shard_map/ppermute | solution.py:154
  26.5 0.0 collective-permute-done.15.refs_3_
  26.5 0.7 collective-permute-start.20
  27.2 0.0 collective-permute-done.refs_1_
  27.2 2.7 %collective-permute-start.4 = (bf16[2,256,512]{2,1,0:T(8,128)(2,1)S(1)}, bf16[2,256,512]{2,1,0:T(8,128)(2,1)S(1)}, u32[]{:S(2)}, u32[]{:S(2)}) collective-permute-start(bf16[2,256,512]{2,1,0:T(8,128)(2,1)S(1)} %get-tuple-element.31), channel_id=1, source_target_pairs={{0,2},{1,3},{2,0},{3,1},{4,6},{5,7},{6,4},{7,5},{8,10},{9,11},{10,... | collective-permute-start | bytes 1572872 | tf_op jit(solution)/shard_map/ppermute | solution.py:154
  29.9 6.3 %collective-permute-done.18.refs_8_ = bf16[2,256,256]{2,1,0:T(8,128)(2,1)S(1)} collective-permute-done((bf16[2,256,256]{2,1,0:T(8,128)(2,1)S(1)}, bf16[2,256,256]{2,1,0:T(8,128)(2,1)S(1)}, u32[]{:S(2)}, u32[]{:S(2)}) %collective-permute-start.18) | collective-permute-done | bytes 262176 | tf_op jit(solution)/shard_map/ppermute | solution.py:154
  36.2 1.3 %collective-permute-start.6 = (bf16[2,256,256]{2,1,0:T(8,128)(2,1)S(1)}, bf16[2,256,256]{2,1,0:T(8,128)(2,1)S(1)}, u32[]{:S(2)}, u32[]{:S(2)}) collective-permute-start(bf16[2,256,256]{2,1,0:T(8,128)(2,1)S(1)} %get-tuple-element.32), channel_id=1, source_target_pairs={{2,0},{3,1},{6,4},{7,5},{10,8},{11,9},{14,12},{15,13},{18,16},{19,... | collective-permute-start | bytes 786440 | tf_op jit(solution)/shard_map/ppermute | solution.py:154
  37.5 0.0 collective-permute-done.20.refs_10_
  37.5 0.7 collective-permute-start.8
  38.2 0.0 collective-permute-done.16.refs_6_
  38.2 0.1 collective-permute-start.17
  38.3 14.8 %collective-permute-done.6.refs_8_ = bf16[2,256,256]{2,1,0:T(8,128)(2,1)S(1)} collective-permute-done((bf16[2,256,256]{2,1,0:T(8,128)(2,1)S(1)}, bf16[2,256,256]{2,1,0:T(8,128)(2,1)S(1)}, u32[]{:S(2)}, u32[]{:S(2)}) %collective-permute-start.6) | collective-permute-done | bytes 262176 | tf_op jit(solution)/shard_map/ppermute | solution.py:154
  53.1 0.0 collective-permute-start.19
  53.1 0.0 collective-permute-done.8.refs_10_
  53.1 2.5 %collective-permute-start.21 = (bf16[2,256,256]{2,1,0:T(8,128)(2,1)S(1)}, bf16[2,256,256]{2,1,0:T(8,128)(2,1)S(1)}, u32[]{:S(2)}, u32[]{:S(2)}) collective-permute-start(bf16[2,256,256]{2,1,0:T(8,128)(2,1)S(1)} %collective-permute-done.20.refs_10_), channel_id=1, source_target_pairs={{0,1},{1,0},{2,3},{3,2},{4,5},{5,4},{6,7},{7,6},{8,9},{9,8},{10,11... | collective-permute-start | bytes 786440 | tf_op jit(solution)/shard_map/ppermute | solution.py:156
  55.6 0.0 collective-permute-done.4.refs_6_
  55.6 0.0 collective-permute-start.5
  55.6 0.0 collective-permute-done.19.refs_9_
  55.6 0.4 collective-permute-start.1
  56.0 0.8 collective-permute-done.21.refs_11_
  56.8 0.4 collective-permute-start.7
  57.1 0.0 collective-permute-done.17.refs_7_
  57.1 0.1 collective-permute-start.9
  57.3 0.0 collective-permute-done.3.refs_5_
  57.3 2.6 %collective-permute-start.2 = (bf16[384,256]{1,0:T(8,128)(2,1)S(1)}, bf16[384,256]{1,0:T(8,128)(2,1)S(1)}, u32[]{:S(2)}, u32[]{:S(2)}) collective-permute-start(bf16[384,256]{1,0:T(8,128)(2,1)S(1)} %get-tuple-element.30), channel_id=1, source_target_pairs={{0,12},{4,8},{8,4},{12,0},{1,13},{5,9},{9,5},{13,1},{2,14},{6,10},... | collective-permute-start | bytes 589832 | tf_op jit(solution)/shard_map/ppermute | solution.py:204
  59.9 0.0 copy-done
  59.9 0.0 copy-done.2
  59.9 1.7 %shard_map.65 = (bf16[384,256]{1,0:T(8,128)(2,1)S(1)}, bf16[384,256]{1,0:T(8,128)(2,1)S(1)}, bf16[384,256]{1,0:T(8,128)(2,1)S(1)}, bf16[384,256]{1,0:T(8,128)(2,1)S(1)}) custom-call(bf16[384,256]{1,0:T(8,128)(2,1)S(1)} %get-tuple-element.38.refs_0_, bf16[384,256]{1,0:T(8,128)(2,1)S(1)} %collective-permute-done.13.refs_1_, ...), custom_call_target="tpu_custom_call" | custom-call | flops 805306368 | bytes 2097152 | tf_op jit(solution)/shard_map/pallas_call | solution.py:209
  61.6 10.7 %collective-permute-done.1.refs_2_ = bf16[384,256]{1,0:T(8,128)(2,1)S(1)} collective-permute-done((bf16[384,256]{1,0:T(8,128)(2,1)S(1)}, bf16[384,256]{1,0:T(8,128)(2,1)S(1)}, u32[]{:S(2)}, u32[]{:S(2)}) %collective-permute-start.1) | collective-permute-done | bytes 196640 | tf_op jit(solution)/shard_map/ppermute | solution.py:204
  72.2 0.0 collective-permute-start.22
  72.3 0.0 collective-permute-done.2.refs_3_
  72.3 4.5 %collective-permute-start.23 = (bf16[384,256]{1,0:T(8,128)(2,1)S(1)}, bf16[384,256]{1,0:T(8,128)(2,1)S(1)}, u32[]{:S(2)}, u32[]{:S(2)}) collective-permute-start(bf16[384,256]{1,0:T(8,128)(2,1)S(1)} %get-tuple-element.47), channel_id=1, source_target_pairs={{0,8},{4,12},{8,0},{12,4},{1,9},{5,13},{9,1},{13,5},{2,10},{6,14},... | collective-permute-start | bytes 589832 | tf_op jit(solution)/shard_map/ppermute | solution.py:221
  76.8 0.0 collective-permute-done.7.refs_9_
  76.8 2.6 %collective-permute-start.24 = (bf16[384,256]{1,0:T(8,128)(2,1)S(1)}, bf16[384,256]{1,0:T(8,128)(2,1)S(1)}, u32[]{:S(2)}, u32[]{:S(2)}) collective-permute-start(bf16[384,256]{1,0:T(8,128)(2,1)S(1)} %get-tuple-element.48), channel_id=1, source_target_pairs={{0,12},{4,8},{8,4},{12,0},{1,13},{5,9},{9,5},{13,1},{2,14},{6,10},... | collective-permute-start | bytes 589832 | tf_op jit(solution)/shard_map/ppermute | solution.py:221
  79.3 0.0 collective-permute-done.9.refs_11_
  79.3 0.0 collective-permute-done.5.refs_7_
  79.4 0.0 copy-start.1
  79.4 1.7 %shard_map.64 = (bf16[384,256]{1,0:T(8,128)(2,1)S(1)}, bf16[384,256]{1,0:T(8,128)(2,1)S(1)}, bf16[384,256]{1,0:T(8,128)(2,1)S(1)}, bf16[384,256]{1,0:T(8,128)(2,1)S(1)}) custom-call(bf16[384,256]{1,0:T(8,128)(2,1)S(1)} %get-tuple-element.27.refs_0_, bf16[384,256]{1,0:T(8,128)(2,1)S(1)} %collective-permute-done.refs_1_, ...), custom_call_target="tpu_custom_call" | custom-call | flops 805306368 | bytes 2097152 | tf_op jit(solution)/shard_map/pallas_call | solution.py:209
  81.0 0.1 collective-permute-start.10
  81.1 1.8 %collective-permute-start.11 = (bf16[384,256]{1,0:T(8,128)(2,1)S(1)}, bf16[384,256]{1,0:T(8,128)(2,1)S(1)}, u32[]{:S(2)}, u32[]{:S(2)}) collective-permute-start(bf16[384,256]{1,0:T(8,128)(2,1)S(1)} %get-tuple-element.36), channel_id=1, source_target_pairs={{0,8},{4,12},{8,0},{12,4},{1,9},{5,13},{9,1},{13,5},{2,10},{6,14},... | collective-permute-start | bytes 589832 | tf_op jit(solution)/shard_map/ppermute | solution.py:221
  82.9 0.0 collective-permute-done.22.refs_1_
  82.9 2.6 %collective-permute-start.12 = (bf16[384,256]{1,0:T(8,128)(2,1)S(1)}, bf16[384,256]{1,0:T(8,128)(2,1)S(1)}, u32[]{:S(2)}, u32[]{:S(2)}) collective-permute-start(bf16[384,256]{1,0:T(8,128)(2,1)S(1)} %get-tuple-element.37), channel_id=1, source_target_pairs={{0,12},{4,8},{8,4},{12,0},{1,13},{5,9},{9,5},{13,1},{2,14},{6,10},... | collective-permute-start | bytes 589832 | tf_op jit(solution)/shard_map/ppermute | solution.py:221
  85.5 5.5 %collective-permute-done.23.refs_2_ = bf16[384,256]{1,0:T(8,128)(2,1)S(1)} collective-permute-done((bf16[384,256]{1,0:T(8,128)(2,1)S(1)}, bf16[384,256]{1,0:T(8,128)(2,1)S(1)}, u32[]{:S(2)}, u32[]{:S(2)}) %collective-permute-start.23) | collective-permute-done | bytes 196640 | tf_op jit(solution)/shard_map/ppermute | solution.py:221
  91.0 0.0 collective-permute-done.24.refs_3_
  91.0 0.0 copy-done.1
  91.0 1.4 %shard_map.66.refs_4_ = bf16[384,2048]{1,0:T(8,128)(2,1)} custom-call(bf16[384,2048]{1,0:T(8,128)(2,1)S(1)} %bitcast.3, bf16[384,256]{1,0:T(8,128)(2,1)S(1)} %get-tuple-element.45.refs_0_, bf16[384,256]{1,0:T(8,128)(2,1)S(1)} %collective-permute-done.22.refs_1_, bf16[384,256]{1,0:T(8,128)(2,1)S(1)} %collective-permute-done.23.refs_2_, ...), custom_call_target="tpu_custom_call" | custom-call | flops 4718592 | bytes 2359296 | tf_op jit(solution)/shard_map/pallas_call | solution.py:226
  92.5 1.0 collective-permute-done.10.refs_1_
  93.5 14.4 %collective-permute-done.11.refs_2_ = bf16[384,256]{1,0:T(8,128)(2,1)S(1)} collective-permute-done((bf16[384,256]{1,0:T(8,128)(2,1)S(1)}, bf16[384,256]{1,0:T(8,128)(2,1)S(1)}, u32[]{:S(2)}, u32[]{:S(2)}) %collective-permute-start.11) | collective-permute-done | bytes 196640 | tf_op jit(solution)/shard_map/ppermute | solution.py:221
  107.9 0.0 collective-permute-done.12.refs_3_
  107.9 1.4 %shard_map.67 = bf16[384,2048]{1,0:T(8,128)(2,1)} custom-call(bf16[384,2048]{1,0:T(8,128)(2,1)S(1)} %bitcast.4, bf16[384,256]{1,0:T(8,128)(2,1)S(1)} %get-tuple-element.34.refs_0_, bf16[384,256]{1,0:T(8,128)(2,1)S(1)} %collective-permute-done.10.refs_1_, bf16[384,256]{1,0:T(8,128)(2,1)S(1)} %collective-permute-done.11.refs_2_, ...), custom_call_target="tpu_custom_call", output_to_operand_aliasing={{}: (5, {})} | custom-call | flops 4718592 | bytes 2359296 | tf_op jit(solution)/shard_map/pallas_call | solution.py:226
Async XLA Ops:
  0.0 57.3 %collective-permute-start.3 = (bf16[4,256,1024]{2,1,0:T(8,128)(2,1)}, bf16[4,256,1024]{2,1,0:T(8,128)(2,1)S(1)}, u32[]{:S(2)}, u32[]{:S(2)}) collective-permute-start(bf16[4,256,1024]{2,1,0:T(8,128)(2,1)} %refs_4_.3), channel_id=1, source_target_pairs={{0,1},{1,0},{2,3},{3,2},{4,5},{5,4},{6,7},{7,6},{8,9},{9,8},{10,11... | collective-permute-start | bytes 6291464 | tf_op jit(solution)/shard_map/ppermute | solution.py:192
  0.5 59.4 %copy-start = (bf16[4,256,1024]{2,1,0:T(8,128)(2,1)S(1)}, bf16[4,256,1024]{2,1,0:T(8,128)(2,1)}, u32[]{:S(2)}) copy-start(bf16[4,256,1024]{2,1,0:T(8,128)(2,1)} %refs_4_.3) | copy-start | bytes 6291460
  0.5 59.4 %copy-start.2 = (bf16[4,1024]{1,0:T(4,128)(2,1)S(1)}, bf16[4,1024]{1,0:T(4,128)(2,1)}, u32[]{:S(2)}) copy-start(bf16[4,1024]{1,0:T(4,128)(2,1)} %refs_12_.3) | copy-start | bytes 24580
  3.9 11.1 %collective-permute-start.13 = (bf16[384,256]{1,0:T(8,128)(2,1)S(1)}, bf16[384,256]{1,0:T(8,128)(2,1)S(1)}, u32[]{:S(2)}, u32[]{:S(2)}) collective-permute-start(bf16[384,256]{1,0:T(8,128)(2,1)S(1)} %get-tuple-element.39), channel_id=1, source_target_pairs={{0,4},{4,0},{8,12},{12,8},{1,5},{5,1},{9,13},{13,9},{2,6},{6,2},{1... | collective-permute-start | bytes 589832 | tf_op jit(solution)/shard_map/ppermute | solution.py:204
  6.5 31.7 %collective-permute-start.16 = (bf16[2,256,512]{2,1,0:T(8,128)(2,1)S(1)}, bf16[2,256,512]{2,1,0:T(8,128)(2,1)S(1)}, u32[]{:S(2)}, u32[]{:S(2)}) collective-permute-start(bf16[2,256,512]{2,1,0:T(8,128)(2,1)S(1)} %get-tuple-element.42), channel_id=1, source_target_pairs={{0,2},{1,3},{2,0},{3,1},{4,6},{5,7},{6,4},{7,5},{8,10},{9,11},{10,... | collective-permute-start | bytes 1572872 | tf_op jit(solution)/shard_map/ppermute | solution.py:154
  8.0 17.2 %collective-permute-start.14 = (bf16[384,256]{1,0:T(8,128)(2,1)S(1)}, bf16[384,256]{1,0:T(8,128)(2,1)S(1)}, u32[]{:S(2)}, u32[]{:S(2)}) collective-permute-start(bf16[384,256]{1,0:T(8,128)(2,1)S(1)} %get-tuple-element.40), channel_id=1, source_target_pairs={{0,8},{4,12},{8,0},{12,4},{1,9},{5,13},{9,1},{13,5},{2,10},{6,14},... | collective-permute-start | bytes 589832 | tf_op jit(solution)/shard_map/ppermute | solution.py:204
  10.6 15.8 %collective-permute-start.15 = (bf16[384,256]{1,0:T(8,128)(2,1)S(1)}, bf16[384,256]{1,0:T(8,128)(2,1)S(1)}, u32[]{:S(2)}, u32[]{:S(2)}) collective-permute-start(bf16[384,256]{1,0:T(8,128)(2,1)S(1)} %get-tuple-element.41), channel_id=1, source_target_pairs={{0,12},{4,8},{8,4},{12,0},{1,13},{5,9},{9,5},{13,1},{2,14},{6,10},... | collective-permute-start | bytes 589832 | tf_op jit(solution)/shard_map/ppermute | solution.py:204
  15.0 12.2 %collective-permute-start = (bf16[384,256]{1,0:T(8,128)(2,1)S(1)}, bf16[384,256]{1,0:T(8,128)(2,1)S(1)}, u32[]{:S(2)}, u32[]{:S(2)}) collective-permute-start(bf16[384,256]{1,0:T(8,128)(2,1)S(1)} %get-tuple-element.28), channel_id=1, source_target_pairs={{0,4},{4,0},{8,12},{12,8},{1,5},{5,1},{9,13},{13,9},{2,6},{6,2},{1... | collective-permute-start | bytes 589832 | tf_op jit(solution)/shard_map/ppermute | solution.py:204
  25.2 11.1 %collective-permute-start.18 = (bf16[2,256,256]{2,1,0:T(8,128)(2,1)S(1)}, bf16[2,256,256]{2,1,0:T(8,128)(2,1)S(1)}, u32[]{:S(2)}, u32[]{:S(2)}) collective-permute-start(bf16[2,256,256]{2,1,0:T(8,128)(2,1)S(1)} %get-tuple-element.43), channel_id=1, source_target_pairs={{2,0},{3,1},{6,4},{7,5},{10,8},{11,9},{14,12},{15,13},{18,16},{19,... | collective-permute-start | bytes 786440 | tf_op jit(solution)/shard_map/ppermute | solution.py:154
  26.5 11.1 %collective-permute-start.20 = (bf16[2,256,256]{2,1,0:T(8,128)(2,1)S(1)}, bf16[2,256,256]{2,1,0:T(8,128)(2,1)S(1)}, u32[]{:S(2)}, u32[]{:S(2)}) collective-permute-start(bf16[2,256,256]{2,1,0:T(8,128)(2,1)S(1)} %get-tuple-element.44), channel_id=1, source_target_pairs={{3,1},{7,5},{11,9},{15,13},{19,17},{23,21},{27,25},{31,29}} | collective-permute-start | bytes 786440 | tf_op jit(solution)/shard_map/ppermute | solution.py:154
  27.2 28.4 %collective-permute-start.4 = (bf16[2,256,512]{2,1,0:T(8,128)(2,1)S(1)}, bf16[2,256,512]{2,1,0:T(8,128)(2,1)S(1)}, u32[]{:S(2)}, u32[]{:S(2)}) collective-permute-start(bf16[2,256,512]{2,1,0:T(8,128)(2,1)S(1)} %get-tuple-element.31), channel_id=1, source_target_pairs={{0,2},{1,3},{2,0},{3,1},{4,6},{5,7},{6,4},{7,5},{8,10},{9,11},{10,... | collective-permute-start | bytes 1572872 | tf_op jit(solution)/shard_map/ppermute | solution.py:154
  36.2 16.9 %collective-permute-start.6 = (bf16[2,256,256]{2,1,0:T(8,128)(2,1)S(1)}, bf16[2,256,256]{2,1,0:T(8,128)(2,1)S(1)}, u32[]{:S(2)}, u32[]{:S(2)}) collective-permute-start(bf16[2,256,256]{2,1,0:T(8,128)(2,1)S(1)} %get-tuple-element.32), channel_id=1, source_target_pairs={{2,0},{3,1},{6,4},{7,5},{10,8},{11,9},{14,12},{15,13},{18,16},{19,... | collective-permute-start | bytes 786440 | tf_op jit(solution)/shard_map/ppermute | solution.py:154
  37.5 15.6 %collective-permute-start.8 = (bf16[2,256,256]{2,1,0:T(8,128)(2,1)S(1)}, bf16[2,256,256]{2,1,0:T(8,128)(2,1)S(1)}, u32[]{:S(2)}, u32[]{:S(2)}) collective-permute-start(bf16[2,256,256]{2,1,0:T(8,128)(2,1)S(1)} %get-tuple-element.33), channel_id=1, source_target_pairs={{3,1},{7,5},{11,9},{15,13},{19,17},{23,21},{27,25},{31,29}} | collective-permute-start | bytes 786440 | tf_op jit(solution)/shard_map/ppermute | solution.py:154
  38.2 18.9 %collective-permute-start.17 = (bf16[2,256,512]{2,1,0:T(8,128)(2,1)S(1)}, bf16[2,256,512]{2,1,0:T(8,128)(2,1)S(1)}, u32[]{:S(2)}, u32[]{:S(2)}) collective-permute-start(bf16[2,256,512]{2,1,0:T(8,128)(2,1)S(1)} %collective-permute-done.16.refs_6_), channel_id=1, source_target_pairs={{0,1},{1,0},{2,3},{3,2},{4,5},{5,4},{6,7},{7,6},{8,9},{9,8},{10,11... | collective-permute-start | bytes 1572872 | tf_op jit(solution)/shard_map/ppermute | solution.py:156
  53.1 2.5 %collective-permute-start.19 = (bf16[2,256,256]{2,1,0:T(8,128)(2,1)S(1)}, bf16[2,256,256]{2,1,0:T(8,128)(2,1)S(1)}, u32[]{:S(2)}, u32[]{:S(2)}) collective-permute-start(bf16[2,256,256]{2,1,0:T(8,128)(2,1)S(1)} %collective-permute-done.18.refs_8_), channel_id=1, source_target_pairs={{0,1},{1,0},{2,3},{3,2},{4,5},{5,4},{6,7},{7,6},{8,9},{9,8},{10,11... | collective-permute-start | bytes 786440 | tf_op jit(solution)/shard_map/ppermute | solution.py:156
  53.1 3.7 %collective-permute-start.21 = (bf16[2,256,256]{2,1,0:T(8,128)(2,1)S(1)}, bf16[2,256,256]{2,1,0:T(8,128)(2,1)S(1)}, u32[]{:S(2)}, u32[]{:S(2)}) collective-permute-start(bf16[2,256,256]{2,1,0:T(8,128)(2,1)S(1)} %collective-permute-done.20.refs_10_), channel_id=1, source_target_pairs={{0,1},{1,0},{2,3},{3,2},{4,5},{5,4},{6,7},{7,6},{8,9},{9,8},{10,11... | collective-permute-start | bytes 786440 | tf_op jit(solution)/shard_map/ppermute | solution.py:156
  55.6 23.7 %collective-permute-start.5 = (bf16[2,256,512]{2,1,0:T(8,128)(2,1)S(1)}, bf16[2,256,512]{2,1,0:T(8,128)(2,1)S(1)}, u32[]{:S(2)}, u32[]{:S(2)}) collective-permute-start(bf16[2,256,512]{2,1,0:T(8,128)(2,1)S(1)} %collective-permute-done.4.refs_6_), channel_id=1, source_target_pairs={{0,1},{1,0},{2,3},{3,2},{4,5},{5,4},{6,7},{7,6},{8,9},{9,8},{10,11... | collective-permute-start | bytes 1572872 | tf_op jit(solution)/shard_map/ppermute | solution.py:156
  55.6 16.6 %collective-permute-start.1 = (bf16[384,256]{1,0:T(8,128)(2,1)S(1)}, bf16[384,256]{1,0:T(8,128)(2,1)S(1)}, u32[]{:S(2)}, u32[]{:S(2)}) collective-permute-start(bf16[384,256]{1,0:T(8,128)(2,1)S(1)} %get-tuple-element.29), channel_id=1, source_target_pairs={{0,8},{4,12},{8,0},{12,4},{1,9},{5,13},{9,1},{13,5},{2,10},{6,14},... | collective-permute-start | bytes 589832 | tf_op jit(solution)/shard_map/ppermute | solution.py:204
  56.8 20.0 %collective-permute-start.7 = (bf16[2,256,256]{2,1,0:T(8,128)(2,1)S(1)}, bf16[2,256,256]{2,1,0:T(8,128)(2,1)S(1)}, u32[]{:S(2)}, u32[]{:S(2)}) collective-permute-start(bf16[2,256,256]{2,1,0:T(8,128)(2,1)S(1)} %collective-permute-done.6.refs_8_), channel_id=1, source_target_pairs={{0,1},{1,0},{2,3},{3,2},{4,5},{5,4},{6,7},{7,6},{8,9},{9,8},{10,11... | collective-permute-start | bytes 786440 | tf_op jit(solution)/shard_map/ppermute | solution.py:156
  57.1 22.2 %collective-permute-start.9 = (bf16[2,256,256]{2,1,0:T(8,128)(2,1)S(1)}, bf16[2,256,256]{2,1,0:T(8,128)(2,1)S(1)}, u32[]{:S(2)}, u32[]{:S(2)}) collective-permute-start(bf16[2,256,256]{2,1,0:T(8,128)(2,1)S(1)} %collective-permute-done.8.refs_10_), channel_id=1, source_target_pairs={{0,1},{1,0},{2,3},{3,2},{4,5},{5,4},{6,7},{7,6},{8,9},{9,8},{10,11... | collective-permute-start | bytes 786440 | tf_op jit(solution)/shard_map/ppermute | solution.py:156
  57.3 15.0 %collective-permute-start.2 = (bf16[384,256]{1,0:T(8,128)(2,1)S(1)}, bf16[384,256]{1,0:T(8,128)(2,1)S(1)}, u32[]{:S(2)}, u32[]{:S(2)}) collective-permute-start(bf16[384,256]{1,0:T(8,128)(2,1)S(1)} %get-tuple-element.30), channel_id=1, source_target_pairs={{0,12},{4,8},{8,4},{12,0},{1,13},{5,9},{9,5},{13,1},{2,14},{6,10},... | collective-permute-start | bytes 589832 | tf_op jit(solution)/shard_map/ppermute | solution.py:204
  72.2 10.7 %collective-permute-start.22 = (bf16[384,256]{1,0:T(8,128)(2,1)S(1)}, bf16[384,256]{1,0:T(8,128)(2,1)S(1)}, u32[]{:S(2)}, u32[]{:S(2)}) collective-permute-start(bf16[384,256]{1,0:T(8,128)(2,1)S(1)} %get-tuple-element.46), channel_id=1, source_target_pairs={{0,4},{4,0},{8,12},{12,8},{1,5},{5,1},{9,13},{13,9},{2,6},{6,2},{1... | collective-permute-start | bytes 589832 | tf_op jit(solution)/shard_map/ppermute | solution.py:221
  72.3 18.8 %collective-permute-start.23 = (bf16[384,256]{1,0:T(8,128)(2,1)S(1)}, bf16[384,256]{1,0:T(8,128)(2,1)S(1)}, u32[]{:S(2)}, u32[]{:S(2)}) collective-permute-start(bf16[384,256]{1,0:T(8,128)(2,1)S(1)} %get-tuple-element.47), channel_id=1, source_target_pairs={{0,8},{4,12},{8,0},{12,4},{1,9},{5,13},{9,1},{13,5},{2,10},{6,14},... | collective-permute-start | bytes 589832 | tf_op jit(solution)/shard_map/ppermute | solution.py:221
  76.8 14.3 %collective-permute-start.24 = (bf16[384,256]{1,0:T(8,128)(2,1)S(1)}, bf16[384,256]{1,0:T(8,128)(2,1)S(1)}, u32[]{:S(2)}, u32[]{:S(2)}) collective-permute-start(bf16[384,256]{1,0:T(8,128)(2,1)S(1)} %get-tuple-element.48), channel_id=1, source_target_pairs={{0,12},{4,8},{8,4},{12,0},{1,13},{5,9},{9,5},{13,1},{2,14},{6,10},... | collective-permute-start | bytes 589832 | tf_op jit(solution)/shard_map/ppermute | solution.py:221
  79.4 11.7 %copy-start.1 = (bf16[1,384,2048]{2,1,0:T(8,128)(2,1)S(1)}, bf16[1,384,2048]{2,1,0:T(8,128)(2,1)}, u32[]{:S(2)}) copy-start(bf16[1,384,2048]{2,1,0:T(8,128)(2,1)} %param.6) | copy-start | bytes 4718596
  81.0 12.4 %collective-permute-start.10 = (bf16[384,256]{1,0:T(8,128)(2,1)S(1)}, bf16[384,256]{1,0:T(8,128)(2,1)S(1)}, u32[]{:S(2)}, u32[]{:S(2)}) collective-permute-start(bf16[384,256]{1,0:T(8,128)(2,1)S(1)} %get-tuple-element.35), channel_id=1, source_target_pairs={{0,4},{4,0},{8,12},{12,8},{1,5},{5,1},{9,13},{13,9},{2,6},{6,2},{1... | collective-permute-start | bytes 589832 | tf_op jit(solution)/shard_map/ppermute | solution.py:221
  81.1 26.8 %collective-permute-start.11 = (bf16[384,256]{1,0:T(8,128)(2,1)S(1)}, bf16[384,256]{1,0:T(8,128)(2,1)S(1)}, u32[]{:S(2)}, u32[]{:S(2)}) collective-permute-start(bf16[384,256]{1,0:T(8,128)(2,1)S(1)} %get-tuple-element.36), channel_id=1, source_target_pairs={{0,8},{4,12},{8,0},{12,4},{1,9},{5,13},{9,1},{13,5},{2,10},{6,14},... | collective-permute-start | bytes 589832 | tf_op jit(solution)/shard_map/ppermute | solution.py:221
  82.9 25.0 %collective-permute-start.12 = (bf16[384,256]{1,0:T(8,128)(2,1)S(1)}, bf16[384,256]{1,0:T(8,128)(2,1)S(1)}, u32[]{:S(2)}, u32[]{:S(2)}) collective-permute-start(bf16[384,256]{1,0:T(8,128)(2,1)S(1)} %get-tuple-element.37), channel_id=1, source_target_pairs={{0,12},{4,8},{8,4},{12,0},{1,13},{5,9},{9,5},{13,1},{2,14},{6,10},... | collective-permute-start | bytes 589832 | tf_op jit(solution)/shard_map/ppermute | solution.py:221

commit v3 on v2

v3 whole, which is shorter than its diff:
```python
import functools

import jax
import jax.numpy as jnp
from jax import lax
from jax.experimental import pallas as pl
from jax.experimental.pallas import tpu as pltpu
from jax.sharding import PartitionSpec as P


GD = 128
BLK = 1024
TILE = 256


VMEM = pl.BlockSpec(memory_space=pltpu.VMEM)
HBM = pl.BlockSpec(memory_space=pltpu.HBM)


def twice_gelu(x):
    return x + x * jnp.tanh(x * (0.7978845608028654 + 0.035677408136300125 * (x * x)))


def partner(here, step, shards):
    if shards & (shards - 1) == 0:
        return here ^ step, here ^ step
    return lax.rem(here + step, shards), lax.rem(here + shards - step, shards)


def swap_pairs(count, step):
    if count & (count - 1) == 0:
        return [(i, i ^ step) for i in range(count)]
    return [(i, (i + step) % count) for i in range(count)]


def steps_of(shards):
    return list(range(shards - 1, 0, -1))


def normalise(value, held, scale, offset, rows_step):
    def step(i, carry):
        at = pl.ds(pl.multiple_of(i * rows_step, rows_step), rows_step)
        act = twice_gelu(value[at, :].astype(jnp.float32))
        centred = act - jnp.mean(act, axis=-1, keepdims=True)
        var = jnp.mean(jnp.square(centred), axis=-1, keepdims=True)
        held[at, :] = (centred * lax.rsqrt(var + 4e-06) * scale + offset).astype(jnp.bfloat16)
        return carry

    steps = value.shape[0] // rows_step
    lax.fori_loop(0, steps, step, 0, unroll=8 if steps % 8 == 0 else 1)


def hand_out(shards, span, lanes, held, outs):
    here = lax.axis_index("sp")
    for out, (s, low, width) in zip(outs, lanes):
        start = pl.multiple_of(partner(here, s, shards)[0] * span + low, GD)
        out[...] = held[:, pl.ds(start, width)]


def weight_copies(cuts, weight_ref, parts, sems, first):
    copies = []
    for k, (part, (group, count, low, cols)) in enumerate(zip(parts, cuts)):
        source = weight_ref.at[pl.ds(group, count), :, pl.ds(low, cols)]
        copies.append(pltpu.make_async_copy(source, part, sems.at[first + k]))
    return copies


def head_kernel(shards, span, rows_step, lanes, cuts, value_ref, gain_ref, bias_ref, weight_ref, *refs):
    outs, parts = refs[:len(lanes)], refs[len(lanes):len(lanes) + len(cuts)]
    rest, gain, bias, value, held, sems = refs[len(lanes) + len(cuts):]
    head = value.shape[0]
    pairs = [
        (value_ref.at[pl.ds(0, head), :], value),
        (gain_ref, gain),
        (bias_ref, bias),
        (value_ref.at[pl.ds(head, rest.shape[0]), :], rest),
    ]
    copies = [pltpu.make_async_copy(source, target, sems.at[k]) for k, (source, target) in enumerate(pairs)]
    copies += weight_copies(cuts, weight_ref, parts, sems, len(pairs))
    for copy in copies:
        copy.start()
    for copy in copies[:3]:
        copy.wait()
    scale = gain[...].astype(jnp.float32).reshape(1, -1)
    offset = bias[...].astype(jnp.float32).reshape(1, -1)
    normalise(value, held, scale, offset, rows_step)
    hand_out(shards, span, lanes, held, outs)
    for copy in copies[3:]:
        copy.wait()


def rest_kernel(shards, span, rows_step, lanes, cuts, value, gain, bias, weight_ref, *refs):
    outs, parts = refs[:len(lanes)], refs[len(lanes):len(lanes) + len(cuts)]
    held, sems = refs[len(lanes) + len(cuts):]
    copies = weight_copies(cuts, weight_ref, parts, sems, 0)
    for copy in copies:
        copy.start()
    scale = gain[...].astype(jnp.float32).reshape(1, -1)
    offset = bias[...].astype(jnp.float32).reshape(1, -1)
    normalise(value, held, scale, offset, rows_step)
    hand_out(shards, span, lanes, held, outs)
    for copy in copies:
        copy.wait()


def mix_kernel(shards, length, first, start, layout, *refs):
    early, pieces, refs = refs[:shards], refs[shards:2 * shards], refs[2 * shards:]
    weights, refs = refs[:len(layout)], refs[len(layout):]
    bias_ref, outs, (values, mixed) = refs[0], refs[1:1 + shards], refs[1 + shards:]
    here, row = lax.axis_index("sp"), lax.axis_index("dp")
    head = early[0].shape[0]
    rest = pieces[0].shape[0]
    rows = head + rest
    groups = pieces[0].shape[1] // GD
    nblocks = -(-length // BLK)
    for s in range(shards):
        origin = partner(here, s, shards)[1]
        top = pl.multiple_of(origin * rows, GD)
        mixed[pl.ds(top, head), :] = early[s][:, pl.ds(start, groups * GD)]
        mixed[pl.ds(top + head, rest), :] = pieces[s][...]
    for g in range(groups):
        for b in range(nblocks):
            count = min(BLK, length - b * BLK)
            lanes = pl.ds(b * GD, GD)
            values[g, pl.ds(0, count), lanes] = mixed[pl.ds(b * BLK, count), pl.ds(g * GD, GD)]
            if count < BLK:
                values[g, pl.ds(count, BLK - count), lanes] = jnp.zeros((BLK - count, GD), jnp.bfloat16)
    tiles = {}
    for ref, (flip, fixed, low, skip) in zip(weights, layout):
        tiles.setdefault((flip, fixed), []).append((ref, low, skip))
    for (flip, fixed), parts in tiles.items():
        at_row = row ^ flip if fixed is None else fixed
        top = pl.multiple_of(at_row * TILE, TILE)
        for g in range(groups):
            total = None
            for ref, low, skip in parts:
                part = ref[skip + g] if fixed is None else ref[skip + g, pl.ds(fixed * TILE, TILE), :]
                cols = lax.broadcasted_iota(jnp.int32, part.shape, 1) + low
                keep = cols <= lax.broadcasted_iota(jnp.int32, part.shape, 0) + top
                part = jnp.where(keep, part, jnp.zeros_like(part))
                term = jnp.dot(part, values[g, pl.ds(low, part.shape[1]), :], preferred_element_type=jnp.float32)
                total = term if total is None else total + term
            shift = bias_ref[pl.ds(first + g, 1), pl.ds(top, TILE)].astype(jnp.float32)
            shift = jnp.broadcast_to(shift, (GD, TILE)).T
            for b in range(nblocks):
                block = total[:, b * GD:(b + 1) * GD] + shift
                mixed[pl.ds(b * BLK + top, TILE), pl.ds(g * GD, GD)] = block.astype(jnp.bfloat16)
    for s in range(shards):
        target = partner(here, s, shards)[0]
        outs[s][...] = mixed[pl.ds(pl.multiple_of(target * rows, rows), rows), :]


def gate_kernel(shards, chunks, chunk, steps, rows_step, gate_ref, *refs):
    pieces = refs[:len(steps)]
    out_ref, held, sems = refs[-3:]
    here = lax.axis_index("sp")
    width = pieces[0].shape[1]
    copies = []
    for k, s in enumerate(steps):
        start = (partner(here, s, shards)[1] * chunks + chunk) * width
        lanes = pl.ds(pl.multiple_of(start, GD), width)

        def step(i, carry, k=k, lanes=lanes):
            rows = pl.ds(pl.multiple_of(i * rows_step, rows_step), rows_step)
            gate = 0.5 * twice_gelu(gate_ref[rows, lanes].astype(jnp.float32))
            held[k, rows, :] = (gate * pieces[k][rows, :].astype(jnp.float32)).astype(jnp.bfloat16)
            return carry

        lax.fori_loop(0, gate_ref.shape[0] // rows_step, step, 0, unroll=4)
        copies.append(pltpu.make_async_copy(held.at[k], out_ref.at[:, lanes], sems.at[k]))
        copies[-1].start()
    for copy in copies:
        copy.wait()


def exchange_step(step, x, shards):
    return lax.ppermute(x, "sp", swap_pairs(shards, step))


def exchange_rows(weight, parts, ndp, first):
    got = [(weight[0], 0, None, 0, first), (weight[1], 1, None, 0, first)]
    for low, least, part in parts:
        far = lax.ppermute(part, "dp", [p for p in swap_pairs(ndp, 2) if p[0] >= least])
        got.append((far, 2, None, low, 0))
        got.append((lax.ppermute(far, "dp", swap_pairs(ndp, 1)), 3, None, low, 0))
    return got


def compute(nsp, ndp, exchange, gate, value, gain, bias, mix_weight, mix_bias):
    rows, width = value.shape
    groups = mix_weight.shape[0]
    length = rows * nsp
    chunks = 2 if groups % 2 == 0 else 1
    per = groups // chunks
    nblocks = -(-length // BLK)
    piece = jax.ShapeDtypeStruct((rows, per * GD), jnp.bfloat16)
    small = pltpu.CompilerParams(vmem_limit_bytes=16 << 20)

    columns = [(0, 2 * TILE, 0), (2 * TILE, TILE, 2), (3 * TILE, TILE, 3)] if exchange else []
    cuts = [(c * per, per, low, cols) for c in range(chunks) for low, cols, _ in columns]
    head = rows // 3
    span = groups * GD

    ncuts = len(cuts) // 2

    def bf16(*shape):
        return jax.ShapeDtypeStruct(shape, jnp.bfloat16)

    def cut_shapes(some):
        return [bf16(n, mix_weight.shape[1], cols) for _, n, _, cols in some]

    def cost(count):
        return pl.CostEstimate(flops=30 * count * width, bytes_accessed=4 * count * width, transcendentals=count * width)

    in_hbm = [pltpu.with_memory_space_constraint(x, pltpu.HBM) for x in (value, gain, bias, mix_weight)]
    lanes = [(s, 0, span) for s in range(nsp)]
    shapes = [bf16(head, span)] * nsp + cut_shapes(cuts[:ncuts]) + [bf16(rows - head, width), bf16(width), bf16(width)]
    made = pl.pallas_call(
        functools.partial(head_kernel, nsp, span, 16, lanes, cuts[:ncuts]),
        out_shape=shapes,
        in_specs=[HBM] * 4,
        out_specs=[VMEM] * len(shapes),
        scratch_shapes=[
            pltpu.VMEM((head, width), jnp.bfloat16),
            pltpu.VMEM((head, width), jnp.bfloat16),
            pltpu.SemaphoreType.DMA((4 + ncuts,)),
        ],
        compiler_params=small,
        cost_estimate=cost(head),
        name="norm_head",
    )(*in_hbm)
    first_sent, parts, ready = made[:nsp], made[nsp:nsp + ncuts], made[nsp + ncuts:]
    far = {s: exchange_step(s, first_sent[s], nsp) for s in steps_of(nsp)}
    early = [first_sent[0]] + [far[s] for s in range(1, nsp)]
    lanes = [(s, c * per * GD, per * GD) for c in range(chunks) for s in range(nsp)]
    shapes = [bf16(rows - head, per * GD)] * (nsp * chunks) + cut_shapes(cuts[ncuts:])
    made = pl.pallas_call(
        functools.partial(rest_kernel, nsp, span, 16, lanes, cuts[ncuts:]),
        out_shape=shapes,
        in_specs=[VMEM] * 3 + [HBM],
        out_specs=[VMEM] * len(shapes),
        scratch_shapes=[
            pltpu.VMEM((rows - head, width), jnp.bfloat16),
            pltpu.SemaphoreType.DMA((max(1, ncuts),)),
        ],
        compiler_params=small,
        cost_estimate=cost(rows - head),
        name="norm_rest",
    )(*ready, in_hbm[3])
    sent, parts = made[:nsp * chunks], list(parts) + list(made[nsp * chunks:])
    weights = []
    if exchange:
        other = lax.ppermute(mix_weight, "dp", swap_pairs(ndp, 1))
        for c in range(chunks):
            mine = parts[c * len(columns):(c + 1) * len(columns)]
            mine = [(low, least, part) for (low, _, least), part in zip(columns, mine)]
            weights.append(exchange_rows((mix_weight, other), mine, ndp, c * per))
    else:
        whole = lax.all_gather(mix_weight, "dp", axis=1, tiled=True)
        weights = [[(whole, 0, i, 0, c * per) for i in range(BLK // TILE)] for c in range(chunks)]
    out = None
    got = []
    for c in range(chunks):
        mine = sent[c * nsp:(c + 1) * nsp]
        far = {s: exchange_step(s, mine[s], nsp) for s in steps_of(nsp)}
        got.append([mine[0]] + [far[s] for s in range(1, nsp)])
    backs = []
    for c in range(chunks):
        layout = [w[1:] for w in weights[c]]
        outs = pl.pallas_call(
            functools.partial(mix_kernel, nsp, length, c * per, c * per * GD, layout),
            out_shape=[piece] * nsp,
            in_specs=[VMEM] * (2 * nsp + len(layout) + 1),
            out_specs=[VMEM] * nsp,
            scratch_shapes=[
                pltpu.VMEM((per, BLK, nblocks * GD), jnp.bfloat16),
                pltpu.VMEM((nblocks * BLK, per * GD), jnp.bfloat16),
            ],
            compiler_params=pltpu.CompilerParams(vmem_limit_bytes=24 << 20),
            cost_estimate=pl.CostEstimate(flops=2 * per * BLK * length * GD, bytes_accessed=per * BLK * BLK, transcendentals=0),
        )(*early, *got[c], *[w[0] for w in weights[c]], mix_bias)
        far = {s: exchange_step(s, outs[s], nsp) for s in steps_of(nsp)}
        backs += [[outs[0]] + [far[s] for s in range(1, nsp)]]
    out = None
    order = list(range(nsp))
    calls = [(c, order) for c in range(chunks - 1)] + [(chunks - 1, order[:-1]), (chunks - 1, order[-1:])]
    for c, steps in calls:
        extra = [] if out is None else [out]
        share = rows * per * GD * len(steps)
        out = pl.pallas_call(
            functools.partial(gate_kernel, nsp, chunks, c, steps, 32),
            out_shape=jax.ShapeDtypeStruct((rows, width), jnp.bfloat16),
            in_specs=[VMEM] * (1 + len(steps)) + [HBM] * len(extra),
            out_specs=HBM,
            scratch_shapes=[pltpu.VMEM((len(steps), rows, per * GD), jnp.bfloat16), pltpu.SemaphoreType.DMA((len(steps),))],
            input_output_aliases={len(steps) + 1: 0} if extra else {},
            compiler_params=small,
            cost_estimate=pl.CostEstimate(flops=12 * share, bytes_accessed=6 * share, transcendentals=share),
        )(gate, *[backs[c][s] for s in steps], *extra)
    return out


def body(nsp, ndp, exchange, gate_input, value_input, norm_gain, norm_bias, mix_weight, mix_bias):
    outs = [
        compute(nsp, ndp, exchange, gate_input[q], value_input[q], norm_gain, norm_bias, mix_weight, mix_bias)
        for q in range(value_input.shape[0])
    ]
    return jnp.stack(outs)


def solution(mesh):
    nsp, ndp = mesh.shape["sp"], mesh.shape["dp"]
    exchange = ndp == BLK // TILE == 4
    placed = (
        P(("grp", "dp"), "sp", None),
        P(("grp", "dp"), "sp", None),
        P(),
        P(),
        P("sp", "dp", None),
        P("sp", None),
    )
    return jax.shard_map(
        functools.partial(body, nsp, ndp, exchange),
        mesh=mesh,
        in_specs=placed,
        out_specs=P(("grp", "dp"), "sp", None),
        check_vma=False,
    )
```

time: 111 us -> 112 us (level); the launches traced: 109 us -> 111 us
  starting transfers between devices: 31.6 us -> 42.7 us
  waiting for transfers between devices: 67.9 us -> 58.5 us
    ppermute x12 -> x15, starting transfers between devices: 19.9 us -> 29.4 us  [exchange_step(): return lax.ppermute(x, 'sp', swap_pairs(shards, step))]
    ppermute x12 -> x15, waiting for transfers between devices: 45.9 us -> 37.1 us  [exchange_step(): return lax.ppermute(x, 'sp', swap_pairs(shards, step))]
    ppermute x6, starting transfers between devices: 3.09 us -> 4.4 us  [exchange_rows(): got.append((lax.ppermute(far, 'dp', swap_pairs(ndp, 1)), 3, None, low, 0))]
    pallas_call x5 -> x7, Pallas kernels: 9.64 us -> 10.1 us  [the longest x3 3.6 us: compute(): pl.pallas_call(functools.partial(gate_kernel, nsp, chunks, c, steps, 32),...]
  transfers between devices with their start and end apart: 25 -> 28, of which waited for: 9 -> 11; matrix products, arithmetic and copies ran while one was open for 0% -> 0% of each run, Pallas kernels for 8% -> 8%
where the time goes in v3:
time: 112 us; the launch traced here: 111 us
  waiting for transfers between devices  58.5 us (52%)
  starting transfers between devices  42.7 us (38%)
  Pallas kernels  10.1 us (9%)
    ppermute x15, waiting for transfers between devices, exchange_step(): return lax.ppermute(x, 'sp', swap_pairs(shards, step))  37.1 us
    ppermute x15, starting transfers between devices, exchange_step(): return lax.ppermute(x, 'sp', swap_pairs(shards, step))  29.4 us
    ppermute x6, waiting for transfers between devices, exchange_rows(): lax.ppermute(part, 'dp', [p for p in swap_pairs(ndp, 2) if p[0] >= least])  20.8 us
    ppermute x6, starting transfers between devices, exchange_rows(): lax.ppermute(part, 'dp', [p for p in swap_pairs(ndp, 2) if p[0] >= least])  8.33 us
    ppermute x6, starting transfers between devices, exchange_rows(): got.append((lax.ppermute(far, 'dp', swap_pairs(ndp, 1)), 3, None, low, 0))  4.4 us
    pallas_call x3, Pallas kernels, compute(): pl.pallas_call(functools.partial(gate_kernel, nsp, chunks, c, steps, 32),...  3.6 us
    pallas_call x2, Pallas kernels, compute(): pl.pallas_call(functools.partial(mix_kernel, nsp, length, c * per, c * pe...  3.39 us
  transfers between devices with their start and end apart: 28, of which 11 were waited for; matrix products, arithmetic and copies ran while one was open for 0% of the time, Pallas kernels for 8%

profile of v3, /device:TPU:0, one launch (start us, length us, event | category | flops | bytes accessed | tf_op | source)
XLA Modules:
  0.0 111.5 jit_solution(2726704903899066848)
XLA Ops:
  0.0 0.5 collective-permute-start.6
  0.5 1.8 %norm_head.1 = (bf16[128,512]{1,0:T(8,128)(2,1)S(1)}, bf16[128,512]{1,0:T(8,128)(2,1)S(1)}, bf16[128,512]{1,0:T(8,128)(2,1)S(1)}, bf16[128,512]{1,0:T(8,128)(2,1...) custom-call(bf16[384,2048]{1,0:T(8,128)(2,1)} %bitcast.6, ...), custom_call_target="tpu_custom_call" | custom-call | flops 7864320 | bytes 1048576 | tf_op jit(solution)/shard_map/norm_head/pallas_call | solution.py:218
  2.3 0.0 copy-start
  2.3 0.0 copy-start.2
  2.3 1.4 %norm_rest.1 = (bf16[256,256]{1,0:T(8,128)(2,1)S(1)}, bf16[256,256]{1,0:T(8,128)(2,1)S(1)}, bf16[256,256]{1,0:T(8,128)(2,1)S(1)}, bf16[256,256]{1,0:T(8,128)(2,1...) custom-call(bf16[256,2048]{1,0:T(8,128)(2,1)S(1)} %get-tuple-element, ...), custom_call_target="tpu_custom_call" | custom-call | flops 15728640 | bytes 2097152 | tf_op jit(solution)/shard_map/norm_rest/pallas_call | solution.py:237
  3.7 2.6 %collective-permute-start.16 = (bf16[256,256]{1,0:T(8,128)(2,1)S(1)}, bf16[256,256]{1,0:T(8,128)(2,1)S(1)}, u32[]{:S(2)}, u32[]{:S(2)}) collective-permute-start(bf16[256,256]{1,0:T(8,128)(2,1)S(1)} %get-tuple-element.53), channel_id=1, source_target_pairs={{0,4},{4,0},{8,12},{12,8},{1,5},{5,1},{9,13},{13,9},{2,6},{6,2},{1... | collective-permute-start | bytes 393224 | tf_op jit(solution)/shard_map/ppermute | solution.py:177
  6.3 2.6 %collective-permute-start.17 = (bf16[256,256]{1,0:T(8,128)(2,1)S(1)}, bf16[256,256]{1,0:T(8,128)(2,1)S(1)}, u32[]{:S(2)}, u32[]{:S(2)}) collective-permute-start(bf16[256,256]{1,0:T(8,128)(2,1)S(1)} %get-tuple-element.54), channel_id=1, source_target_pairs={{0,8},{4,12},{8,0},{12,4},{1,9},{5,13},{9,1},{13,5},{2,10},{6,14},... | collective-permute-start | bytes 393224 | tf_op jit(solution)/shard_map/ppermute | solution.py:177
  8.9 0.0 collective-permute-start.18
  8.9 0.9 collective-permute-start
  9.8 3.1 %collective-permute-done.16.refs_5_ = bf16[256,256]{1,0:T(8,128)(2,1)S(1)} collective-permute-done((bf16[256,256]{1,0:T(8,128)(2,1)S(1)}, bf16[256,256]{1,0:T(8,128)(2,1)S(1)}, u32[]{:S(2)}, u32[]{:S(2)}) %collective-permute-start.16) | collective-permute-done | bytes 131104 | tf_op jit(solution)/shard_map/ppermute | solution.py:177
  12.9 2.0 %collective-permute-start.19 = (bf16[2,256,512]{2,1,0:T(8,128)(2,1)S(1)}, bf16[2,256,512]{2,1,0:T(8,128)(2,1)S(1)}, u32[]{:S(2)}, u32[]{:S(2)}) collective-permute-start(bf16[2,256,512]{2,1,0:T(8,128)(2,1)S(1)} %get-tuple-element.56), channel_id=1, source_target_pairs={{0,2},{1,3},{2,0},{3,1},{4,6},{5,7},{6,4},{7,5},{8,10},{9,11},{10,... | collective-permute-start | bytes 1572872 | tf_op jit(solution)/shard_map/ppermute | solution.py:183
  15.0 4.3 %collective-permute-done.17.refs_6_ = bf16[256,256]{1,0:T(8,128)(2,1)S(1)} collective-permute-done((bf16[256,256]{1,0:T(8,128)(2,1)S(1)}, bf16[256,256]{1,0:T(8,128)(2,1)S(1)}, u32[]{:S(2)}, u32[]{:S(2)}) %collective-permute-start.17) | collective-permute-done | bytes 131104 | tf_op jit(solution)/shard_map/ppermute | solution.py:177
  19.2 0.0 collective-permute-start.1
  19.2 0.0 collective-permute-done.18.refs_7_
  19.3 2.5 %collective-permute-start.2 = (bf16[128,512]{1,0:T(8,128)(2,1)S(1)}, bf16[128,512]{1,0:T(8,128)(2,1)S(1)}, u32[]{:S(2)}, u32[]{:S(2)}) collective-permute-start(bf16[128,512]{1,0:T(8,128)(2,1)S(1)} %get-tuple-element.37), channel_id=1, source_target_pairs={{0,12},{4,8},{8,4},{12,0},{1,13},{5,9},{9,5},{13,1},{2,14},{6,10},... | collective-permute-start | bytes 393224 | tf_op jit(solution)/shard_map/ppermute | solution.py:177
  21.7 0.0 collective-permute-done.refs_1_
  21.7 8.1 %collective-permute-start.3 = (bf16[256,256]{1,0:T(8,128)(2,1)S(1)}, bf16[256,256]{1,0:T(8,128)(2,1)S(1)}, u32[]{:S(2)}, u32[]{:S(2)}) collective-permute-start(bf16[256,256]{1,0:T(8,128)(2,1)S(1)} %get-tuple-element.42), channel_id=1, source_target_pairs={{0,4},{4,0},{8,12},{12,8},{1,5},{5,1},{9,13},{13,9},{2,6},{6,2},{1... | collective-permute-start | bytes 393224 | tf_op jit(solution)/shard_map/ppermute | solution.py:177
  29.9 0.6 collective-permute-done.1.refs_2_
  30.5 1.3 %collective-permute-start.21 = (bf16[2,256,256]{2,1,0:T(8,128)(2,1)S(1)}, bf16[2,256,256]{2,1,0:T(8,128)(2,1)S(1)}, u32[]{:S(2)}, u32[]{:S(2)}) collective-permute-start(bf16[2,256,256]{2,1,0:T(8,128)(2,1)S(1)} %get-tuple-element.57), channel_id=1, source_target_pairs={{2,0},{3,1},{6,4},{7,5},{10,8},{11,9},{14,12},{15,13},{18,16},{19,... | collective-permute-start | bytes 786440 | tf_op jit(solution)/shard_map/ppermute | solution.py:183
  31.8 0.0 collective-permute-done.2.refs_3_
  31.8 0.7 collective-permute-start.23
  32.5 0.3 collective-permute-done.3.refs_5_
  32.8 2.4 %collective-permute-start.7 = (bf16[2,256,512]{2,1,0:T(8,128)(2,1)S(1)}, bf16[2,256,512]{2,1,0:T(8,128)(2,1)S(1)}, u32[]{:S(2)}, u32[]{:S(2)}) collective-permute-start(bf16[2,256,512]{2,1,0:T(8,128)(2,1)S(1)} %get-tuple-element.45), channel_id=1, source_target_pairs={{0,2},{1,3},{2,0},{3,1},{4,6},{5,7},{6,4},{7,5},{8,10},{9,11},{10,... | collective-permute-start | bytes 1572872 | tf_op jit(solution)/shard_map/ppermute | solution.py:183
  35.2 6.3 %collective-permute-done.21.refs_12_ = bf16[2,256,256]{2,1,0:T(8,128)(2,1)S(1)} collective-permute-done((bf16[2,256,256]{2,1,0:T(8,128)(2,1)S(1)}, bf16[2,256,256]{2,1,0:T(8,128)(2,1)S(1)}, u32[]{:S(2)}, u32[]{:S(2)}) %collective-permute-start.21) | collective-permute-done | bytes 262176 | tf_op jit(solution)/shard_map/ppermute | solution.py:183
  41.5 1.3 %collective-permute-start.9 = (bf16[2,256,256]{2,1,0:T(8,128)(2,1)S(1)}, bf16[2,256,256]{2,1,0:T(8,128)(2,1)S(1)}, u32[]{:S(2)}, u32[]{:S(2)}) collective-permute-start(bf16[2,256,256]{2,1,0:T(8,128)(2,1)S(1)} %get-tuple-element.46), channel_id=1, source_target_pairs={{2,0},{3,1},{6,4},{7,5},{10,8},{11,9},{14,12},{15,13},{18,16},{19,... | collective-permute-start | bytes 786440 | tf_op jit(solution)/shard_map/ppermute | solution.py:183
  42.8 0.0 collective-permute-done.23.refs_14_
  42.8 0.7 collective-permute-start.11
  43.5 0.0 collective-permute-done.19.refs_10_
  43.5 0.4 collective-permute-start.20
  44.0 14.4 %collective-permute-done.9.refs_12_ = bf16[2,256,256]{2,1,0:T(8,128)(2,1)S(1)} collective-permute-done((bf16[2,256,256]{2,1,0:T(8,128)(2,1)S(1)}, bf16[2,256,256]{2,1,0:T(8,128)(2,1)S(1)}, u32[]{:S(2)}, u32[]{:S(2)}) %collective-permute-start.9) | collective-permute-done | bytes 262176 | tf_op jit(solution)/shard_map/ppermute | solution.py:183
  58.4 0.3 collective-permute-start.22
  58.7 0.0 collective-permute-done.11.refs_14_
  58.7 2.8 %collective-permute-start.24 = (bf16[2,256,256]{2,1,0:T(8,128)(2,1)S(1)}, bf16[2,256,256]{2,1,0:T(8,128)(2,1)S(1)}, u32[]{:S(2)}, u32[]{:S(2)}) collective-permute-start(bf16[2,256,256]{2,1,0:T(8,128)(2,1)S(1)} %collective-permute-done.23.refs_14_), channel_id=1, source_target_pairs={{0,1},{1,0},{2,3},{3,2},{4,5},{5,4},{6,7},{7,6},{8,9},{9,8},{10,11... | collective-permute-start | bytes 786440 | tf_op jit(solution)/shard_map/ppermute | solution.py:185
  61.5 0.0 collective-permute-done.7.refs_10_
  61.5 0.0 collective-permute-start.8
  61.5 0.0 collective-permute-done.22.refs_13_
  61.5 0.5 collective-permute-start.10
  62.0 0.6 collective-permute-done.24.refs_15_
  62.7 0.4 collective-permute-start.12
  63.0 0.0 collective-permute-done.20.refs_11_
  63.0 0.0 collective-permute-start.4
  63.0 0.0 collective-permute-done.6.refs_9_
  63.0 2.6 %collective-permute-start.5 = (bf16[256,256]{1,0:T(8,128)(2,1)S(1)}, bf16[256,256]{1,0:T(8,128)(2,1)S(1)}, u32[]{:S(2)}, u32[]{:S(2)}) collective-permute-start(bf16[256,256]{1,0:T(8,128)(2,1)S(1)} %get-tuple-element.44), channel_id=1, source_target_pairs={{0,12},{4,8},{8,4},{12,0},{1,13},{5,9},{9,5},{13,1},{2,14},{6,10},... | collective-permute-start | bytes 393224 | tf_op jit(solution)/shard_map/ppermute | solution.py:177
  65.6 1.7 %shard_map.65 = (bf16[384,256]{1,0:T(8,128)(2,1)S(1)}, bf16[384,256]{1,0:T(8,128)(2,1)S(1)}, bf16[384,256]{1,0:T(8,128)(2,1)S(1)}, bf16[384,256]{1,0:T(8,128)(2,1)S(1)}) custom-call(bf16[128,512]{1,0:T(8,128)(2,1)S(1)} %get-tuple-element.34.refs_0_, bf16[128,512]{1,0:T(8,128)(2,1)S(1)} %collective-permute-done.refs_1_, ...), custom_call_target="tpu_custom_call" | custom-call | flops 805306368 | bytes 2097152 | tf_op jit(solution)/shard_map/pallas_call | solution.py:270
  67.3 7.7 %collective-permute-done.4.refs_6_ = bf16[256,256]{1,0:T(8,128)(2,1)S(1)} collective-permute-done((bf16[256,256]{1,0:T(8,128)(2,1)S(1)}, bf16[256,256]{1,0:T(8,128)(2,1)S(1)}, u32[]{:S(2)}, u32[]{:S(2)}) %collective-permute-start.4) | collective-permute-done | bytes 131104 | tf_op jit(solution)/shard_map/ppermute | solution.py:177
  75.1 0.0 collective-permute-start.25
  75.1 0.0 collective-permute-done.5.refs_7_
  75.1 3.1 %collective-permute-start.26 = (bf16[384,256]{1,0:T(8,128)(2,1)S(1)}, bf16[384,256]{1,0:T(8,128)(2,1)S(1)}, u32[]{:S(2)}, u32[]{:S(2)}) collective-permute-start(bf16[384,256]{1,0:T(8,128)(2,1)S(1)} %get-tuple-element.61), channel_id=1, source_target_pairs={{0,8},{4,12},{8,0},{12,4},{1,9},{5,13},{9,1},{13,5},{2,10},{6,14},... | collective-permute-start | bytes 589832 | tf_op jit(solution)/shard_map/ppermute | solution.py:177
  78.2 0.0 collective-permute-done.10.refs_13_
  78.2 2.5 %collective-permute-start.27 = (bf16[384,256]{1,0:T(8,128)(2,1)S(1)}, bf16[384,256]{1,0:T(8,128)(2,1)S(1)}, u32[]{:S(2)}, u32[]{:S(2)}) collective-permute-start(bf16[384,256]{1,0:T(8,128)(2,1)S(1)} %get-tuple-element.62), channel_id=1, source_target_pairs={{0,12},{4,8},{8,4},{12,0},{1,13},{5,9},{9,5},{13,1},{2,14},{6,10},... | collective-permute-start | bytes 589832 | tf_op jit(solution)/shard_map/ppermute | solution.py:177
  80.7 0.0 collective-permute-done.12.refs_15_
  80.7 0.0 collective-permute-done.8.refs_11_
  80.7 1.7 %shard_map.64 = (bf16[384,256]{1,0:T(8,128)(2,1)S(1)}, bf16[384,256]{1,0:T(8,128)(2,1)S(1)}, bf16[384,256]{1,0:T(8,128)(2,1)S(1)}, bf16[384,256]{1,0:T(8,128)(2,1)S(1)}) custom-call(bf16[128,512]{1,0:T(8,128)(2,1)S(1)} %get-tuple-element.34.refs_0_, bf16[128,512]{1,0:T(8,128)(2,1)S(1)} %collective-permute-done.refs_1_, ...), custom_call_target="tpu_custom_call" | custom-call | flops 805306368 | bytes 2097152 | tf_op jit(solution)/shard_map/pallas_call | solution.py:270
  82.4 0.1 collective-permute-start.14
  82.5 1.8 %collective-permute-start.15 = (bf16[384,256]{1,0:T(8,128)(2,1)S(1)}, bf16[384,256]{1,0:T(8,128)(2,1)S(1)}, u32[]{:S(2)}, u32[]{:S(2)}) collective-permute-start(bf16[384,256]{1,0:T(8,128)(2,1)S(1)} %get-tuple-element.51), channel_id=1, source_target_pairs={{0,8},{4,12},{8,0},{12,4},{1,9},{5,13},{9,1},{13,5},{2,10},{6,14},... | collective-permute-start | bytes 589832 | tf_op jit(solution)/shard_map/ppermute | solution.py:177
  84.4 2.5 %collective-permute-start.13 = (bf16[384,256]{1,0:T(8,128)(2,1)S(1)}, bf16[384,256]{1,0:T(8,128)(2,1)S(1)}, u32[]{:S(2)}, u32[]{:S(2)}) collective-permute-start(bf16[384,256]{1,0:T(8,128)(2,1)S(1)} %get-tuple-element.48), channel_id=1, source_target_pairs={{0,12},{4,8},{8,4},{12,0},{1,13},{5,9},{9,5},{13,1},{2,14},{6,10},... | collective-permute-start | bytes 589832 | tf_op jit(solution)/shard_map/ppermute | solution.py:177
  86.9 5.6 %collective-permute-done.26.refs_2_ = bf16[384,256]{1,0:T(8,128)(2,1)S(1)} collective-permute-done((bf16[384,256]{1,0:T(8,128)(2,1)S(1)}, bf16[384,256]{1,0:T(8,128)(2,1)S(1)}, u32[]{:S(2)}, u32[]{:S(2)}) %collective-permute-start.26) | collective-permute-done | bytes 196640 | tf_op jit(solution)/shard_map/ppermute | solution.py:177
  92.5 0.0 collective-permute-done.27.refs_3_
  92.5 1.5 %shard_map.66.refs_3_ = bf16[384,2048]{1,0:T(8,128)(2,1)} custom-call(bf16[384,2048]{1,0:T(8,128)(2,1)S(1)} %bitcast.3, bf16[384,256]{1,0:T(8,128)(2,1)S(1)} %get-tuple-element.59.refs_0_, bf16[384,256]{1,0:T(8,128)(2,1)S(1)} %collective-permute-done.25.refs_1_, bf16[384,256]{1,0:T(8,128)(2,1)S(1)} %collective-permute-done.26.refs_2_, ...), custom_call_target="tpu_custom_call" | custom-call | flops 4718592 | bytes 2359296 | tf_op jit(solution)/shard_map/pallas_call | solution.py:290
  93.9 0.9 collective-permute-done.14.refs_1_
  94.9 14.4 %collective-permute-done.15.refs_2_ = bf16[384,256]{1,0:T(8,128)(2,1)S(1)} collective-permute-done((bf16[384,256]{1,0:T(8,128)(2,1)S(1)}, bf16[384,256]{1,0:T(8,128)(2,1)S(1)}, u32[]{:S(2)}, u32[]{:S(2)}) %collective-permute-start.15) | collective-permute-done | bytes 196640 | tf_op jit(solution)/shard_map/ppermute | solution.py:177
  109.3 1.3 %shard_map.67.refs_1_ = bf16[384,2048]{1,0:T(8,128)(2,1)} custom-call(bf16[384,2048]{1,0:T(8,128)(2,1)S(1)} %bitcast.4, bf16[384,256]{1,0:T(8,128)(2,1)S(1)} %get-tuple-element.49.refs_0_, bf16[384,256]{1,0:T(8,128)(2,1)S(1)} %collective-permute-done.14.refs_1_, ...), custom_call_target="tpu_custom_call", output_to_operand_aliasing={{}: (4, {})} | custom-call | flops 3538944 | bytes 1769472 | tf_op jit(solution)/shard_map/pallas_call | solution.py:290
  110.6 0.0 collective-permute-done.13.refs_0_
  110.6 0.9 shard_map.68
  (5 shorter events, 0.0 us)
Async XLA Ops:
  0.0 63.0 %collective-permute-start.6 = (bf16[4,256,1024]{2,1,0:T(8,128)(2,1)}, bf16[4,256,1024]{2,1,0:T(8,128)(2,1)S(1)}, u32[]{:S(2)}, u32[]{:S(2)}) collective-permute-start(bf16[4,256,1024]{2,1,0:T(8,128)(2,1)} %refs_8_.3), channel_id=1, source_target_pairs={{0,1},{1,0},{2,3},{3,2},{4,5},{5,4},{6,7},{7,6},{8,9},{9,8},{10,11... | collective-permute-start | bytes 6291464 | tf_op jit(solution)/shard_map/ppermute | solution.py:253
  2.3 63.4 %copy-start = (bf16[4,256,1024]{2,1,0:T(8,128)(2,1)S(1)}, bf16[4,256,1024]{2,1,0:T(8,128)(2,1)}, u32[]{:S(2)}) copy-start(bf16[4,256,1024]{2,1,0:T(8,128)(2,1)} %refs_8_.3) | copy-start | bytes 6291460
  2.3 63.4 %copy-start.2 = (bf16[4,1024]{1,0:T(4,128)(2,1)S(1)}, bf16[4,1024]{1,0:T(4,128)(2,1)}, u32[]{:S(2)}) copy-start(bf16[4,1024]{1,0:T(4,128)(2,1)} %refs_16_.3) | copy-start | bytes 24580
  3.7 9.3 %collective-permute-start.16 = (bf16[256,256]{1,0:T(8,128)(2,1)S(1)}, bf16[256,256]{1,0:T(8,128)(2,1)S(1)}, u32[]{:S(2)}, u32[]{:S(2)}) collective-permute-start(bf16[256,256]{1,0:T(8,128)(2,1)S(1)} %get-tuple-element.53), channel_id=1, source_target_pairs={{0,4},{4,0},{8,12},{12,8},{1,5},{5,1},{9,13},{13,9},{2,6},{6,2},{1... | collective-permute-start | bytes 393224 | tf_op jit(solution)/shard_map/ppermute | solution.py:177
  6.3 13.0 %collective-permute-start.17 = (bf16[256,256]{1,0:T(8,128)(2,1)S(1)}, bf16[256,256]{1,0:T(8,128)(2,1)S(1)}, u32[]{:S(2)}, u32[]{:S(2)}) collective-permute-start(bf16[256,256]{1,0:T(8,128)(2,1)S(1)} %get-tuple-element.54), channel_id=1, source_target_pairs={{0,8},{4,12},{8,0},{12,4},{1,9},{5,13},{9,1},{13,5},{2,10},{6,14},... | collective-permute-start | bytes 393224 | tf_op jit(solution)/shard_map/ppermute | solution.py:177
  8.9 10.4 %collective-permute-start.18 = (bf16[256,256]{1,0:T(8,128)(2,1)S(1)}, bf16[256,256]{1,0:T(8,128)(2,1)S(1)}, u32[]{:S(2)}, u32[]{:S(2)}) collective-permute-start(bf16[256,256]{1,0:T(8,128)(2,1)S(1)} %get-tuple-element.55), channel_id=1, source_target_pairs={{0,12},{4,8},{8,4},{12,0},{1,13},{5,9},{9,5},{13,1},{2,14},{6,10},... | collective-permute-start | bytes 393224 | tf_op jit(solution)/shard_map/ppermute | solution.py:177
  8.9 12.9 %collective-permute-start = (bf16[128,512]{1,0:T(8,128)(2,1)S(1)}, bf16[128,512]{1,0:T(8,128)(2,1)S(1)}, u32[]{:S(2)}, u32[]{:S(2)}) collective-permute-start(bf16[128,512]{1,0:T(8,128)(2,1)S(1)} %get-tuple-element.35), channel_id=1, source_target_pairs={{0,4},{4,0},{8,12},{12,8},{1,5},{5,1},{9,13},{13,9},{2,6},{6,2},{1... | collective-permute-start | bytes 393224 | tf_op jit(solution)/shard_map/ppermute | solution.py:177
  12.9 30.6 %collective-permute-start.19 = (bf16[2,256,512]{2,1,0:T(8,128)(2,1)S(1)}, bf16[2,256,512]{2,1,0:T(8,128)(2,1)S(1)}, u32[]{:S(2)}, u32[]{:S(2)}) collective-permute-start(bf16[2,256,512]{2,1,0:T(8,128)(2,1)S(1)} %get-tuple-element.56), channel_id=1, source_target_pairs={{0,2},{1,3},{2,0},{3,1},{4,6},{5,7},{6,4},{7,5},{8,10},{9,11},{10,... | collective-permute-start | bytes 1572872 | tf_op jit(solution)/shard_map/ppermute | solution.py:183
  19.2 11.2 %collective-permute-start.1 = (bf16[128,512]{1,0:T(8,128)(2,1)S(1)}, bf16[128,512]{1,0:T(8,128)(2,1)S(1)}, u32[]{:S(2)}, u32[]{:S(2)}) collective-permute-start(bf16[128,512]{1,0:T(8,128)(2,1)S(1)} %get-tuple-element.36), channel_id=1, source_target_pairs={{0,8},{4,12},{8,0},{12,4},{1,9},{5,13},{9,1},{13,5},{2,10},{6,14},... | collective-permute-start | bytes 393224 | tf_op jit(solution)/shard_map/ppermute | solution.py:177
  19.3 12.5 %collective-permute-start.2 = (bf16[128,512]{1,0:T(8,128)(2,1)S(1)}, bf16[128,512]{1,0:T(8,128)(2,1)S(1)}, u32[]{:S(2)}, u32[]{:S(2)}) collective-permute-start(bf16[128,512]{1,0:T(8,128)(2,1)S(1)} %get-tuple-element.37), channel_id=1, source_target_pairs={{0,12},{4,8},{8,4},{12,0},{1,13},{5,9},{9,5},{13,1},{2,14},{6,10},... | collective-permute-start | bytes 393224 | tf_op jit(solution)/shard_map/ppermute | solution.py:177
  21.7 11.1 %collective-permute-start.3 = (bf16[256,256]{1,0:T(8,128)(2,1)S(1)}, bf16[256,256]{1,0:T(8,128)(2,1)S(1)}, u32[]{:S(2)}, u32[]{:S(2)}) collective-permute-start(bf16[256,256]{1,0:T(8,128)(2,1)S(1)} %get-tuple-element.42), channel_id=1, source_target_pairs={{0,4},{4,0},{8,12},{12,8},{1,5},{5,1},{9,13},{13,9},{2,6},{6,2},{1... | collective-permute-start | bytes 393224 | tf_op jit(solution)/shard_map/ppermute | solution.py:177
  30.5 11.1 %collective-permute-start.21 = (bf16[2,256,256]{2,1,0:T(8,128)(2,1)S(1)}, bf16[2,256,256]{2,1,0:T(8,128)(2,1)S(1)}, u32[]{:S(2)}, u32[]{:S(2)}) collective-permute-start(bf16[2,256,256]{2,1,0:T(8,128)(2,1)S(1)} %get-tuple-element.57), channel_id=1, source_target_pairs={{2,0},{3,1},{6,4},{7,5},{10,8},{11,9},{14,12},{15,13},{18,16},{19,... | collective-permute-start | bytes 786440 | tf_op jit(solution)/shard_map/ppermute | solution.py:183
  31.8 11.1 %collective-permute-start.23 = (bf16[2,256,256]{2,1,0:T(8,128)(2,1)S(1)}, bf16[2,256,256]{2,1,0:T(8,128)(2,1)S(1)}, u32[]{:S(2)}, u32[]{:S(2)}) collective-permute-start(bf16[2,256,256]{2,1,0:T(8,128)(2,1)S(1)} %get-tuple-element.58), channel_id=1, source_target_pairs={{3,1},{7,5},{11,9},{15,13},{19,17},{23,21},{27,25},{31,29}} | collective-permute-start | bytes 786440 | tf_op jit(solution)/shard_map/ppermute | solution.py:183
  32.8 28.7 %collective-permute-start.7 = (bf16[2,256,512]{2,1,0:T(8,128)(2,1)S(1)}, bf16[2,256,512]{2,1,0:T(8,128)(2,1)S(1)}, u32[]{:S(2)}, u32[]{:S(2)}) collective-permute-start(bf16[2,256,512]{2,1,0:T(8,128)(2,1)S(1)} %get-tuple-element.45), channel_id=1, source_target_pairs={{0,2},{1,3},{2,0},{3,1},{4,6},{5,7},{6,4},{7,5},{8,10},{9,11},{10,... | collective-permute-start | bytes 1572872 | tf_op jit(solution)/shard_map/ppermute | solution.py:183
  41.5 16.9 %collective-permute-start.9 = (bf16[2,256,256]{2,1,0:T(8,128)(2,1)S(1)}, bf16[2,256,256]{2,1,0:T(8,128)(2,1)S(1)}, u32[]{:S(2)}, u32[]{:S(2)}) collective-permute-start(bf16[2,256,256]{2,1,0:T(8,128)(2,1)S(1)} %get-tuple-element.46), channel_id=1, source_target_pairs={{2,0},{3,1},{6,4},{7,5},{10,8},{11,9},{14,12},{15,13},{18,16},{19,... | collective-permute-start | bytes 786440 | tf_op jit(solution)/shard_map/ppermute | solution.py:183
  42.8 15.8 %collective-permute-start.11 = (bf16[2,256,256]{2,1,0:T(8,128)(2,1)S(1)}, bf16[2,256,256]{2,1,0:T(8,128)(2,1)S(1)}, u32[]{:S(2)}, u32[]{:S(2)}) collective-permute-start(bf16[2,256,256]{2,1,0:T(8,128)(2,1)S(1)} %get-tuple-element.47), channel_id=1, source_target_pairs={{3,1},{7,5},{11,9},{15,13},{19,17},{23,21},{27,25},{31,29}} | collective-permute-start | bytes 786440 | tf_op jit(solution)/shard_map/ppermute | solution.py:183
  43.5 19.5 %collective-permute-start.20 = (bf16[2,256,512]{2,1,0:T(8,128)(2,1)S(1)}, bf16[2,256,512]{2,1,0:T(8,128)(2,1)S(1)}, u32[]{:S(2)}, u32[]{:S(2)}) collective-permute-start(bf16[2,256,512]{2,1,0:T(8,128)(2,1)S(1)} %collective-permute-done.19.refs_10_), channel_id=1, source_target_pairs={{0,1},{1,0},{2,3},{3,2},{4,5},{5,4},{6,7},{7,6},{8,9},{9,8},{10,11... | collective-permute-start | bytes 1572872 | tf_op jit(solution)/shard_map/ppermute | solution.py:185
  58.4 3.1 %collective-permute-start.22 = (bf16[2,256,256]{2,1,0:T(8,128)(2,1)S(1)}, bf16[2,256,256]{2,1,0:T(8,128)(2,1)S(1)}, u32[]{:S(2)}, u32[]{:S(2)}) collective-permute-start(bf16[2,256,256]{2,1,0:T(8,128)(2,1)S(1)} %collective-permute-done.21.refs_12_), channel_id=1, source_target_pairs={{0,1},{1,0},{2,3},{3,2},{4,5},{5,4},{6,7},{7,6},{8,9},{9,8},{10,11... | collective-permute-start | bytes 786440 | tf_op jit(solution)/shard_map/ppermute | solution.py:185
  58.7 4.0 %collective-permute-start.24 = (bf16[2,256,256]{2,1,0:T(8,128)(2,1)S(1)}, bf16[2,256,256]{2,1,0:T(8,128)(2,1)S(1)}, u32[]{:S(2)}, u32[]{:S(2)}) collective-permute-start(bf16[2,256,256]{2,1,0:T(8,128)(2,1)S(1)} %collective-permute-done.23.refs_14_), channel_id=1, source_target_pairs={{0,1},{1,0},{2,3},{3,2},{4,5},{5,4},{6,7},{7,6},{8,9},{9,8},{10,11... | collective-permute-start | bytes 786440 | tf_op jit(solution)/shard_map/ppermute | solution.py:185
  61.5 19.2 %collective-permute-start.8 = (bf16[2,256,512]{2,1,0:T(8,128)(2,1)S(1)}, bf16[2,256,512]{2,1,0:T(8,128)(2,1)S(1)}, u32[]{:S(2)}, u32[]{:S(2)}) collective-permute-start(bf16[2,256,512]{2,1,0:T(8,128)(2,1)S(1)} %collective-permute-done.7.refs_10_), channel_id=1, source_target_pairs={{0,1},{1,0},{2,3},{3,2},{4,5},{5,4},{6,7},{7,6},{8,9},{9,8},{10,11... | collective-permute-start | bytes 1572872 | tf_op jit(solution)/shard_map/ppermute | solution.py:185
  61.5 16.7 %collective-permute-start.10 = (bf16[2,256,256]{2,1,0:T(8,128)(2,1)S(1)}, bf16[2,256,256]{2,1,0:T(8,128)(2,1)S(1)}, u32[]{:S(2)}, u32[]{:S(2)}) collective-permute-start(bf16[2,256,256]{2,1,0:T(8,128)(2,1)S(1)} %collective-permute-done.9.refs_12_), channel_id=1, source_target_pairs={{0,1},{1,0},{2,3},{3,2},{4,5},{5,4},{6,7},{7,6},{8,9},{9,8},{10,11... | collective-permute-start | bytes 786440 | tf_op jit(solution)/shard_map/ppermute | solution.py:185
  62.7 18.1 %collective-permute-start.12 = (bf16[2,256,256]{2,1,0:T(8,128)(2,1)S(1)}, bf16[2,256,256]{2,1,0:T(8,128)(2,1)S(1)}, u32[]{:S(2)}, u32[]{:S(2)}) collective-permute-start(bf16[2,256,256]{2,1,0:T(8,128)(2,1)S(1)} %collective-permute-done.11.refs_14_), channel_id=1, source_target_pairs={{0,1},{1,0},{2,3},{3,2},{4,5},{5,4},{6,7},{7,6},{8,9},{9,8},{10,11... | collective-permute-start | bytes 786440 | tf_op jit(solution)/shard_map/ppermute | solution.py:185
  63.0 12.0 %collective-permute-start.4 = (bf16[256,256]{1,0:T(8,128)(2,1)S(1)}, bf16[256,256]{1,0:T(8,128)(2,1)S(1)}, u32[]{:S(2)}, u32[]{:S(2)}) collective-permute-start(bf16[256,256]{1,0:T(8,128)(2,1)S(1)} %get-tuple-element.43), channel_id=1, source_target_pairs={{0,8},{4,12},{8,0},{12,4},{1,9},{5,13},{9,1},{13,5},{2,10},{6,14},... | collective-permute-start | bytes 393224 | tf_op jit(solution)/shard_map/ppermute | solution.py:177
  63.0 12.0 %collective-permute-start.5 = (bf16[256,256]{1,0:T(8,128)(2,1)S(1)}, bf16[256,256]{1,0:T(8,128)(2,1)S(1)}, u32[]{:S(2)}, u32[]{:S(2)}) collective-permute-start(bf16[256,256]{1,0:T(8,128)(2,1)S(1)} %get-tuple-element.44), channel_id=1, source_target_pairs={{0,12},{4,8},{8,4},{12,0},{1,13},{5,9},{9,5},{13,1},{2,14},{6,10},... | collective-permute-start | bytes 393224 | tf_op jit(solution)/shard_map/ppermute | solution.py:177
  75.1 9.3 %collective-permute-start.25 = (bf16[384,256]{1,0:T(8,128)(2,1)S(1)}, bf16[384,256]{1,0:T(8,128)(2,1)S(1)}, u32[]{:S(2)}, u32[]{:S(2)}) collective-permute-start(bf16[384,256]{1,0:T(8,128)(2,1)S(1)} %get-tuple-element.60), channel_id=1, source_target_pairs={{0,4},{4,0},{8,12},{12,8},{1,5},{5,1},{9,13},{13,9},{2,6},{6,2},{1... | collective-permute-start | bytes 589832 | tf_op jit(solution)/shard_map/ppermute | solution.py:177
  75.1 17.4 %collective-permute-start.26 = (bf16[384,256]{1,0:T(8,128)(2,1)S(1)}, bf16[384,256]{1,0:T(8,128)(2,1)S(1)}, u32[]{:S(2)}, u32[]{:S(2)}) collective-permute-start(bf16[384,256]{1,0:T(8,128)(2,1)S(1)} %get-tuple-element.61), channel_id=1, source_target_pairs={{0,8},{4,12},{8,0},{12,4},{1,9},{5,13},{9,1},{13,5},{2,10},{6,14},... | collective-permute-start | bytes 589832 | tf_op jit(solution)/shard_map/ppermute | solution.py:177
  78.2 14.3 %collective-permute-start.27 = (bf16[384,256]{1,0:T(8,128)(2,1)S(1)}, bf16[384,256]{1,0:T(8,128)(2,1)S(1)}, u32[]{:S(2)}, u32[]{:S(2)}) collective-permute-start(bf16[384,256]{1,0:T(8,128)(2,1)S(1)} %get-tuple-element.62), channel_id=1, source_target_pairs={{0,12},{4,8},{8,4},{12,0},{1,13},{5,9},{9,5},{13,1},{2,14},{6,10},... | collective-permute-start | bytes 589832 | tf_op jit(solution)/shard_map/ppermute | solution.py:177
  80.7 11.7 %copy-start.1 = (bf16[1,384,2048]{2,1,0:T(8,128)(2,1)S(1)}, bf16[1,384,2048]{2,1,0:T(8,128)(2,1)}, u32[]{:S(2)}) copy-start(bf16[1,384,2048]{2,1,0:T(8,128)(2,1)} %param.6) | copy-start | bytes 4718596
  82.4 12.4 %collective-permute-start.14 = (bf16[384,256]{1,0:T(8,128)(2,1)S(1)}, bf16[384,256]{1,0:T(8,128)(2,1)S(1)}, u32[]{:S(2)}, u32[]{:S(2)}) collective-permute-start(bf16[384,256]{1,0:T(8,128)(2,1)S(1)} %get-tuple-element.50), channel_id=1, source_target_pairs={{0,4},{4,0},{8,12},{12,8},{1,5},{5,1},{9,13},{13,9},{2,6},{6,2},{1... | collective-permute-start | bytes 589832 | tf_op jit(solution)/shard_map/ppermute | solution.py:177
  82.5 26.8 %collective-permute-start.15 = (bf16[384,256]{1,0:T(8,128)(2,1)S(1)}, bf16[384,256]{1,0:T(8,128)(2,1)S(1)}, u32[]{:S(2)}, u32[]{:S(2)}) collective-permute-start(bf16[384,256]{1,0:T(8,128)(2,1)S(1)} %get-tuple-element.51), channel_id=1, source_target_pairs={{0,8},{4,12},{8,0},{12,4},{1,9},{5,13},{9,1},{13,5},{2,10},{6,14},... | collective-permute-start | bytes 589832 | tf_op jit(solution)/shard_map/ppermute | solution.py:177
  84.4 26.2 %collective-permute-start.13 = (bf16[384,256]{1,0:T(8,128)(2,1)S(1)}, bf16[384,256]{1,0:T(8,128)(2,1)S(1)}, u32[]{:S(2)}, u32[]{:S(2)}) collective-permute-start(bf16[384,256]{1,0:T(8,128)(2,1)S(1)} %get-tuple-element.48), channel_id=1, source_target_pairs={{0,12},{4,8},{8,4},{12,0},{1,13},{5,9},{9,5},{13,1},{2,14},{6,10},... | collective-permute-start | bytes 589832 | tf_op jit(solution)/shard_map/ppermute | solution.py:177

commit v4 on v3

--- a/solution.py
+++ b/solution.py
@@ -47,7 +47,7 @@
         return carry
 
     steps = value.shape[0] // rows_step
-    lax.fori_loop(0, steps, step, 0, unroll=8 if steps % 8 == 0 else 1)
+    lax.fori_loop(0, steps, step, 0, unroll=next(u for u in (8, 6, 4, 1) if steps % u == 0))
 
 
 def hand_out(shards, span, lanes, held, outs):
@@ -69,10 +69,12 @@
     outs, parts = refs[:len(lanes)], refs[len(lanes):len(lanes) + len(cuts)]
     rest, gain, bias, value, held, sems = refs[len(lanes) + len(cuts):]
     head = value.shape[0]
+    half = head // 2
     pairs = [
-        (value_ref.at[pl.ds(0, head), :], value),
+        (value_ref.at[pl.ds(0, half), :], value.at[pl.ds(0, half), :]),
         (gain_ref, gain),
         (bias_ref, bias),
+        (value_ref.at[pl.ds(half, head - half), :], value.at[pl.ds(half, head - half), :]),
         (value_ref.at[pl.ds(head, rest.shape[0]), :], rest),
     ]
     copies = [pltpu.make_async_copy(source, target, sems.at[k]) for k, (source, target) in enumerate(pairs)]
@@ -83,9 +85,11 @@
         copy.wait()
     scale = gain[...].astype(jnp.float32).reshape(1, -1)
     offset = bias[...].astype(jnp.float32).reshape(1, -1)
-    normalise(value, held, scale, offset, rows_step)
+    normalise(value.at[pl.ds(0, half), :], held.at[pl.ds(0, half), :], scale, offset, rows_step)
+    copies[3].wait()
+    normalise(value.at[pl.ds(half, head - half), :], held.at[pl.ds(half, head - half), :], scale, offset, rows_step)
     hand_out(shards, span, lanes, held, outs)
-    for copy in copies[3:]:
+    for copy in copies[4:]:
         copy.wait()
 
 
@@ -156,19 +160,24 @@
     here = lax.axis_index("sp")
     width = pieces[0].shape[1]
     copies = []
+    parts = sems.shape[1]
+    block = gate_ref.shape[0] // parts
     for k, s in enumerate(steps):
         start = (partner(here, s, shards)[1] * chunks + chunk) * width
         lanes = pl.ds(pl.multiple_of(start, GD), width)
 
-        def step(i, carry, k=k, lanes=lanes):
-            rows = pl.ds(pl.multiple_of(i * rows_step, rows_step), rows_step)
-            gate = 0.5 * twice_gelu(gate_ref[rows, lanes].astype(jnp.float32))
-            held[k, rows, :] = (gate * pieces[k][rows, :].astype(jnp.float32)).astype(jnp.bfloat16)
-            return carry
-
-        lax.fori_loop(0, gate_ref.shape[0] // rows_step, step, 0, unroll=4)
-        copies.append(pltpu.make_async_copy(held.at[k], out_ref.at[:, lanes], sems.at[k]))
-        copies[-1].start()
+        for part in range(parts):
+
+            def step(i, carry, k=k, part=part, lanes=lanes):
+                rows = pl.ds(pl.multiple_of(part * block + i * rows_step, rows_step), rows_step)
+                gate = 0.5 * twice_gelu(gate_ref[rows, lanes].astype(jnp.float32))
+                held[k, rows, :] = (gate * pieces[k][rows, :].astype(jnp.float32)).astype(jnp.bfloat16)
+                return carry
+
+            lax.fori_loop(0, block // rows_step, step, 0, unroll=4)
+            rows = pl.ds(part * block, block)
+            copies.append(pltpu.make_async_copy(held.at[k, rows, :], out_ref.at[rows, lanes], sems.at[k, part]))
+            copies[-1].start()
     for copy in copies:
         copy.wait()
 
@@ -223,7 +232,7 @@
         scratch_shapes=[
             pltpu.VMEM((head, width), jnp.bfloat16),
             pltpu.VMEM((head, width), jnp.bfloat16),
-            pltpu.SemaphoreType.DMA((4 + ncuts,)),
+            pltpu.SemaphoreType.DMA((5 + ncuts,)),
         ],
         compiler_params=small,
         cost_estimate=cost(head),
@@ -292,7 +301,7 @@
             out_shape=jax.ShapeDtypeStruct((rows, width), jnp.bfloat16),
             in_specs=[VMEM] * (1 + len(steps)) + [HBM] * len(extra),
             out_specs=HBM,
-            scratch_shapes=[pltpu.VMEM((len(steps), rows, per * GD), jnp.bfloat16), pltpu.SemaphoreType.DMA((len(steps),))],
+            scratch_shapes=[pltpu.VMEM((len(steps), rows, per * GD), jnp.bfloat16), pltpu.SemaphoreType.DMA((len(steps), 3 if rows % 96 == 0 else 1))],
             input_output_aliases={len(steps) + 1: 0} if extra else {},
             compiler_params=small,
             cost_estimate=pl.CostEstimate(flops=12 * share, bytes_accessed=6 * share, transcendentals=share),

time: 112 us -> 112 us (level)
  no operation moved by 1% of the time
where the time goes in v4:
time: 112 us; the launch traced here: 111 us
  waiting for transfers between devices  58.7 us (52%)
  starting transfers between devices  42.7 us (38%)
  Pallas kernels  9.82 us (9%)
    ppermute x15, waiting for transfers between devices, exchange_step(): return lax.ppermute(x, 'sp', swap_pairs(shards, step))  37.2 us
    ppermute x15, starting transfers between devices, exchange_step(): return lax.ppermute(x, 'sp', swap_pairs(shards, step))  29.4 us
    ppermute x6, waiting for transfers between devices, exchange_rows(): lax.ppermute(part, 'dp', [p for p in swap_pairs(ndp, 2) if p[0] >= least])  20.8 us
    ppermute x6, starting transfers between devices, exchange_rows(): lax.ppermute(part, 'dp', [p for p in swap_pairs(ndp, 2) if p[0] >= least])  8.32 us
    ppermute x6, starting transfers between devices, exchange_rows(): got.append((lax.ppermute(far, 'dp', swap_pairs(ndp, 1)), 3, None, low, 0))  4.4 us
    pallas_call x2, Pallas kernels, compute(): pl.pallas_call(functools.partial(mix_kernel, nsp, length, c * per, c * pe...  3.37 us
    pallas_call x3, Pallas kernels, compute(): pl.pallas_call(functools.partial(gate_kernel, nsp, chunks, c, steps, 32),...  3.32 us
  transfers between devices with their start and end apart: 28, of which 11 were waited for; matrix products, arithmetic and copies ran while one was open for 0% of the time, Pallas kernels for 8%

profile of v4, /device:TPU:0, one launch (start us, length us, event | category | flops | bytes accessed | tf_op | source)
XLA Modules:
  0.0 111.3 jit_solution(15446468645330209094)
XLA Ops:
  0.0 0.5 collective-permute-start.6
  0.5 1.8 %norm_head.1 = (bf16[128,512]{1,0:T(8,128)(2,1)S(1)}, bf16[128,512]{1,0:T(8,128)(2,1)S(1)}, bf16[128,512]{1,0:T(8,128)(2,1)S(1)}, bf16[128,512]{1,0:T(8,128)(2,1...) custom-call(bf16[384,2048]{1,0:T(8,128)(2,1)} %bitcast.6, ...), custom_call_target="tpu_custom_call" | custom-call | flops 7864320 | bytes 1048576 | tf_op jit(solution)/shard_map/norm_head/pallas_call | solution.py:227
  2.3 0.0 copy-start
  2.3 0.0 copy-start.2
  2.3 1.4 %norm_rest.1 = (bf16[256,256]{1,0:T(8,128)(2,1)S(1)}, bf16[256,256]{1,0:T(8,128)(2,1)S(1)}, bf16[256,256]{1,0:T(8,128)(2,1)S(1)}, bf16[256,256]{1,0:T(8,128)(2,1...) custom-call(bf16[256,2048]{1,0:T(8,128)(2,1)S(1)} %get-tuple-element, ...), custom_call_target="tpu_custom_call" | custom-call | flops 15728640 | bytes 2097152 | tf_op jit(solution)/shard_map/norm_rest/pallas_call | solution.py:246
  3.7 2.6 %collective-permute-start.16 = (bf16[256,256]{1,0:T(8,128)(2,1)S(1)}, bf16[256,256]{1,0:T(8,128)(2,1)S(1)}, u32[]{:S(2)}, u32[]{:S(2)}) collective-permute-start(bf16[256,256]{1,0:T(8,128)(2,1)S(1)} %get-tuple-element.53), channel_id=1, source_target_pairs={{0,4},{4,0},{8,12},{12,8},{1,5},{5,1},{9,13},{13,9},{2,6},{6,2},{1... | collective-permute-start | bytes 393224 | tf_op jit(solution)/shard_map/ppermute | solution.py:186
  6.3 2.6 %collective-permute-start.17 = (bf16[256,256]{1,0:T(8,128)(2,1)S(1)}, bf16[256,256]{1,0:T(8,128)(2,1)S(1)}, u32[]{:S(2)}, u32[]{:S(2)}) collective-permute-start(bf16[256,256]{1,0:T(8,128)(2,1)S(1)} %get-tuple-element.54), channel_id=1, source_target_pairs={{0,8},{4,12},{8,0},{12,4},{1,9},{5,13},{9,1},{13,5},{2,10},{6,14},... | collective-permute-start | bytes 393224 | tf_op jit(solution)/shard_map/ppermute | solution.py:186
  8.9 0.0 collective-permute-start.18
  8.9 0.9 collective-permute-start
  9.8 3.1 %collective-permute-done.16.refs_5_ = bf16[256,256]{1,0:T(8,128)(2,1)S(1)} collective-permute-done((bf16[256,256]{1,0:T(8,128)(2,1)S(1)}, bf16[256,256]{1,0:T(8,128)(2,1)S(1)}, u32[]{:S(2)}, u32[]{:S(2)}) %collective-permute-start.16) | collective-permute-done | bytes 131104 | tf_op jit(solution)/shard_map/ppermute | solution.py:186
  12.9 2.0 %collective-permute-start.19 = (bf16[2,256,512]{2,1,0:T(8,128)(2,1)S(1)}, bf16[2,256,512]{2,1,0:T(8,128)(2,1)S(1)}, u32[]{:S(2)}, u32[]{:S(2)}) collective-permute-start(bf16[2,256,512]{2,1,0:T(8,128)(2,1)S(1)} %get-tuple-element.56), channel_id=1, source_target_pairs={{0,2},{1,3},{2,0},{3,1},{4,6},{5,7},{6,4},{7,5},{8,10},{9,11},{10,... | collective-permute-start | bytes 1572872 | tf_op jit(solution)/shard_map/ppermute | solution.py:192
  15.0 4.3 %collective-permute-done.17.refs_6_ = bf16[256,256]{1,0:T(8,128)(2,1)S(1)} collective-permute-done((bf16[256,256]{1,0:T(8,128)(2,1)S(1)}, bf16[256,256]{1,0:T(8,128)(2,1)S(1)}, u32[]{:S(2)}, u32[]{:S(2)}) %collective-permute-start.17) | collective-permute-done | bytes 131104 | tf_op jit(solution)/shard_map/ppermute | solution.py:186
  19.3 0.0 collective-permute-start.1
  19.3 0.0 collective-permute-done.18.refs_7_
  19.3 2.5 %collective-permute-start.2 = (bf16[128,512]{1,0:T(8,128)(2,1)S(1)}, bf16[128,512]{1,0:T(8,128)(2,1)S(1)}, u32[]{:S(2)}, u32[]{:S(2)}) collective-permute-start(bf16[128,512]{1,0:T(8,128)(2,1)S(1)} %get-tuple-element.37), channel_id=1, source_target_pairs={{0,12},{4,8},{8,4},{12,0},{1,13},{5,9},{9,5},{13,1},{2,14},{6,10},... | collective-permute-start | bytes 393224 | tf_op jit(solution)/shard_map/ppermute | solution.py:186
  21.8 0.0 collective-permute-done.refs_1_
  21.8 8.1 %collective-permute-start.3 = (bf16[256,256]{1,0:T(8,128)(2,1)S(1)}, bf16[256,256]{1,0:T(8,128)(2,1)S(1)}, u32[]{:S(2)}, u32[]{:S(2)}) collective-permute-start(bf16[256,256]{1,0:T(8,128)(2,1)S(1)} %get-tuple-element.42), channel_id=1, source_target_pairs={{0,4},{4,0},{8,12},{12,8},{1,5},{5,1},{9,13},{13,9},{2,6},{6,2},{1... | collective-permute-start | bytes 393224 | tf_op jit(solution)/shard_map/ppermute | solution.py:186
  29.9 0.6 collective-permute-done.1.refs_2_
  30.5 1.3 %collective-permute-start.21 = (bf16[2,256,256]{2,1,0:T(8,128)(2,1)S(1)}, bf16[2,256,256]{2,1,0:T(8,128)(2,1)S(1)}, u32[]{:S(2)}, u32[]{:S(2)}) collective-permute-start(bf16[2,256,256]{2,1,0:T(8,128)(2,1)S(1)} %get-tuple-element.57), channel_id=1, source_target_pairs={{2,0},{3,1},{6,4},{7,5},{10,8},{11,9},{14,12},{15,13},{18,16},{19,... | collective-permute-start | bytes 786440 | tf_op jit(solution)/shard_map/ppermute | solution.py:192
  31.8 0.0 collective-permute-done.2.refs_3_
  31.8 0.7 collective-permute-start.23
  32.5 0.4 collective-permute-done.3.refs_5_
  32.8 2.4 %collective-permute-start.7 = (bf16[2,256,512]{2,1,0:T(8,128)(2,1)S(1)}, bf16[2,256,512]{2,1,0:T(8,128)(2,1)S(1)}, u32[]{:S(2)}, u32[]{:S(2)}) collective-permute-start(bf16[2,256,512]{2,1,0:T(8,128)(2,1)S(1)} %get-tuple-element.45), channel_id=1, source_target_pairs={{0,2},{1,3},{2,0},{3,1},{4,6},{5,7},{6,4},{7,5},{8,10},{9,11},{10,... | collective-permute-start | bytes 1572872 | tf_op jit(solution)/shard_map/ppermute | solution.py:192
  35.2 6.3 %collective-permute-done.21.refs_12_ = bf16[2,256,256]{2,1,0:T(8,128)(2,1)S(1)} collective-permute-done((bf16[2,256,256]{2,1,0:T(8,128)(2,1)S(1)}, bf16[2,256,256]{2,1,0:T(8,128)(2,1)S(1)}, u32[]{:S(2)}, u32[]{:S(2)}) %collective-permute-start.21) | collective-permute-done | bytes 262176 | tf_op jit(solution)/shard_map/ppermute | solution.py:192
  41.5 1.3 %collective-permute-start.9 = (bf16[2,256,256]{2,1,0:T(8,128)(2,1)S(1)}, bf16[2,256,256]{2,1,0:T(8,128)(2,1)S(1)}, u32[]{:S(2)}, u32[]{:S(2)}) collective-permute-start(bf16[2,256,256]{2,1,0:T(8,128)(2,1)S(1)} %get-tuple-element.46), channel_id=1, source_target_pairs={{2,0},{3,1},{6,4},{7,5},{10,8},{11,9},{14,12},{15,13},{18,16},{19,... | collective-permute-start | bytes 786440 | tf_op jit(solution)/shard_map/ppermute | solution.py:192
  42.8 0.0 collective-permute-done.23.refs_14_
  42.8 0.7 collective-permute-start.11
  43.5 0.0 collective-permute-done.19.refs_10_
  43.5 0.4 collective-permute-start.20
  44.0 14.4 %collective-permute-done.9.refs_12_ = bf16[2,256,256]{2,1,0:T(8,128)(2,1)S(1)} collective-permute-done((bf16[2,256,256]{2,1,0:T(8,128)(2,1)S(1)}, bf16[2,256,256]{2,1,0:T(8,128)(2,1)S(1)}, u32[]{:S(2)}, u32[]{:S(2)}) %collective-permute-start.9) | collective-permute-done | bytes 262176 | tf_op jit(solution)/shard_map/ppermute | solution.py:192
  58.4 0.3 collective-permute-start.22
  58.7 0.0 collective-permute-done.11.refs_14_
  58.7 2.8 %collective-permute-start.24 = (bf16[2,256,256]{2,1,0:T(8,128)(2,1)S(1)}, bf16[2,256,256]{2,1,0:T(8,128)(2,1)S(1)}, u32[]{:S(2)}, u32[]{:S(2)}) collective-permute-start(bf16[2,256,256]{2,1,0:T(8,128)(2,1)S(1)} %collective-permute-done.23.refs_14_), channel_id=1, source_target_pairs={{0,1},{1,0},{2,3},{3,2},{4,5},{5,4},{6,7},{7,6},{8,9},{9,8},{10,11... | collective-permute-start | bytes 786440 | tf_op jit(solution)/shard_map/ppermute | solution.py:194
  61.5 0.0 collective-permute-done.7.refs_10_
  61.5 0.0 collective-permute-start.8
  61.5 0.0 collective-permute-done.22.refs_13_
  61.5 0.5 collective-permute-start.10
  62.0 0.6 collective-permute-done.24.refs_15_
  62.7 0.4 collective-permute-start.12
  63.0 0.0 collective-permute-done.20.refs_11_
  63.0 0.0 collective-permute-start.4
  63.0 0.0 collective-permute-done.6.refs_9_
  63.1 2.6 %collective-permute-start.5 = (bf16[256,256]{1,0:T(8,128)(2,1)S(1)}, bf16[256,256]{1,0:T(8,128)(2,1)S(1)}, u32[]{:S(2)}, u32[]{:S(2)}) collective-permute-start(bf16[256,256]{1,0:T(8,128)(2,1)S(1)} %get-tuple-element.44), channel_id=1, source_target_pairs={{0,12},{4,8},{8,4},{12,0},{1,13},{5,9},{9,5},{13,1},{2,14},{6,10},... | collective-permute-start | bytes 393224 | tf_op jit(solution)/shard_map/ppermute | solution.py:186
  65.7 1.7 %shard_map.65 = (bf16[384,256]{1,0:T(8,128)(2,1)S(1)}, bf16[384,256]{1,0:T(8,128)(2,1)S(1)}, bf16[384,256]{1,0:T(8,128)(2,1)S(1)}, bf16[384,256]{1,0:T(8,128)(2,1)S(1)}) custom-call(bf16[128,512]{1,0:T(8,128)(2,1)S(1)} %get-tuple-element.34.refs_0_, bf16[128,512]{1,0:T(8,128)(2,1)S(1)} %collective-permute-done.refs_1_, ...), custom_call_target="tpu_custom_call" | custom-call | flops 805306368 | bytes 2097152 | tf_op jit(solution)/shard_map/pallas_call | solution.py:279
  67.3 7.7 %collective-permute-done.4.refs_6_ = bf16[256,256]{1,0:T(8,128)(2,1)S(1)} collective-permute-done((bf16[256,256]{1,0:T(8,128)(2,1)S(1)}, bf16[256,256]{1,0:T(8,128)(2,1)S(1)}, u32[]{:S(2)}, u32[]{:S(2)}) %collective-permute-start.4) | collective-permute-done | bytes 131104 | tf_op jit(solution)/shard_map/ppermute | solution.py:186
  75.1 0.0 collective-permute-start.25
  75.1 0.0 collective-permute-done.5.refs_7_
  75.1 3.1 %collective-permute-start.26 = (bf16[384,256]{1,0:T(8,128)(2,1)S(1)}, bf16[384,256]{1,0:T(8,128)(2,1)S(1)}, u32[]{:S(2)}, u32[]{:S(2)}) collective-permute-start(bf16[384,256]{1,0:T(8,128)(2,1)S(1)} %get-tuple-element.61), channel_id=1, source_target_pairs={{0,8},{4,12},{8,0},{12,4},{1,9},{5,13},{9,1},{13,5},{2,10},{6,14},... | collective-permute-start | bytes 589832 | tf_op jit(solution)/shard_map/ppermute | solution.py:186
  78.2 0.0 collective-permute-done.10.refs_13_
  78.2 2.5 %collective-permute-start.27 = (bf16[384,256]{1,0:T(8,128)(2,1)S(1)}, bf16[384,256]{1,0:T(8,128)(2,1)S(1)}, u32[]{:S(2)}, u32[]{:S(2)}) collective-permute-start(bf16[384,256]{1,0:T(8,128)(2,1)S(1)} %get-tuple-element.62), channel_id=1, source_target_pairs={{0,12},{4,8},{8,4},{12,0},{1,13},{5,9},{9,5},{13,1},{2,14},{6,10},... | collective-permute-start | bytes 589832 | tf_op jit(solution)/shard_map/ppermute | solution.py:186
  80.7 0.0 collective-permute-done.12.refs_15_
  80.7 0.0 collective-permute-done.8.refs_11_
  80.7 1.7 %shard_map.64 = (bf16[384,256]{1,0:T(8,128)(2,1)S(1)}, bf16[384,256]{1,0:T(8,128)(2,1)S(1)}, bf16[384,256]{1,0:T(8,128)(2,1)S(1)}, bf16[384,256]{1,0:T(8,128)(2,1)S(1)}) custom-call(bf16[128,512]{1,0:T(8,128)(2,1)S(1)} %get-tuple-element.34.refs_0_, bf16[128,512]{1,0:T(8,128)(2,1)S(1)} %collective-permute-done.refs_1_, ...), custom_call_target="tpu_custom_call" | custom-call | flops 805306368 | bytes 2097152 | tf_op jit(solution)/shard_map/pallas_call | solution.py:279
  82.5 0.1 collective-permute-start.14
  82.5 1.8 %collective-permute-start.15 = (bf16[384,256]{1,0:T(8,128)(2,1)S(1)}, bf16[384,256]{1,0:T(8,128)(2,1)S(1)}, u32[]{:S(2)}, u32[]{:S(2)}) collective-permute-start(bf16[384,256]{1,0:T(8,128)(2,1)S(1)} %get-tuple-element.51), channel_id=1, source_target_pairs={{0,8},{4,12},{8,0},{12,4},{1,9},{5,13},{9,1},{13,5},{2,10},{6,14},... | collective-permute-start | bytes 589832 | tf_op jit(solution)/shard_map/ppermute | solution.py:186
  84.4 0.0 collective-permute-done.25.refs_1_
  84.4 2.5 %collective-permute-start.13 = (bf16[384,256]{1,0:T(8,128)(2,1)S(1)}, bf16[384,256]{1,0:T(8,128)(2,1)S(1)}, u32[]{:S(2)}, u32[]{:S(2)}) collective-permute-start(bf16[384,256]{1,0:T(8,128)(2,1)S(1)} %get-tuple-element.48), channel_id=1, source_target_pairs={{0,12},{4,8},{8,4},{12,0},{1,13},{5,9},{9,5},{13,1},{2,14},{6,10},... | collective-permute-start | bytes 589832 | tf_op jit(solution)/shard_map/ppermute | solution.py:186
  86.9 5.6 %collective-permute-done.26.refs_2_ = bf16[384,256]{1,0:T(8,128)(2,1)S(1)} collective-permute-done((bf16[384,256]{1,0:T(8,128)(2,1)S(1)}, bf16[384,256]{1,0:T(8,128)(2,1)S(1)}, u32[]{:S(2)}, u32[]{:S(2)}) %collective-permute-start.26) | collective-permute-done | bytes 196640 | tf_op jit(solution)/shard_map/ppermute | solution.py:186
  92.5 1.3 %shard_map.66.refs_3_ = bf16[384,2048]{1,0:T(8,128)(2,1)} custom-call(bf16[384,2048]{1,0:T(8,128)(2,1)S(1)} %bitcast.3, bf16[384,256]{1,0:T(8,128)(2,1)S(1)} %get-tuple-element.59.refs_0_, bf16[384,256]{1,0:T(8,128)(2,1)S(1)} %collective-permute-done.25.refs_1_, bf16[384,256]{1,0:T(8,128)(2,1)S(1)} %collective-permute-done.26.refs_2_, ...), custom_call_target="tpu_custom_call" | custom-call | flops 4718592 | bytes 2359296 | tf_op jit(solution)/shard_map/pallas_call | solution.py:299
  93.8 1.1 collective-permute-done.14.refs_1_
  94.9 14.4 %collective-permute-done.15.refs_2_ = bf16[384,256]{1,0:T(8,128)(2,1)S(1)} collective-permute-done((bf16[384,256]{1,0:T(8,128)(2,1)S(1)}, bf16[384,256]{1,0:T(8,128)(2,1)S(1)}, u32[]{:S(2)}, u32[]{:S(2)}) %collective-permute-start.15) | collective-permute-done | bytes 196640 | tf_op jit(solution)/shard_map/ppermute | solution.py:186
  109.3 1.2 %shard_map.67.refs_1_ = bf16[384,2048]{1,0:T(8,128)(2,1)} custom-call(bf16[384,2048]{1,0:T(8,128)(2,1)S(1)} %bitcast.4, bf16[384,256]{1,0:T(8,128)(2,1)S(1)} %get-tuple-element.49.refs_0_, bf16[384,256]{1,0:T(8,128)(2,1)S(1)} %collective-permute-done.14.refs_1_, ...), custom_call_target="tpu_custom_call", output_to_operand_aliasing={{}: (4, {})} | custom-call | flops 3538944 | bytes 1769472 | tf_op jit(solution)/shard_map/pallas_call | solution.py:299
  110.5 0.0 collective-permute-done.13.refs_0_
  110.5 0.8 shard_map.68
  (5 shorter events, 0.0 us)
Async XLA Ops:
  0.0 63.0 %collective-permute-start.6 = (bf16[4,256,1024]{2,1,0:T(8,128)(2,1)}, bf16[4,256,1024]{2,1,0:T(8,128)(2,1)S(1)}, u32[]{:S(2)}, u32[]{:S(2)}) collective-permute-start(bf16[4,256,1024]{2,1,0:T(8,128)(2,1)} %refs_8_.3), channel_id=1, source_target_pairs={{0,1},{1,0},{2,3},{3,2},{4,5},{5,4},{6,7},{7,6},{8,9},{9,8},{10,11... | collective-permute-start | bytes 6291464 | tf_op jit(solution)/shard_map/ppermute | solution.py:262
  2.3 63.4 %copy-start = (bf16[4,256,1024]{2,1,0:T(8,128)(2,1)S(1)}, bf16[4,256,1024]{2,1,0:T(8,128)(2,1)}, u32[]{:S(2)}) copy-start(bf16[4,256,1024]{2,1,0:T(8,128)(2,1)} %refs_8_.3) | copy-start | bytes 6291460
  2.3 63.4 %copy-start.2 = (bf16[4,1024]{1,0:T(4,128)(2,1)S(1)}, bf16[4,1024]{1,0:T(4,128)(2,1)}, u32[]{:S(2)}) copy-start(bf16[4,1024]{1,0:T(4,128)(2,1)} %refs_16_.3) | copy-start | bytes 24580
  3.7 9.3 %collective-permute-start.16 = (bf16[256,256]{1,0:T(8,128)(2,1)S(1)}, bf16[256,256]{1,0:T(8,128)(2,1)S(1)}, u32[]{:S(2)}, u32[]{:S(2)}) collective-permute-start(bf16[256,256]{1,0:T(8,128)(2,1)S(1)} %get-tuple-element.53), channel_id=1, source_target_pairs={{0,4},{4,0},{8,12},{12,8},{1,5},{5,1},{9,13},{13,9},{2,6},{6,2},{1... | collective-permute-start | bytes 393224 | tf_op jit(solution)/shard_map/ppermute | solution.py:186
  6.3 13.0 %collective-permute-start.17 = (bf16[256,256]{1,0:T(8,128)(2,1)S(1)}, bf16[256,256]{1,0:T(8,128)(2,1)S(1)}, u32[]{:S(2)}, u32[]{:S(2)}) collective-permute-start(bf16[256,256]{1,0:T(8,128)(2,1)S(1)} %get-tuple-element.54), channel_id=1, source_target_pairs={{0,8},{4,12},{8,0},{12,4},{1,9},{5,13},{9,1},{13,5},{2,10},{6,14},... | collective-permute-start | bytes 393224 | tf_op jit(solution)/shard_map/ppermute | solution.py:186
  8.9 10.4 %collective-permute-start.18 = (bf16[256,256]{1,0:T(8,128)(2,1)S(1)}, bf16[256,256]{1,0:T(8,128)(2,1)S(1)}, u32[]{:S(2)}, u32[]{:S(2)}) collective-permute-start(bf16[256,256]{1,0:T(8,128)(2,1)S(1)} %get-tuple-element.55), channel_id=1, source_target_pairs={{0,12},{4,8},{8,4},{12,0},{1,13},{5,9},{9,5},{13,1},{2,14},{6,10},... | collective-permute-start | bytes 393224 | tf_op jit(solution)/shard_map/ppermute | solution.py:186
  8.9 12.9 %collective-permute-start = (bf16[128,512]{1,0:T(8,128)(2,1)S(1)}, bf16[128,512]{1,0:T(8,128)(2,1)S(1)}, u32[]{:S(2)}, u32[]{:S(2)}) collective-permute-start(bf16[128,512]{1,0:T(8,128)(2,1)S(1)} %get-tuple-element.35), channel_id=1, source_target_pairs={{0,4},{4,0},{8,12},{12,8},{1,5},{5,1},{9,13},{13,9},{2,6},{6,2},{1... | collective-permute-start | bytes 393224 | tf_op jit(solution)/shard_map/ppermute | solution.py:186
  12.9 30.6 %collective-permute-start.19 = (bf16[2,256,512]{2,1,0:T(8,128)(2,1)S(1)}, bf16[2,256,512]{2,1,0:T(8,128)(2,1)S(1)}, u32[]{:S(2)}, u32[]{:S(2)}) collective-permute-start(bf16[2,256,512]{2,1,0:T(8,128)(2,1)S(1)} %get-tuple-element.56), channel_id=1, source_target_pairs={{0,2},{1,3},{2,0},{3,1},{4,6},{5,7},{6,4},{7,5},{8,10},{9,11},{10,... | collective-permute-start | bytes 1572872 | tf_op jit(solution)/shard_map/ppermute | solution.py:192
  19.3 11.2 %collective-permute-start.1 = (bf16[128,512]{1,0:T(8,128)(2,1)S(1)}, bf16[128,512]{1,0:T(8,128)(2,1)S(1)}, u32[]{:S(2)}, u32[]{:S(2)}) collective-permute-start(bf16[128,512]{1,0:T(8,128)(2,1)S(1)} %get-tuple-element.36), channel_id=1, source_target_pairs={{0,8},{4,12},{8,0},{12,4},{1,9},{5,13},{9,1},{13,5},{2,10},{6,14},... | collective-permute-start | bytes 393224 | tf_op jit(solution)/shard_map/ppermute | solution.py:186
  19.3 12.5 %collective-permute-start.2 = (bf16[128,512]{1,0:T(8,128)(2,1)S(1)}, bf16[128,512]{1,0:T(8,128)(2,1)S(1)}, u32[]{:S(2)}, u32[]{:S(2)}) collective-permute-start(bf16[128,512]{1,0:T(8,128)(2,1)S(1)} %get-tuple-element.37), channel_id=1, source_target_pairs={{0,12},{4,8},{8,4},{12,0},{1,13},{5,9},{9,5},{13,1},{2,14},{6,10},... | collective-permute-start | bytes 393224 | tf_op jit(solution)/shard_map/ppermute | solution.py:186
  21.8 11.1 %collective-permute-start.3 = (bf16[256,256]{1,0:T(8,128)(2,1)S(1)}, bf16[256,256]{1,0:T(8,128)(2,1)S(1)}, u32[]{:S(2)}, u32[]{:S(2)}) collective-permute-start(bf16[256,256]{1,0:T(8,128)(2,1)S(1)} %get-tuple-element.42), channel_id=1, source_target_pairs={{0,4},{4,0},{8,12},{12,8},{1,5},{5,1},{9,13},{13,9},{2,6},{6,2},{1... | collective-permute-start | bytes 393224 | tf_op jit(solution)/shard_map/ppermute | solution.py:186
  30.5 11.1 %collective-permute-start.21 = (bf16[2,256,256]{2,1,0:T(8,128)(2,1)S(1)}, bf16[2,256,256]{2,1,0:T(8,128)(2,1)S(1)}, u32[]{:S(2)}, u32[]{:S(2)}) collective-permute-start(bf16[2,256,256]{2,1,0:T(8,128)(2,1)S(1)} %get-tuple-element.57), channel_id=1, source_target_pairs={{2,0},{3,1},{6,4},{7,5},{10,8},{11,9},{14,12},{15,13},{18,16},{19,... | collective-permute-start | bytes 786440 | tf_op jit(solution)/shard_map/ppermute | solution.py:192
  31.8 11.1 %collective-permute-start.23 = (bf16[2,256,256]{2,1,0:T(8,128)(2,1)S(1)}, bf16[2,256,256]{2,1,0:T(8,128)(2,1)S(1)}, u32[]{:S(2)}, u32[]{:S(2)}) collective-permute-start(bf16[2,256,256]{2,1,0:T(8,128)(2,1)S(1)} %get-tuple-element.58), channel_id=1, source_target_pairs={{3,1},{7,5},{11,9},{15,13},{19,17},{23,21},{27,25},{31,29}} | collective-permute-start | bytes 786440 | tf_op jit(solution)/shard_map/ppermute | solution.py:192
  32.8 28.7 %collective-permute-start.7 = (bf16[2,256,512]{2,1,0:T(8,128)(2,1)S(1)}, bf16[2,256,512]{2,1,0:T(8,128)(2,1)S(1)}, u32[]{:S(2)}, u32[]{:S(2)}) collective-permute-start(bf16[2,256,512]{2,1,0:T(8,128)(2,1)S(1)} %get-tuple-element.45), channel_id=1, source_target_pairs={{0,2},{1,3},{2,0},{3,1},{4,6},{5,7},{6,4},{7,5},{8,10},{9,11},{10,... | collective-permute-start | bytes 1572872 | tf_op jit(solution)/shard_map/ppermute | solution.py:192
  41.5 16.9 %collective-permute-start.9 = (bf16[2,256,256]{2,1,0:T(8,128)(2,1)S(1)}, bf16[2,256,256]{2,1,0:T(8,128)(2,1)S(1)}, u32[]{:S(2)}, u32[]{:S(2)}) collective-permute-start(bf16[2,256,256]{2,1,0:T(8,128)(2,1)S(1)} %get-tuple-element.46), channel_id=1, source_target_pairs={{2,0},{3,1},{6,4},{7,5},{10,8},{11,9},{14,12},{15,13},{18,16},{19,... | collective-permute-start | bytes 786440 | tf_op jit(solution)/shard_map/ppermute | solution.py:192
  42.8 15.8 %collective-permute-start.11 = (bf16[2,256,256]{2,1,0:T(8,128)(2,1)S(1)}, bf16[2,256,256]{2,1,0:T(8,128)(2,1)S(1)}, u32[]{:S(2)}, u32[]{:S(2)}) collective-permute-start(bf16[2,256,256]{2,1,0:T(8,128)(2,1)S(1)} %get-tuple-element.47), channel_id=1, source_target_pairs={{3,1},{7,5},{11,9},{15,13},{19,17},{23,21},{27,25},{31,29}} | collective-permute-start | bytes 786440 | tf_op jit(solution)/shard_map/ppermute | solution.py:192
  43.5 19.5 %collective-permute-start.20 = (bf16[2,256,512]{2,1,0:T(8,128)(2,1)S(1)}, bf16[2,256,512]{2,1,0:T(8,128)(2,1)S(1)}, u32[]{:S(2)}, u32[]{:S(2)}) collective-permute-start(bf16[2,256,512]{2,1,0:T(8,128)(2,1)S(1)} %collective-permute-done.19.refs_10_), channel_id=1, source_target_pairs={{0,1},{1,0},{2,3},{3,2},{4,5},{5,4},{6,7},{7,6},{8,9},{9,8},{10,11... | collective-permute-start | bytes 1572872 | tf_op jit(solution)/shard_map/ppermute | solution.py:194
  58.4 3.1 %collective-permute-start.22 = (bf16[2,256,256]{2,1,0:T(8,128)(2,1)S(1)}, bf16[2,256,256]{2,1,0:T(8,128)(2,1)S(1)}, u32[]{:S(2)}, u32[]{:S(2)}) collective-permute-start(bf16[2,256,256]{2,1,0:T(8,128)(2,1)S(1)} %collective-permute-done.21.refs_12_), channel_id=1, source_target_pairs={{0,1},{1,0},{2,3},{3,2},{4,5},{5,4},{6,7},{7,6},{8,9},{9,8},{10,11... | collective-permute-start | bytes 786440 | tf_op jit(solution)/shard_map/ppermute | solution.py:194
  58.7 4.0 %collective-permute-start.24 = (bf16[2,256,256]{2,1,0:T(8,128)(2,1)S(1)}, bf16[2,256,256]{2,1,0:T(8,128)(2,1)S(1)}, u32[]{:S(2)}, u32[]{:S(2)}) collective-permute-start(bf16[2,256,256]{2,1,0:T(8,128)(2,1)S(1)} %collective-permute-done.23.refs_14_), channel_id=1, source_target_pairs={{0,1},{1,0},{2,3},{3,2},{4,5},{5,4},{6,7},{7,6},{8,9},{9,8},{10,11... | collective-permute-start | bytes 786440 | tf_op jit(solution)/shard_map/ppermute | solution.py:194
  61.5 19.2 %collective-permute-start.8 = (bf16[2,256,512]{2,1,0:T(8,128)(2,1)S(1)}, bf16[2,256,512]{2,1,0:T(8,128)(2,1)S(1)}, u32[]{:S(2)}, u32[]{:S(2)}) collective-permute-start(bf16[2,256,512]{2,1,0:T(8,128)(2,1)S(1)} %collective-permute-done.7.refs_10_), channel_id=1, source_target_pairs={{0,1},{1,0},{2,3},{3,2},{4,5},{5,4},{6,7},{7,6},{8,9},{9,8},{10,11... | collective-permute-start | bytes 1572872 | tf_op jit(solution)/shard_map/ppermute | solution.py:194
  61.5 16.7 %collective-permute-start.10 = (bf16[2,256,256]{2,1,0:T(8,128)(2,1)S(1)}, bf16[2,256,256]{2,1,0:T(8,128)(2,1)S(1)}, u32[]{:S(2)}, u32[]{:S(2)}) collective-permute-start(bf16[2,256,256]{2,1,0:T(8,128)(2,1)S(1)} %collective-permute-done.9.refs_12_), channel_id=1, source_target_pairs={{0,1},{1,0},{2,3},{3,2},{4,5},{5,4},{6,7},{7,6},{8,9},{9,8},{10,11... | collective-permute-start | bytes 786440 | tf_op jit(solution)/shard_map/ppermute | solution.py:194
  62.7 18.1 %collective-permute-start.12 = (bf16[2,256,256]{2,1,0:T(8,128)(2,1)S(1)}, bf16[2,256,256]{2,1,0:T(8,128)(2,1)S(1)}, u32[]{:S(2)}, u32[]{:S(2)}) collective-permute-start(bf16[2,256,256]{2,1,0:T(8,128)(2,1)S(1)} %collective-permute-done.11.refs_14_), channel_id=1, source_target_pairs={{0,1},{1,0},{2,3},{3,2},{4,5},{5,4},{6,7},{7,6},{8,9},{9,8},{10,11... | collective-permute-start | bytes 786440 | tf_op jit(solution)/shard_map/ppermute | solution.py:194
  63.0 12.0 %collective-permute-start.4 = (bf16[256,256]{1,0:T(8,128)(2,1)S(1)}, bf16[256,256]{1,0:T(8,128)(2,1)S(1)}, u32[]{:S(2)}, u32[]{:S(2)}) collective-permute-start(bf16[256,256]{1,0:T(8,128)(2,1)S(1)} %get-tuple-element.43), channel_id=1, source_target_pairs={{0,8},{4,12},{8,0},{12,4},{1,9},{5,13},{9,1},{13,5},{2,10},{6,14},... | collective-permute-start | bytes 393224 | tf_op jit(solution)/shard_map/ppermute | solution.py:186
  63.1 12.0 %collective-permute-start.5 = (bf16[256,256]{1,0:T(8,128)(2,1)S(1)}, bf16[256,256]{1,0:T(8,128)(2,1)S(1)}, u32[]{:S(2)}, u32[]{:S(2)}) collective-permute-start(bf16[256,256]{1,0:T(8,128)(2,1)S(1)} %get-tuple-element.44), channel_id=1, source_target_pairs={{0,12},{4,8},{8,4},{12,0},{1,13},{5,9},{9,5},{13,1},{2,14},{6,10},... | collective-permute-start | bytes 393224 | tf_op jit(solution)/shard_map/ppermute | solution.py:186
  75.1 9.3 %collective-permute-start.25 = (bf16[384,256]{1,0:T(8,128)(2,1)S(1)}, bf16[384,256]{1,0:T(8,128)(2,1)S(1)}, u32[]{:S(2)}, u32[]{:S(2)}) collective-permute-start(bf16[384,256]{1,0:T(8,128)(2,1)S(1)} %get-tuple-element.60), channel_id=1, source_target_pairs={{0,4},{4,0},{8,12},{12,8},{1,5},{5,1},{9,13},{13,9},{2,6},{6,2},{1... | collective-permute-start | bytes 589832 | tf_op jit(solution)/shard_map/ppermute | solution.py:186
  75.1 17.4 %collective-permute-start.26 = (bf16[384,256]{1,0:T(8,128)(2,1)S(1)}, bf16[384,256]{1,0:T(8,128)(2,1)S(1)}, u32[]{:S(2)}, u32[]{:S(2)}) collective-permute-start(bf16[384,256]{1,0:T(8,128)(2,1)S(1)} %get-tuple-element.61), channel_id=1, source_target_pairs={{0,8},{4,12},{8,0},{12,4},{1,9},{5,13},{9,1},{13,5},{2,10},{6,14},... | collective-permute-start | bytes 589832 | tf_op jit(solution)/shard_map/ppermute | solution.py:186
  78.2 14.3 %collective-permute-start.27 = (bf16[384,256]{1,0:T(8,128)(2,1)S(1)}, bf16[384,256]{1,0:T(8,128)(2,1)S(1)}, u32[]{:S(2)}, u32[]{:S(2)}) collective-permute-start(bf16[384,256]{1,0:T(8,128)(2,1)S(1)} %get-tuple-element.62), channel_id=1, source_target_pairs={{0,12},{4,8},{8,4},{12,0},{1,13},{5,9},{9,5},{13,1},{2,14},{6,10},... | collective-permute-start | bytes 589832 | tf_op jit(solution)/shard_map/ppermute | solution.py:186
  80.7 11.7 %copy-start.1 = (bf16[1,384,2048]{2,1,0:T(8,128)(2,1)S(1)}, bf16[1,384,2048]{2,1,0:T(8,128)(2,1)}, u32[]{:S(2)}) copy-start(bf16[1,384,2048]{2,1,0:T(8,128)(2,1)} %param.6) | copy-start | bytes 4718596
  82.5 12.4 %collective-permute-start.14 = (bf16[384,256]{1,0:T(8,128)(2,1)S(1)}, bf16[384,256]{1,0:T(8,128)(2,1)S(1)}, u32[]{:S(2)}, u32[]{:S(2)}) collective-permute-start(bf16[384,256]{1,0:T(8,128)(2,1)S(1)} %get-tuple-element.50), channel_id=1, source_target_pairs={{0,4},{4,0},{8,12},{12,8},{1,5},{5,1},{9,13},{13,9},{2,6},{6,2},{1... | collective-permute-start | bytes 589832 | tf_op jit(solution)/shard_map/ppermute | solution.py:186
  82.5 26.8 %collective-permute-start.15 = (bf16[384,256]{1,0:T(8,128)(2,1)S(1)}, bf16[384,256]{1,0:T(8,128)(2,1)S(1)}, u32[]{:S(2)}, u32[]{:S(2)}) collective-permute-start(bf16[384,256]{1,0:T(8,128)(2,1)S(1)} %get-tuple-element.51), channel_id=1, source_target_pairs={{0,8},{4,12},{8,0},{12,4},{1,9},{5,13},{9,1},{13,5},{2,10},{6,14},... | collective-permute-start | bytes 589832 | tf_op jit(solution)/shard_map/ppermute | solution.py:186
  84.4 26.1 %collective-permute-start.13 = (bf16[384,256]{1,0:T(8,128)(2,1)S(1)}, bf16[384,256]{1,0:T(8,128)(2,1)S(1)}, u32[]{:S(2)}, u32[]{:S(2)}) collective-permute-start(bf16[384,256]{1,0:T(8,128)(2,1)S(1)} %get-tuple-element.48), channel_id=1, source_target_pairs={{0,12},{4,8},{8,4},{12,0},{1,13},{5,9},{9,5},{13,1},{2,14},{6,10},... | collective-permute-start | bytes 589832 | tf_op jit(solution)/shard_map/ppermute | solution.py:186

commit v5 on v4

--- a/solution.py
+++ b/solution.py
@@ -47,7 +47,7 @@
         return carry
 
     steps = value.shape[0] // rows_step
-    lax.fori_loop(0, steps, step, 0, unroll=next(u for u in (8, 6, 4, 1) if steps % u == 0))
+    lax.fori_loop(0, steps, step, 0, unroll=next(u for u in (8, 9, 7, 6, 5, 4, 3, 2, 1) if steps % u == 0))
 
 
 def hand_out(shards, span, lanes, held, outs):
@@ -67,15 +67,14 @@
 
 def head_kernel(shards, span, rows_step, lanes, cuts, value_ref, gain_ref, bias_ref, weight_ref, *refs):
     outs, parts = refs[:len(lanes)], refs[len(lanes):len(lanes) + len(cuts)]
-    rest, gain, bias, value, held, sems = refs[len(lanes) + len(cuts):]
+    gain, bias, value, held, sems = refs[len(lanes) + len(cuts):]
     head = value.shape[0]
-    half = head // 2
+    half = head // 32 * 16
     pairs = [
         (value_ref.at[pl.ds(0, half), :], value.at[pl.ds(0, half), :]),
         (gain_ref, gain),
         (bias_ref, bias),
         (value_ref.at[pl.ds(half, head - half), :], value.at[pl.ds(half, head - half), :]),
-        (value_ref.at[pl.ds(head, rest.shape[0]), :], rest),
     ]
     copies = [pltpu.make_async_copy(source, target, sems.at[k]) for k, (source, target) in enumerate(pairs)]
     copies += weight_copies(cuts, weight_ref, parts, sems, len(pairs))
@@ -93,17 +92,26 @@
         copy.wait()
 
 
-def rest_kernel(shards, span, rows_step, lanes, cuts, value, gain, bias, weight_ref, *refs):
+def rest_kernel(shards, span, rows_step, first, lanes, cuts, gain, bias, value_ref, weight_ref, *refs):
     outs, parts = refs[:len(lanes)], refs[len(lanes):len(lanes) + len(cuts)]
-    held, sems = refs[len(lanes) + len(cuts):]
-    copies = weight_copies(cuts, weight_ref, parts, sems, 0)
+    value, held, sems = refs[len(lanes) + len(cuts):]
+    half = value.shape[0] // 32 * 16
+    blocks = [pl.ds(0, half), pl.ds(half, value.shape[0] - half)]
+    starts = [first, first + half]
+    copies = [
+        pltpu.make_async_copy(value_ref.at[pl.ds(start, at.size), :], value.at[at, :], sems.at[k])
+        for k, (start, at) in enumerate(zip(starts, blocks))
+    ]
+    copies += weight_copies(cuts, weight_ref, parts, sems, len(copies))
     for copy in copies:
         copy.start()
     scale = gain[...].astype(jnp.float32).reshape(1, -1)
     offset = bias[...].astype(jnp.float32).reshape(1, -1)
-    normalise(value, held, scale, offset, rows_step)
+    for copy, at in zip(copies, blocks):
+        copy.wait()
+        normalise(value.at[at, :], held.at[at, :], scale, offset, rows_step)
     hand_out(shards, span, lanes, held, outs)
-    for copy in copies:
+    for copy in copies[len(blocks):]:
         copy.wait()
 
 
@@ -207,10 +215,10 @@
 
     columns = [(0, 2 * TILE, 0), (2 * TILE, TILE, 2), (3 * TILE, TILE, 3)] if exchange else []
     cuts = [(c * per, per, low, cols) for c in range(chunks) for low, cols, _ in columns]
-    head = rows // 3
+    head = rows // 4
     span = groups * GD
 
-    ncuts = len(cuts) // 2
+    ncuts = min(1, len(cuts))
 
     def bf16(*shape):
         return jax.ShapeDtypeStruct(shape, jnp.bfloat16)
@@ -223,7 +231,7 @@
 
     in_hbm = [pltpu.with_memory_space_constraint(x, pltpu.HBM) for x in (value, gain, bias, mix_weight)]
     lanes = [(s, 0, span) for s in range(nsp)]
-    shapes = [bf16(head, span)] * nsp + cut_shapes(cuts[:ncuts]) + [bf16(rows - head, width), bf16(width), bf16(width)]
+    shapes = [bf16(head, span)] * nsp + cut_shapes(cuts[:ncuts]) + [bf16(width), bf16(width)]
     made = pl.pallas_call(
         functools.partial(head_kernel, nsp, span, 16, lanes, cuts[:ncuts]),
         out_shape=shapes,
@@ -232,7 +240,7 @@
         scratch_shapes=[
             pltpu.VMEM((head, width), jnp.bfloat16),
             pltpu.VMEM((head, width), jnp.bfloat16),
-            pltpu.SemaphoreType.DMA((5 + ncuts,)),
+            pltpu.SemaphoreType.DMA((4 + ncuts,)),
         ],
         compiler_params=small,
         cost_estimate=cost(head),
@@ -244,18 +252,19 @@
     lanes = [(s, c * per * GD, per * GD) for c in range(chunks) for s in range(nsp)]
     shapes = [bf16(rows - head, per * GD)] * (nsp * chunks) + cut_shapes(cuts[ncuts:])
     made = pl.pallas_call(
-        functools.partial(rest_kernel, nsp, span, 16, lanes, cuts[ncuts:]),
+        functools.partial(rest_kernel, nsp, span, 16, head, lanes, cuts[ncuts:]),
         out_shape=shapes,
-        in_specs=[VMEM] * 3 + [HBM],
+        in_specs=[VMEM] * 2 + [HBM] * 2,
         out_specs=[VMEM] * len(shapes),
         scratch_shapes=[
             pltpu.VMEM((rows - head, width), jnp.bfloat16),
-            pltpu.SemaphoreType.DMA((max(1, ncuts),)),
+            pltpu.VMEM((rows - head, width), jnp.bfloat16),
+            pltpu.SemaphoreType.DMA((2 + len(cuts) - ncuts,)),
         ],
         compiler_params=small,
         cost_estimate=cost(rows - head),
         name="norm_rest",
-    )(*ready, in_hbm[3])
+    )(*ready, in_hbm[0], in_hbm[3])
     sent, parts = made[:nsp * chunks], list(parts) + list(made[nsp * chunks:])
     weights = []
     if exchange:

time: 112 us -> 112 us (level)
  waiting for transfers between devices: 58.7 us -> 51.5 us
  starting transfers between devices: 42.7 us -> 49.4 us
  Pallas kernels: 9.82 us -> 11.1 us
    ppermute x15, starting transfers between devices: 29.4 us -> 36.1 us  [exchange_step(): return lax.ppermute(x, 'sp', swap_pairs(shards, step))]
    ppermute x6, waiting for transfers between devices: 20.8 us -> 17.2 us  [exchange_rows(): lax.ppermute(part, 'dp', [p for p in swap_pairs(ndp, 2) if p[0] >= least])]
    ppermute x15, waiting for transfers between devices: 37.2 us -> 34.2 us  [exchange_step(): return lax.ppermute(x, 'sp', swap_pairs(shards, step))]
    ppermute x6, starting transfers between devices: 4.4 us -> 6.03 us  [exchange_rows(): got.append((lax.ppermute(far, 'dp', swap_pairs(ndp, 1)), 3, None, low, 0))]
    ppermute x6, starting transfers between devices: 8.32 us -> 6.73 us  [exchange_rows(): lax.ppermute(part, 'dp', [p for p in swap_pairs(ndp, 2) if p[0] >= least])]
    pallas_call x1, Pallas kernels: 1.37 us -> 2.74 us  [compute(): pl.pallas_call(functools.partial(rest_kernel, nsp, span, 16, head, lanes,...]
  transfers between devices with their start and end apart: 28 -> 28, of which waited for: 11 -> 8; matrix products, arithmetic and copies ran while one was open for 0% -> 0% of each run, Pallas kernels for 8% -> 9%
where the time goes in v5:
time: 112 us
  waiting for transfers between devices  51.5 us (46%)
  starting transfers between devices  49.4 us (44%)
  Pallas kernels  11.1 us (10%)
    ppermute x15, starting transfers between devices, exchange_step(): return lax.ppermute(x, 'sp', swap_pairs(shards, step))  36.1 us
    ppermute x15, waiting for transfers between devices, exchange_step(): return lax.ppermute(x, 'sp', swap_pairs(shards, step))  34.2 us
    ppermute x6, waiting for transfers between devices, exchange_rows(): lax.ppermute(part, 'dp', [p for p in swap_pairs(ndp, 2) if p[0] >= least])  17.2 us
    ppermute x6, starting transfers between devices, exchange_rows(): lax.ppermute(part, 'dp', [p for p in swap_pairs(ndp, 2) if p[0] >= least])  6.73 us
    ppermute x6, starting transfers between devices, exchange_rows(): got.append((lax.ppermute(far, 'dp', swap_pairs(ndp, 1)), 3, None, low, 0))  6.03 us
    pallas_call x2, Pallas kernels, compute(): pl.pallas_call(functools.partial(mix_kernel, nsp, length, c * per, c * pe...  3.4 us
    pallas_call x3, Pallas kernels, compute(): pl.pallas_call(functools.partial(gate_kernel, nsp, chunks, c, steps, 32),...  3.31 us
    pallas_call x1, Pallas kernels, compute(): pl.pallas_call(functools.partial(rest_kernel, nsp, span, 16, head, lanes,...  2.74 us
  transfers between devices with their start and end apart: 28, of which 8 were waited for; matrix products, arithmetic and copies ran while one was open for 0% of the time, Pallas kernels for 9%

profile of v5, /device:TPU:0, one launch (start us, length us, event | category | flops | bytes accessed | tf_op | source)
XLA Modules:
  0.0 112.1 jit_solution(3580920402036602864)
XLA Ops:
  0.0 0.5 collective-permute-start.6
  0.5 1.6 %norm_head.1 = (bf16[96,512]{1,0:T(8,128)(2,1)S(1)}, bf16[96,512]{1,0:T(8,128)(2,1)S(1)}, bf16[96,512]{1,0:T(8,128)(2,1)S(1)}, bf16[96,512]{1,0:T(8,128)(2,1)S(1...) custom-call(bf16[384,2048]{1,0:T(8,128)(2,1)} %bitcast.6, ...), custom_call_target="tpu_custom_call" | custom-call | flops 5898240 | bytes 786432 | tf_op jit(solution)/shard_map/norm_head/pallas_call | solution.py:235
  2.1 2.6 %collective-permute-start = (bf16[96,512]{1,0:T(8,128)(2,1)S(1)}, bf16[96,512]{1,0:T(8,128)(2,1)S(1)}, u32[]{:S(2)}, u32[]{:S(2)}) collective-permute-start(bf16[96,512]{1,0:T(8,128)(2,1)S(1)} %get-tuple-element.34), channel_id=1, source_target_pairs={{0,4},{4,0},{8,12},{12,8},{1,5},{5,1},{9,13},{13,9},{2,6},{6,2},{1... | collective-permute-start | bytes 294920 | tf_op jit(solution)/shard_map/ppermute | solution.py:194
  4.8 2.7 %norm_rest.1 = (bf16[288,256]{1,0:T(8,128)(2,1)S(1)}, bf16[288,256]{1,0:T(8,128)(2,1)S(1)}, bf16[288,256]{1,0:T(8,128)(2,1)S(1)}, bf16[288,256]{1,0:T(8,128)(2,1...) custom-call(bf16[2048]{0:T(1024)(128)(2,1)S(1)} %get-tuple-element.3, ...), custom_call_target="tpu_custom_call" | custom-call | flops 17694720 | bytes 2359296 | tf_op jit(solution)/shard_map/norm_rest/pallas_call | solution.py:254
  7.5 0.1 collective-permute-start.16
  7.6 1.9 %collective-permute-start.19 = (bf16[2,256,512]{2,1,0:T(8,128)(2,1)S(1)}, bf16[2,256,512]{2,1,0:T(8,128)(2,1)S(1)}, u32[]{:S(2)}, u32[]{:S(2)}) collective-permute-start(bf16[2,256,512]{2,1,0:T(8,128)(2,1)S(1)} %get-tuple-element.54), channel_id=1, source_target_pairs={{0,2},{1,3},{2,0},{3,1},{4,6},{5,7},{6,4},{7,5},{8,10},{9,11},{10,... | collective-permute-start | bytes 1572872 | tf_op jit(solution)/shard_map/ppermute | solution.py:200
  9.5 2.6 %collective-permute-start.1 = (bf16[96,512]{1,0:T(8,128)(2,1)S(1)}, bf16[96,512]{1,0:T(8,128)(2,1)S(1)}, u32[]{:S(2)}, u32[]{:S(2)}) collective-permute-start(bf16[96,512]{1,0:T(8,128)(2,1)S(1)} %get-tuple-element.35), channel_id=1, source_target_pairs={{0,8},{4,12},{8,0},{12,4},{1,9},{5,13},{9,1},{13,5},{2,10},{6,14},... | collective-permute-start | bytes 294920 | tf_op jit(solution)/shard_map/ppermute | solution.py:194
  12.1 0.0 collective-permute-done.refs_1_
  12.1 1.3 %collective-permute-start.2 = (bf16[96,512]{1,0:T(8,128)(2,1)S(1)}, bf16[96,512]{1,0:T(8,128)(2,1)S(1)}, u32[]{:S(2)}, u32[]{:S(2)}) collective-permute-start(bf16[96,512]{1,0:T(8,128)(2,1)S(1)} %get-tuple-element.36), channel_id=1, source_target_pairs={{0,12},{4,8},{8,4},{12,0},{1,13},{5,9},{9,5},{13,1},{2,14},{6,10},... | collective-permute-start | bytes 294920 | tf_op jit(solution)/shard_map/ppermute | solution.py:194
  13.5 1.9 %collective-permute-done.1.refs_2_ = bf16[96,512]{1,0:T(8,128)(2,1)S(1)} collective-permute-done((bf16[96,512]{1,0:T(8,128)(2,1)S(1)}, bf16[96,512]{1,0:T(8,128)(2,1)S(1)}, u32[]{:S(2)}, u32[]{:S(2)}) %collective-permute-start.1) | collective-permute-done | bytes 98336 | tf_op jit(solution)/shard_map/ppermute | solution.py:194
  15.3 3.2 %collective-permute-start.17 = (bf16[288,256]{1,0:T(8,128)(2,1)S(1)}, bf16[288,256]{1,0:T(8,128)(2,1)S(1)}, u32[]{:S(2)}, u32[]{:S(2)}) collective-permute-start(bf16[288,256]{1,0:T(8,128)(2,1)S(1)} %get-tuple-element.52), channel_id=1, source_target_pairs={{0,8},{4,12},{8,0},{12,4},{1,9},{5,13},{9,1},{13,5},{2,10},{6,14},... | collective-permute-start | bytes 442376 | tf_op jit(solution)/shard_map/ppermute | solution.py:194
  18.5 1.4 %collective-permute-done.2.refs_3_ = bf16[96,512]{1,0:T(8,128)(2,1)S(1)} collective-permute-done((bf16[96,512]{1,0:T(8,128)(2,1)S(1)}, bf16[96,512]{1,0:T(8,128)(2,1)S(1)}, u32[]{:S(2)}, u32[]{:S(2)}) %collective-permute-start.2) | collective-permute-done | bytes 98336 | tf_op jit(solution)/shard_map/ppermute | solution.py:194
  19.9 5.9 %collective-permute-start.18 = (bf16[288,256]{1,0:T(8,128)(2,1)S(1)}, bf16[288,256]{1,0:T(8,128)(2,1)S(1)}, u32[]{:S(2)}, u32[]{:S(2)}) collective-permute-start(bf16[288,256]{1,0:T(8,128)(2,1)S(1)} %get-tuple-element.53), channel_id=1, source_target_pairs={{0,12},{4,8},{8,4},{12,0},{1,13},{5,9},{9,5},{13,1},{2,14},{6,10},... | collective-permute-start | bytes 442376 | tf_op jit(solution)/shard_map/ppermute | solution.py:194
  25.7 0.0 collective-permute-done.16.refs_5_
  25.8 1.8 %collective-permute-start.3 = (bf16[288,256]{1,0:T(8,128)(2,1)S(1)}, bf16[288,256]{1,0:T(8,128)(2,1)S(1)}, u32[]{:S(2)}, u32[]{:S(2)}) collective-permute-start(bf16[288,256]{1,0:T(8,128)(2,1)S(1)} %get-tuple-element.40), channel_id=1, source_target_pairs={{0,4},{4,0},{8,12},{12,8},{1,5},{5,1},{9,13},{13,9},{2,6},{6,2},{1... | collective-permute-start | bytes 442376 | tf_op jit(solution)/shard_map/ppermute | solution.py:194
  27.5 0.0 collective-permute-done.17.refs_6_
  27.5 1.3 %collective-permute-start.21 = (bf16[2,256,256]{2,1,0:T(8,128)(2,1)S(1)}, bf16[2,256,256]{2,1,0:T(8,128)(2,1)S(1)}, u32[]{:S(2)}, u32[]{:S(2)}) collective-permute-start(bf16[2,256,256]{2,1,0:T(8,128)(2,1)S(1)} %get-tuple-element.55), channel_id=1, source_target_pairs={{2,0},{3,1},{6,4},{7,5},{10,8},{11,9},{14,12},{15,13},{18,16},{19,... | collective-permute-start | bytes 786440 | tf_op jit(solution)/shard_map/ppermute | solution.py:200
  28.8 4.1 %collective-permute-done.18.refs_7_ = bf16[288,256]{1,0:T(8,128)(2,1)S(1)} collective-permute-done((bf16[288,256]{1,0:T(8,128)(2,1)S(1)}, bf16[288,256]{1,0:T(8,128)(2,1)S(1)}, u32[]{:S(2)}, u32[]{:S(2)}) %collective-permute-start.18) | collective-permute-done | bytes 147488 | tf_op jit(solution)/shard_map/ppermute | solution.py:194
  32.9 0.7 collective-permute-start.23
  33.6 0.0 collective-permute-done.3.refs_5_
  33.6 0.9 collective-permute-start.7
  34.6 4.1 %collective-permute-done.21.refs_12_ = bf16[2,256,256]{2,1,0:T(8,128)(2,1)S(1)} collective-permute-done((bf16[2,256,256]{2,1,0:T(8,128)(2,1)S(1)}, bf16[2,256,256]{2,1,0:T(8,128)(2,1)S(1)}, u32[]{:S(2)}, u32[]{:S(2)}) %collective-permute-start.21) | collective-permute-done | bytes 262176 | tf_op jit(solution)/shard_map/ppermute | solution.py:200
  38.6 1.3 %collective-permute-start.9 = (bf16[2,256,256]{2,1,0:T(8,128)(2,1)S(1)}, bf16[2,256,256]{2,1,0:T(8,128)(2,1)S(1)}, u32[]{:S(2)}, u32[]{:S(2)}) collective-permute-start(bf16[2,256,256]{2,1,0:T(8,128)(2,1)S(1)} %get-tuple-element.44), channel_id=1, source_target_pairs={{2,0},{3,1},{6,4},{7,5},{10,8},{11,9},{14,12},{15,13},{18,16},{19,... | collective-permute-start | bytes 786440 | tf_op jit(solution)/shard_map/ppermute | solution.py:200
  39.9 0.0 collective-permute-done.23.refs_14_
  39.9 0.7 collective-permute-start.11
  40.6 0.0 collective-permute-done.19.refs_10_
  40.6 1.8 %collective-permute-start.20 = (bf16[2,256,512]{2,1,0:T(8,128)(2,1)S(1)}, bf16[2,256,512]{2,1,0:T(8,128)(2,1)S(1)}, u32[]{:S(2)}, u32[]{:S(2)}) collective-permute-start(bf16[2,256,512]{2,1,0:T(8,128)(2,1)S(1)} %collective-permute-done.19.refs_10_), channel_id=1, source_target_pairs={{0,1},{1,0},{2,3},{3,2},{4,5},{5,4},{6,7},{7,6},{8,9},{9,8},{10,11... | collective-permute-start | bytes 1572872 | tf_op jit(solution)/shard_map/ppermute | solution.py:202
  42.4 13.1 %collective-permute-done.9.refs_12_ = bf16[2,256,256]{2,1,0:T(8,128)(2,1)S(1)} collective-permute-done((bf16[2,256,256]{2,1,0:T(8,128)(2,1)S(1)}, bf16[2,256,256]{2,1,0:T(8,128)(2,1)S(1)}, u32[]{:S(2)}, u32[]{:S(2)}) %collective-permute-start.9) | collective-permute-done | bytes 262176 | tf_op jit(solution)/shard_map/ppermute | solution.py:200
  55.5 1.0 collective-permute-start.22
  56.5 0.0 collective-permute-done.11.refs_14_
  56.5 2.8 %collective-permute-start.24 = (bf16[2,256,256]{2,1,0:T(8,128)(2,1)S(1)}, bf16[2,256,256]{2,1,0:T(8,128)(2,1)S(1)}, u32[]{:S(2)}, u32[]{:S(2)}) collective-permute-start(bf16[2,256,256]{2,1,0:T(8,128)(2,1)S(1)} %collective-permute-done.23.refs_14_), channel_id=1, source_target_pairs={{0,1},{1,0},{2,3},{3,2},{4,5},{5,4},{6,7},{7,6},{8,9},{9,8},{10,11... | collective-permute-start | bytes 786440 | tf_op jit(solution)/shard_map/ppermute | solution.py:202
  59.3 0.0 collective-permute-done.7.refs_10_
  59.3 0.0 collective-permute-start.8
  59.3 0.0 collective-permute-done.22.refs_13_
  59.3 3.2 %collective-permute-start.4 = (bf16[288,256]{1,0:T(8,128)(2,1)S(1)}, bf16[288,256]{1,0:T(8,128)(2,1)S(1)}, u32[]{:S(2)}, u32[]{:S(2)}) collective-permute-start(bf16[288,256]{1,0:T(8,128)(2,1)S(1)} %get-tuple-element.41), channel_id=1, source_target_pairs={{0,8},{4,12},{8,0},{12,4},{1,9},{5,13},{9,1},{13,5},{2,10},{6,14},... | collective-permute-start | bytes 442376 | tf_op jit(solution)/shard_map/ppermute | solution.py:194
  62.5 0.0 collective-permute-done.24.refs_15_
  62.5 0.2 collective-permute-start.10
  62.6 0.0 collective-permute-done.20.refs_11_
  62.6 0.3 collective-permute-start.12
  63.0 0.0 collective-permute-done.6.refs_9_
  63.0 3.9 %collective-permute-start.5 = (bf16[288,256]{1,0:T(8,128)(2,1)S(1)}, bf16[288,256]{1,0:T(8,128)(2,1)S(1)}, u32[]{:S(2)}, u32[]{:S(2)}) collective-permute-start(bf16[288,256]{1,0:T(8,128)(2,1)S(1)} %get-tuple-element.42), channel_id=1, source_target_pairs={{0,12},{4,8},{8,4},{12,0},{1,13},{5,9},{9,5},{13,1},{2,14},{6,10},... | collective-permute-start | bytes 442376 | tf_op jit(solution)/shard_map/ppermute | solution.py:194
  66.8 0.0 copy-done
  66.8 1.7 %shard_map.65 = (bf16[384,256]{1,0:T(8,128)(2,1)S(1)}, bf16[384,256]{1,0:T(8,128)(2,1)S(1)}, bf16[384,256]{1,0:T(8,128)(2,1)S(1)}, bf16[384,256]{1,0:T(8,128)(2,1)S(1)}) custom-call(bf16[96,512]{1,0:T(8,128)(2,1)S(1)} %get-tuple-element.33.refs_0_, bf16[96,512]{1,0:T(8,128)(2,1)S(1)} %collective-permute-done.refs_1_, ...), custom_call_target="tpu_custom_call" | custom-call | flops 805306368 | bytes 2097152 | tf_op jit(solution)/shard_map/pallas_call | solution.py:288
  68.5 4.9 %collective-permute-done.4.refs_6_ = bf16[288,256]{1,0:T(8,128)(2,1)S(1)} collective-permute-done((bf16[288,256]{1,0:T(8,128)(2,1)S(1)}, bf16[288,256]{1,0:T(8,128)(2,1)S(1)}, u32[]{:S(2)}, u32[]{:S(2)}) %collective-permute-start.4) | collective-permute-done | bytes 147488 | tf_op jit(solution)/shard_map/ppermute | solution.py:194
  73.5 0.5 collective-permute-start.25
  74.0 0.0 collective-permute-done.5.refs_7_
  74.0 5.0 %collective-permute-start.26 = (bf16[384,256]{1,0:T(8,128)(2,1)S(1)}, bf16[384,256]{1,0:T(8,128)(2,1)S(1)}, u32[]{:S(2)}, u32[]{:S(2)}) collective-permute-start(bf16[384,256]{1,0:T(8,128)(2,1)S(1)} %get-tuple-element.59), channel_id=1, source_target_pairs={{0,8},{4,12},{8,0},{12,4},{1,9},{5,13},{9,1},{13,5},{2,10},{6,14},... | collective-permute-start | bytes 589832 | tf_op jit(solution)/shard_map/ppermute | solution.py:194
  79.0 0.0 collective-permute-done.10.refs_13_
  79.0 0.5 collective-permute-start.27
  79.5 0.0 collective-permute-done.12.refs_15_
  79.5 0.0 collective-permute-done.8.refs_11_
  79.5 1.7 %shard_map.64 = (bf16[384,256]{1,0:T(8,128)(2,1)S(1)}, bf16[384,256]{1,0:T(8,128)(2,1)S(1)}, bf16[384,256]{1,0:T(8,128)(2,1)S(1)}, bf16[384,256]{1,0:T(8,128)(2,1)S(1)}) custom-call(bf16[96,512]{1,0:T(8,128)(2,1)S(1)} %get-tuple-element.33.refs_0_, bf16[96,512]{1,0:T(8,128)(2,1)S(1)} %collective-permute-done.refs_1_, ...), custom_call_target="tpu_custom_call" | custom-call | flops 805306368 | bytes 2097152 | tf_op jit(solution)/shard_map/pallas_call | solution.py:288
  81.2 0.2 collective-permute-start.14
  81.4 3.8 %collective-permute-start.15 = (bf16[384,256]{1,0:T(8,128)(2,1)S(1)}, bf16[384,256]{1,0:T(8,128)(2,1)S(1)}, u32[]{:S(2)}, u32[]{:S(2)}) collective-permute-start(bf16[384,256]{1,0:T(8,128)(2,1)S(1)} %get-tuple-element.49), channel_id=1, source_target_pairs={{0,8},{4,12},{8,0},{12,4},{1,9},{5,13},{9,1},{13,5},{2,10},{6,14},... | collective-permute-start | bytes 589832 | tf_op jit(solution)/shard_map/ppermute | solution.py:194
  85.2 0.0 collective-permute-done.25.refs_1_
  85.2 1.6 %collective-permute-start.13 = (bf16[384,256]{1,0:T(8,128)(2,1)S(1)}, bf16[384,256]{1,0:T(8,128)(2,1)S(1)}, u32[]{:S(2)}, u32[]{:S(2)}) collective-permute-start(bf16[384,256]{1,0:T(8,128)(2,1)S(1)} %get-tuple-element.46), channel_id=1, source_target_pairs={{0,12},{4,8},{8,4},{12,0},{1,13},{5,9},{9,5},{13,1},{2,14},{6,10},... | collective-permute-start | bytes 589832 | tf_op jit(solution)/shard_map/ppermute | solution.py:194
  86.8 6.4 %collective-permute-done.26.refs_2_ = bf16[384,256]{1,0:T(8,128)(2,1)S(1)} collective-permute-done((bf16[384,256]{1,0:T(8,128)(2,1)S(1)}, bf16[384,256]{1,0:T(8,128)(2,1)S(1)}, u32[]{:S(2)}, u32[]{:S(2)}) %collective-permute-start.26) | collective-permute-done | bytes 196640 | tf_op jit(solution)/shard_map/ppermute | solution.py:194
  93.3 0.0 collective-permute-done.27.refs_3_
  93.3 1.3 %shard_map.66.refs_3_ = bf16[384,2048]{1,0:T(8,128)(2,1)} custom-call(bf16[384,2048]{1,0:T(8,128)(2,1)S(1)} %bitcast.3, bf16[384,256]{1,0:T(8,128)(2,1)S(1)} %get-tuple-element.57.refs_0_, bf16[384,256]{1,0:T(8,128)(2,1)S(1)} %collective-permute-done.25.refs_1_, bf16[384,256]{1,0:T(8,128)(2,1)S(1)} %collective-permute-done.26.refs_2_, ...), custom_call_target="tpu_custom_call" | custom-call | flops 4718592 | bytes 2359296 | tf_op jit(solution)/shard_map/pallas_call | solution.py:308
  94.6 0.0 collective-permute-done.14.refs_1_
  94.6 15.5 %collective-permute-done.15.refs_2_ = bf16[384,256]{1,0:T(8,128)(2,1)S(1)} collective-permute-done((bf16[384,256]{1,0:T(8,128)(2,1)S(1)}, bf16[384,256]{1,0:T(8,128)(2,1)S(1)}, u32[]{:S(2)}, u32[]{:S(2)}) %collective-permute-start.15) | collective-permute-done | bytes 196640 | tf_op jit(solution)/shard_map/ppermute | solution.py:194
  110.1 1.2 %shard_map.67.refs_1_ = bf16[384,2048]{1,0:T(8,128)(2,1)} custom-call(bf16[384,2048]{1,0:T(8,128)(2,1)S(1)} %bitcast.4, bf16[384,256]{1,0:T(8,128)(2,1)S(1)} %get-tuple-element.47.refs_0_, bf16[384,256]{1,0:T(8,128)(2,1)S(1)} %collective-permute-done.14.refs_1_, ...), custom_call_target="tpu_custom_call", output_to_operand_aliasing={{}: (4, {})} | custom-call | flops 3538944 | bytes 1769472 | tf_op jit(solution)/shard_map/pallas_call | solution.py:308
  111.3 0.0 collective-permute-done.13.refs_0_
  111.3 0.8 shard_map.68
  (5 shorter events, 0.0 us)
Async XLA Ops:
  0.0 63.0 %collective-permute-start.6 = (bf16[4,256,1024]{2,1,0:T(8,128)(2,1)}, bf16[4,256,1024]{2,1,0:T(8,128)(2,1)S(1)}, u32[]{:S(2)}, u32[]{:S(2)}) collective-permute-start(bf16[4,256,1024]{2,1,0:T(8,128)(2,1)} %refs_8_.3), channel_id=1, source_target_pairs={{0,1},{1,0},{2,3},{3,2},{4,5},{5,4},{6,7},{7,6},{8,9},{9,8},{10,11... | collective-permute-start | bytes 6291464 | tf_op jit(solution)/shard_map/ppermute | solution.py:271
  2.1 10.0 %collective-permute-start = (bf16[96,512]{1,0:T(8,128)(2,1)S(1)}, bf16[96,512]{1,0:T(8,128)(2,1)S(1)}, u32[]{:S(2)}, u32[]{:S(2)}) collective-permute-start(bf16[96,512]{1,0:T(8,128)(2,1)S(1)} %get-tuple-element.34), channel_id=1, source_target_pairs={{0,4},{4,0},{8,12},{12,8},{1,5},{5,1},{9,13},{13,9},{2,6},{6,2},{1... | collective-permute-start | bytes 294920 | tf_op jit(solution)/shard_map/ppermute | solution.py:194
  4.8 62.1 %copy-start = (bf16[4,256,1024]{2,1,0:T(8,128)(2,1)S(1)}, bf16[4,256,1024]{2,1,0:T(8,128)(2,1)}, u32[]{:S(2)}) copy-start(bf16[4,256,1024]{2,1,0:T(8,128)(2,1)} %refs_8_.3) | copy-start | bytes 6291460
  4.8 62.1 %copy-start.2 = (bf16[4,1024]{1,0:T(4,128)(2,1)S(1)}, bf16[4,1024]{1,0:T(4,128)(2,1)}, u32[]{:S(2)}) copy-start(bf16[4,1024]{1,0:T(4,128)(2,1)} %refs_16_.3) | copy-start | bytes 24580
  7.5 18.2 %collective-permute-start.16 = (bf16[288,256]{1,0:T(8,128)(2,1)S(1)}, bf16[288,256]{1,0:T(8,128)(2,1)S(1)}, u32[]{:S(2)}, u32[]{:S(2)}) collective-permute-start(bf16[288,256]{1,0:T(8,128)(2,1)S(1)} %get-tuple-element.51), channel_id=1, source_target_pairs={{0,4},{4,0},{8,12},{12,8},{1,5},{5,1},{9,13},{13,9},{2,6},{6,2},{1... | collective-permute-start | bytes 442376 | tf_op jit(solution)/shard_map/ppermute | solution.py:194
  7.6 33.0 %collective-permute-start.19 = (bf16[2,256,512]{2,1,0:T(8,128)(2,1)S(1)}, bf16[2,256,512]{2,1,0:T(8,128)(2,1)S(1)}, u32[]{:S(2)}, u32[]{:S(2)}) collective-permute-start(bf16[2,256,512]{2,1,0:T(8,128)(2,1)S(1)} %get-tuple-element.54), channel_id=1, source_target_pairs={{0,2},{1,3},{2,0},{3,1},{4,6},{5,7},{6,4},{7,5},{8,10},{9,11},{10,... | collective-permute-start | bytes 1572872 | tf_op jit(solution)/shard_map/ppermute | solution.py:200
  9.5 5.8 %collective-permute-start.1 = (bf16[96,512]{1,0:T(8,128)(2,1)S(1)}, bf16[96,512]{1,0:T(8,128)(2,1)S(1)}, u32[]{:S(2)}, u32[]{:S(2)}) collective-permute-start(bf16[96,512]{1,0:T(8,128)(2,1)S(1)} %get-tuple-element.35), channel_id=1, source_target_pairs={{0,8},{4,12},{8,0},{12,4},{1,9},{5,13},{9,1},{13,5},{2,10},{6,14},... | collective-permute-start | bytes 294920 | tf_op jit(solution)/shard_map/ppermute | solution.py:194
  12.1 7.8 %collective-permute-start.2 = (bf16[96,512]{1,0:T(8,128)(2,1)S(1)}, bf16[96,512]{1,0:T(8,128)(2,1)S(1)}, u32[]{:S(2)}, u32[]{:S(2)}) collective-permute-start(bf16[96,512]{1,0:T(8,128)(2,1)S(1)} %get-tuple-element.36), channel_id=1, source_target_pairs={{0,12},{4,8},{8,4},{12,0},{1,13},{5,9},{9,5},{13,1},{2,14},{6,10},... | collective-permute-start | bytes 294920 | tf_op jit(solution)/shard_map/ppermute | solution.py:194
  15.3 12.2 %collective-permute-start.17 = (bf16[288,256]{1,0:T(8,128)(2,1)S(1)}, bf16[288,256]{1,0:T(8,128)(2,1)S(1)}, u32[]{:S(2)}, u32[]{:S(2)}) collective-permute-start(bf16[288,256]{1,0:T(8,128)(2,1)S(1)} %get-tuple-element.52), channel_id=1, source_target_pairs={{0,8},{4,12},{8,0},{12,4},{1,9},{5,13},{9,1},{13,5},{2,10},{6,14},... | collective-permute-start | bytes 442376 | tf_op jit(solution)/shard_map/ppermute | solution.py:194
  19.9 13.0 %collective-permute-start.18 = (bf16[288,256]{1,0:T(8,128)(2,1)S(1)}, bf16[288,256]{1,0:T(8,128)(2,1)S(1)}, u32[]{:S(2)}, u32[]{:S(2)}) collective-permute-start(bf16[288,256]{1,0:T(8,128)(2,1)S(1)} %get-tuple-element.53), channel_id=1, source_target_pairs={{0,12},{4,8},{8,4},{12,0},{1,13},{5,9},{9,5},{13,1},{2,14},{6,10},... | collective-permute-start | bytes 442376 | tf_op jit(solution)/shard_map/ppermute | solution.py:194
  25.8 7.9 %collective-permute-start.3 = (bf16[288,256]{1,0:T(8,128)(2,1)S(1)}, bf16[288,256]{1,0:T(8,128)(2,1)S(1)}, u32[]{:S(2)}, u32[]{:S(2)}) collective-permute-start(bf16[288,256]{1,0:T(8,128)(2,1)S(1)} %get-tuple-element.40), channel_id=1, source_target_pairs={{0,4},{4,0},{8,12},{12,8},{1,5},{5,1},{9,13},{13,9},{2,6},{6,2},{1... | collective-permute-start | bytes 442376 | tf_op jit(solution)/shard_map/ppermute | solution.py:194
  27.5 11.1 %collective-permute-start.21 = (bf16[2,256,256]{2,1,0:T(8,128)(2,1)S(1)}, bf16[2,256,256]{2,1,0:T(8,128)(2,1)S(1)}, u32[]{:S(2)}, u32[]{:S(2)}) collective-permute-start(bf16[2,256,256]{2,1,0:T(8,128)(2,1)S(1)} %get-tuple-element.55), channel_id=1, source_target_pairs={{2,0},{3,1},{6,4},{7,5},{10,8},{11,9},{14,12},{15,13},{18,16},{19,... | collective-permute-start | bytes 786440 | tf_op jit(solution)/shard_map/ppermute | solution.py:200
  32.9 7.0 %collective-permute-start.23 = (bf16[2,256,256]{2,1,0:T(8,128)(2,1)S(1)}, bf16[2,256,256]{2,1,0:T(8,128)(2,1)S(1)}, u32[]{:S(2)}, u32[]{:S(2)}) collective-permute-start(bf16[2,256,256]{2,1,0:T(8,128)(2,1)S(1)} %get-tuple-element.56), channel_id=1, source_target_pairs={{3,1},{7,5},{11,9},{15,13},{19,17},{23,21},{27,25},{31,29}} | collective-permute-start | bytes 786440 | tf_op jit(solution)/shard_map/ppermute | solution.py:200
  33.6 25.6 %collective-permute-start.7 = (bf16[2,256,512]{2,1,0:T(8,128)(2,1)S(1)}, bf16[2,256,512]{2,1,0:T(8,128)(2,1)S(1)}, u32[]{:S(2)}, u32[]{:S(2)}) collective-permute-start(bf16[2,256,512]{2,1,0:T(8,128)(2,1)S(1)} %get-tuple-element.43), channel_id=1, source_target_pairs={{0,2},{1,3},{2,0},{3,1},{4,6},{5,7},{6,4},{7,5},{8,10},{9,11},{10,... | collective-permute-start | bytes 1572872 | tf_op jit(solution)/shard_map/ppermute | solution.py:200
  38.6 16.9 %collective-permute-start.9 = (bf16[2,256,256]{2,1,0:T(8,128)(2,1)S(1)}, bf16[2,256,256]{2,1,0:T(8,128)(2,1)S(1)}, u32[]{:S(2)}, u32[]{:S(2)}) collective-permute-start(bf16[2,256,256]{2,1,0:T(8,128)(2,1)S(1)} %get-tuple-element.44), channel_id=1, source_target_pairs={{2,0},{3,1},{6,4},{7,5},{10,8},{11,9},{14,12},{15,13},{18,16},{19,... | collective-permute-start | bytes 786440 | tf_op jit(solution)/shard_map/ppermute | solution.py:200
  39.9 16.5 %collective-permute-start.11 = (bf16[2,256,256]{2,1,0:T(8,128)(2,1)S(1)}, bf16[2,256,256]{2,1,0:T(8,128)(2,1)S(1)}, u32[]{:S(2)}, u32[]{:S(2)}) collective-permute-start(bf16[2,256,256]{2,1,0:T(8,128)(2,1)S(1)} %get-tuple-element.45), channel_id=1, source_target_pairs={{3,1},{7,5},{11,9},{15,13},{19,17},{23,21},{27,25},{31,29}} | collective-permute-start | bytes 786440 | tf_op jit(solution)/shard_map/ppermute | solution.py:200
  40.6 22.0 %collective-permute-start.20 = (bf16[2,256,512]{2,1,0:T(8,128)(2,1)S(1)}, bf16[2,256,512]{2,1,0:T(8,128)(2,1)S(1)}, u32[]{:S(2)}, u32[]{:S(2)}) collective-permute-start(bf16[2,256,512]{2,1,0:T(8,128)(2,1)S(1)} %collective-permute-done.19.refs_10_), channel_id=1, source_target_pairs={{0,1},{1,0},{2,3},{3,2},{4,5},{5,4},{6,7},{7,6},{8,9},{9,8},{10,11... | collective-permute-start | bytes 1572872 | tf_op jit(solution)/shard_map/ppermute | solution.py:202
  55.5 3.8 %collective-permute-start.22 = (bf16[2,256,256]{2,1,0:T(8,128)(2,1)S(1)}, bf16[2,256,256]{2,1,0:T(8,128)(2,1)S(1)}, u32[]{:S(2)}, u32[]{:S(2)}) collective-permute-start(bf16[2,256,256]{2,1,0:T(8,128)(2,1)S(1)} %collective-permute-done.21.refs_12_), channel_id=1, source_target_pairs={{0,1},{1,0},{2,3},{3,2},{4,5},{5,4},{6,7},{7,6},{8,9},{9,8},{10,11... | collective-permute-start | bytes 786440 | tf_op jit(solution)/shard_map/ppermute | solution.py:202
  56.5 6.0 %collective-permute-start.24 = (bf16[2,256,256]{2,1,0:T(8,128)(2,1)S(1)}, bf16[2,256,256]{2,1,0:T(8,128)(2,1)S(1)}, u32[]{:S(2)}, u32[]{:S(2)}) collective-permute-start(bf16[2,256,256]{2,1,0:T(8,128)(2,1)S(1)} %collective-permute-done.23.refs_14_), channel_id=1, source_target_pairs={{0,1},{1,0},{2,3},{3,2},{4,5},{5,4},{6,7},{7,6},{8,9},{9,8},{10,11... | collective-permute-start | bytes 786440 | tf_op jit(solution)/shard_map/ppermute | solution.py:202
  59.3 20.2 %collective-permute-start.8 = (bf16[2,256,512]{2,1,0:T(8,128)(2,1)S(1)}, bf16[2,256,512]{2,1,0:T(8,128)(2,1)S(1)}, u32[]{:S(2)}, u32[]{:S(2)}) collective-permute-start(bf16[2,256,512]{2,1,0:T(8,128)(2,1)S(1)} %collective-permute-done.7.refs_10_), channel_id=1, source_target_pairs={{0,1},{1,0},{2,3},{3,2},{4,5},{5,4},{6,7},{7,6},{8,9},{9,8},{10,11... | collective-permute-start | bytes 1572872 | tf_op jit(solution)/shard_map/ppermute | solution.py:202
  59.3 14.2 %collective-permute-start.4 = (bf16[288,256]{1,0:T(8,128)(2,1)S(1)}, bf16[288,256]{1,0:T(8,128)(2,1)S(1)}, u32[]{:S(2)}, u32[]{:S(2)}) collective-permute-start(bf16[288,256]{1,0:T(8,128)(2,1)S(1)} %get-tuple-element.41), channel_id=1, source_target_pairs={{0,8},{4,12},{8,0},{12,4},{1,9},{5,13},{9,1},{13,5},{2,10},{6,14},... | collective-permute-start | bytes 442376 | tf_op jit(solution)/shard_map/ppermute | solution.py:194
  62.5 16.6 %collective-permute-start.10 = (bf16[2,256,256]{2,1,0:T(8,128)(2,1)S(1)}, bf16[2,256,256]{2,1,0:T(8,128)(2,1)S(1)}, u32[]{:S(2)}, u32[]{:S(2)}) collective-permute-start(bf16[2,256,256]{2,1,0:T(8,128)(2,1)S(1)} %collective-permute-done.9.refs_12_), channel_id=1, source_target_pairs={{0,1},{1,0},{2,3},{3,2},{4,5},{5,4},{6,7},{7,6},{8,9},{9,8},{10,11... | collective-permute-start | bytes 786440 | tf_op jit(solution)/shard_map/ppermute | solution.py:202
  62.6 16.9 %collective-permute-start.12 = (bf16[2,256,256]{2,1,0:T(8,128)(2,1)S(1)}, bf16[2,256,256]{2,1,0:T(8,128)(2,1)S(1)}, u32[]{:S(2)}, u32[]{:S(2)}) collective-permute-start(bf16[2,256,256]{2,1,0:T(8,128)(2,1)S(1)} %collective-permute-done.11.refs_14_), channel_id=1, source_target_pairs={{0,1},{1,0},{2,3},{3,2},{4,5},{5,4},{6,7},{7,6},{8,9},{9,8},{10,11... | collective-permute-start | bytes 786440 | tf_op jit(solution)/shard_map/ppermute | solution.py:202
  63.0 11.0 %collective-permute-start.5 = (bf16[288,256]{1,0:T(8,128)(2,1)S(1)}, bf16[288,256]{1,0:T(8,128)(2,1)S(1)}, u32[]{:S(2)}, u32[]{:S(2)}) collective-permute-start(bf16[288,256]{1,0:T(8,128)(2,1)S(1)} %get-tuple-element.42), channel_id=1, source_target_pairs={{0,12},{4,8},{8,4},{12,0},{1,13},{5,9},{9,5},{13,1},{2,14},{6,10},... | collective-permute-start | bytes 442376 | tf_op jit(solution)/shard_map/ppermute | solution.py:194
  73.5 11.7 %collective-permute-start.25 = (bf16[384,256]{1,0:T(8,128)(2,1)S(1)}, bf16[384,256]{1,0:T(8,128)(2,1)S(1)}, u32[]{:S(2)}, u32[]{:S(2)}) collective-permute-start(bf16[384,256]{1,0:T(8,128)(2,1)S(1)} %get-tuple-element.58), channel_id=1, source_target_pairs={{0,4},{4,0},{8,12},{12,8},{1,5},{5,1},{9,13},{13,9},{2,6},{6,2},{1... | collective-permute-start | bytes 589832 | tf_op jit(solution)/shard_map/ppermute | solution.py:194
  74.0 19.3 %collective-permute-start.26 = (bf16[384,256]{1,0:T(8,128)(2,1)S(1)}, bf16[384,256]{1,0:T(8,128)(2,1)S(1)}, u32[]{:S(2)}, u32[]{:S(2)}) collective-permute-start(bf16[384,256]{1,0:T(8,128)(2,1)S(1)} %get-tuple-element.59), channel_id=1, source_target_pairs={{0,8},{4,12},{8,0},{12,4},{1,9},{5,13},{9,1},{13,5},{2,10},{6,14},... | collective-permute-start | bytes 589832 | tf_op jit(solution)/shard_map/ppermute | solution.py:194
  79.0 14.2 %collective-permute-start.27 = (bf16[384,256]{1,0:T(8,128)(2,1)S(1)}, bf16[384,256]{1,0:T(8,128)(2,1)S(1)}, u32[]{:S(2)}, u32[]{:S(2)}) collective-permute-start(bf16[384,256]{1,0:T(8,128)(2,1)S(1)} %get-tuple-element.60), channel_id=1, source_target_pairs={{0,12},{4,8},{8,4},{12,0},{1,13},{5,9},{9,5},{13,1},{2,14},{6,10},... | collective-permute-start | bytes 589832 | tf_op jit(solution)/shard_map/ppermute | solution.py:194
  79.5 13.8 %copy-start.1 = (bf16[1,384,2048]{2,1,0:T(8,128)(2,1)S(1)}, bf16[1,384,2048]{2,1,0:T(8,128)(2,1)}, u32[]{:S(2)}) copy-start(bf16[1,384,2048]{2,1,0:T(8,128)(2,1)} %param.6) | copy-start | bytes 4718596
  81.2 13.4 %collective-permute-start.14 = (bf16[384,256]{1,0:T(8,128)(2,1)S(1)}, bf16[384,256]{1,0:T(8,128)(2,1)S(1)}, u32[]{:S(2)}, u32[]{:S(2)}) collective-permute-start(bf16[384,256]{1,0:T(8,128)(2,1)S(1)} %get-tuple-element.48), channel_id=1, source_target_pairs={{0,4},{4,0},{8,12},{12,8},{1,5},{5,1},{9,13},{13,9},{2,6},{6,2},{1... | collective-permute-start | bytes 589832 | tf_op jit(solution)/shard_map/ppermute | solution.py:194
  81.4 28.7 %collective-permute-start.15 = (bf16[384,256]{1,0:T(8,128)(2,1)S(1)}, bf16[384,256]{1,0:T(8,128)(2,1)S(1)}, u32[]{:S(2)}, u32[]{:S(2)}) collective-permute-start(bf16[384,256]{1,0:T(8,128)(2,1)S(1)} %get-tuple-element.49), channel_id=1, source_target_pairs={{0,8},{4,12},{8,0},{12,4},{1,9},{5,13},{9,1},{13,5},{2,10},{6,14},... | collective-permute-start | bytes 589832 | tf_op jit(solution)/shard_map/ppermute | solution.py:194
  85.2 26.1 %collective-permute-start.13 = (bf16[384,256]{1,0:T(8,128)(2,1)S(1)}, bf16[384,256]{1,0:T(8,128)(2,1)S(1)}, u32[]{:S(2)}, u32[]{:S(2)}) collective-permute-start(bf16[384,256]{1,0:T(8,128)(2,1)S(1)} %get-tuple-element.46), channel_id=1, source_target_pairs={{0,12},{4,8},{8,4},{12,0},{1,13},{5,9},{9,5},{13,1},{2,14},{6,10},... | collective-permute-start | bytes 589832 | tf_op jit(solution)/shard_map/ppermute | solution.py:194

commit v6 on v5

--- a/solution.py
+++ b/solution.py
@@ -69,12 +69,10 @@
     outs, parts = refs[:len(lanes)], refs[len(lanes):len(lanes) + len(cuts)]
     gain, bias, value, held, sems = refs[len(lanes) + len(cuts):]
     head = value.shape[0]
-    half = head // 32 * 16
     pairs = [
-        (value_ref.at[pl.ds(0, half), :], value.at[pl.ds(0, half), :]),
+        (value_ref.at[pl.ds(0, head), :], value),
         (gain_ref, gain),
         (bias_ref, bias),
-        (value_ref.at[pl.ds(half, head - half), :], value.at[pl.ds(half, head - half), :]),
     ]
     copies = [pltpu.make_async_copy(source, target, sems.at[k]) for k, (source, target) in enumerate(pairs)]
     copies += weight_copies(cuts, weight_ref, parts, sems, len(pairs))
@@ -84,11 +82,9 @@
         copy.wait()
     scale = gain[...].astype(jnp.float32).reshape(1, -1)
     offset = bias[...].astype(jnp.float32).reshape(1, -1)
-    normalise(value.at[pl.ds(0, half), :], held.at[pl.ds(0, half), :], scale, offset, rows_step)
-    copies[3].wait()
-    normalise(value.at[pl.ds(half, head - half), :], held.at[pl.ds(half, head - half), :], scale, offset, rows_step)
+    normalise(value, held, scale, offset, rows_step)
     hand_out(shards, span, lanes, held, outs)
-    for copy in copies[4:]:
+    for copy in copies[3:]:
         copy.wait()
 
 
@@ -240,7 +236,7 @@
         scratch_shapes=[
             pltpu.VMEM((head, width), jnp.bfloat16),
             pltpu.VMEM((head, width), jnp.bfloat16),
-            pltpu.SemaphoreType.DMA((4 + ncuts,)),
+            pltpu.SemaphoreType.DMA((3 + ncuts,)),
         ],
         compiler_params=small,
         cost_estimate=cost(head),

time: 112 us -> 112 us (level)
  no operation moved by 1% of the time
where the time goes in v6:
time: 112 us
  waiting for transfers between devices  51.4 us (46%)
  starting transfers between devices  49.4 us (44%)
  Pallas kernels  11 us (10%)
    ppermute x15, starting transfers between devices, exchange_step(): return lax.ppermute(x, 'sp', swap_pairs(shards, step))  36.2 us
    ppermute x15, waiting for transfers between devices, exchange_step(): return lax.ppermute(x, 'sp', swap_pairs(shards, step))  34.2 us
    ppermute x6, waiting for transfers between devices, exchange_rows(): lax.ppermute(part, 'dp', [p for p in swap_pairs(ndp, 2) if p[0] >= least])  17.2 us
    ppermute x6, starting transfers between devices, exchange_rows(): lax.ppermute(part, 'dp', [p for p in swap_pairs(ndp, 2) if p[0] >= least])  6.72 us
    ppermute x6, starting transfers between devices, exchange_rows(): got.append((lax.ppermute(far, 'dp', swap_pairs(ndp, 1)), 3, None, low, 0))  6.04 us
    pallas_call x2, Pallas kernels, compute(): pl.pallas_call(functools.partial(mix_kernel, nsp, length, c * per, c * pe...  3.4 us
    pallas_call x3, Pallas kernels, compute(): pl.pallas_call(functools.partial(gate_kernel, nsp, chunks, c, steps, 32),...  3.31 us
    pallas_call x1, Pallas kernels, compute(): pl.pallas_call(functools.partial(rest_kernel, nsp, span, 16, head, lanes,...  2.74 us
  transfers between devices with their start and end apart: 28, of which 8 were waited for; matrix products, arithmetic and copies ran while one was open for 0% of the time, Pallas kernels for 9%

profile of v6, /device:TPU:0, one launch (start us, length us, event | category | flops | bytes accessed | tf_op | source)
XLA Modules:
  0.0 112.0 jit_solution(16262592187608164044)
XLA Ops:
  0.0 0.5 collective-permute-start.6
  0.5 1.5 %norm_head.1 = (bf16[96,512]{1,0:T(8,128)(2,1)S(1)}, bf16[96,512]{1,0:T(8,128)(2,1)S(1)}, bf16[96,512]{1,0:T(8,128)(2,1)S(1)}, bf16[96,512]{1,0:T(8,128)(2,1)S(1...) custom-call(bf16[384,2048]{1,0:T(8,128)(2,1)} %bitcast.6, ...), custom_call_target="tpu_custom_call" | custom-call | flops 5898240 | bytes 786432 | tf_op jit(solution)/shard_map/norm_head/pallas_call | solution.py:231
  2.0 2.6 %collective-permute-start = (bf16[96,512]{1,0:T(8,128)(2,1)S(1)}, bf16[96,512]{1,0:T(8,128)(2,1)S(1)}, u32[]{:S(2)}, u32[]{:S(2)}) collective-permute-start(bf16[96,512]{1,0:T(8,128)(2,1)S(1)} %get-tuple-element.34), channel_id=1, source_target_pairs={{0,4},{4,0},{8,12},{12,8},{1,5},{5,1},{9,13},{13,9},{2,6},{6,2},{1... | collective-permute-start | bytes 294920 | tf_op jit(solution)/shard_map/ppermute | solution.py:190
  4.7 2.7 %norm_rest.1 = (bf16[288,256]{1,0:T(8,128)(2,1)S(1)}, bf16[288,256]{1,0:T(8,128)(2,1)S(1)}, bf16[288,256]{1,0:T(8,128)(2,1)S(1)}, bf16[288,256]{1,0:T(8,128)(2,1...) custom-call(bf16[2048]{0:T(1024)(128)(2,1)S(1)} %get-tuple-element.3, ...), custom_call_target="tpu_custom_call" | custom-call | flops 17694720 | bytes 2359296 | tf_op jit(solution)/shard_map/norm_rest/pallas_call | solution.py:250
  7.4 0.1 collective-permute-start.16
  7.5 1.9 %collective-permute-start.19 = (bf16[2,256,512]{2,1,0:T(8,128)(2,1)S(1)}, bf16[2,256,512]{2,1,0:T(8,128)(2,1)S(1)}, u32[]{:S(2)}, u32[]{:S(2)}) collective-permute-start(bf16[2,256,512]{2,1,0:T(8,128)(2,1)S(1)} %get-tuple-element.54), channel_id=1, source_target_pairs={{0,2},{1,3},{2,0},{3,1},{4,6},{5,7},{6,4},{7,5},{8,10},{9,11},{10,... | collective-permute-start | bytes 1572872 | tf_op jit(solution)/shard_map/ppermute | solution.py:196
  9.4 2.6 %collective-permute-start.1 = (bf16[96,512]{1,0:T(8,128)(2,1)S(1)}, bf16[96,512]{1,0:T(8,128)(2,1)S(1)}, u32[]{:S(2)}, u32[]{:S(2)}) collective-permute-start(bf16[96,512]{1,0:T(8,128)(2,1)S(1)} %get-tuple-element.35), channel_id=1, source_target_pairs={{0,8},{4,12},{8,0},{12,4},{1,9},{5,13},{9,1},{13,5},{2,10},{6,14},... | collective-permute-start | bytes 294920 | tf_op jit(solution)/shard_map/ppermute | solution.py:190
  12.0 0.0 collective-permute-done.refs_1_
  12.0 1.3 %collective-permute-start.2 = (bf16[96,512]{1,0:T(8,128)(2,1)S(1)}, bf16[96,512]{1,0:T(8,128)(2,1)S(1)}, u32[]{:S(2)}, u32[]{:S(2)}) collective-permute-start(bf16[96,512]{1,0:T(8,128)(2,1)S(1)} %get-tuple-element.36), channel_id=1, source_target_pairs={{0,12},{4,8},{8,4},{12,0},{1,13},{5,9},{9,5},{13,1},{2,14},{6,10},... | collective-permute-start | bytes 294920 | tf_op jit(solution)/shard_map/ppermute | solution.py:190
  13.4 1.9 %collective-permute-done.1.refs_2_ = bf16[96,512]{1,0:T(8,128)(2,1)S(1)} collective-permute-done((bf16[96,512]{1,0:T(8,128)(2,1)S(1)}, bf16[96,512]{1,0:T(8,128)(2,1)S(1)}, u32[]{:S(2)}, u32[]{:S(2)}) %collective-permute-start.1) | collective-permute-done | bytes 98336 | tf_op jit(solution)/shard_map/ppermute | solution.py:190
  15.2 3.2 %collective-permute-start.17 = (bf16[288,256]{1,0:T(8,128)(2,1)S(1)}, bf16[288,256]{1,0:T(8,128)(2,1)S(1)}, u32[]{:S(2)}, u32[]{:S(2)}) collective-permute-start(bf16[288,256]{1,0:T(8,128)(2,1)S(1)} %get-tuple-element.52), channel_id=1, source_target_pairs={{0,8},{4,12},{8,0},{12,4},{1,9},{5,13},{9,1},{13,5},{2,10},{6,14},... | collective-permute-start | bytes 442376 | tf_op jit(solution)/shard_map/ppermute | solution.py:190
  18.4 1.4 %collective-permute-done.2.refs_3_ = bf16[96,512]{1,0:T(8,128)(2,1)S(1)} collective-permute-done((bf16[96,512]{1,0:T(8,128)(2,1)S(1)}, bf16[96,512]{1,0:T(8,128)(2,1)S(1)}, u32[]{:S(2)}, u32[]{:S(2)}) %collective-permute-start.2) | collective-permute-done | bytes 98336 | tf_op jit(solution)/shard_map/ppermute | solution.py:190
  19.8 5.8 %collective-permute-start.18 = (bf16[288,256]{1,0:T(8,128)(2,1)S(1)}, bf16[288,256]{1,0:T(8,128)(2,1)S(1)}, u32[]{:S(2)}, u32[]{:S(2)}) collective-permute-start(bf16[288,256]{1,0:T(8,128)(2,1)S(1)} %get-tuple-element.53), channel_id=1, source_target_pairs={{0,12},{4,8},{8,4},{12,0},{1,13},{5,9},{9,5},{13,1},{2,14},{6,10},... | collective-permute-start | bytes 442376 | tf_op jit(solution)/shard_map/ppermute | solution.py:190
  25.6 0.0 collective-permute-done.16.refs_5_
  25.6 1.8 %collective-permute-start.3 = (bf16[288,256]{1,0:T(8,128)(2,1)S(1)}, bf16[288,256]{1,0:T(8,128)(2,1)S(1)}, u32[]{:S(2)}, u32[]{:S(2)}) collective-permute-start(bf16[288,256]{1,0:T(8,128)(2,1)S(1)} %get-tuple-element.40), channel_id=1, source_target_pairs={{0,4},{4,0},{8,12},{12,8},{1,5},{5,1},{9,13},{13,9},{2,6},{6,2},{1... | collective-permute-start | bytes 442376 | tf_op jit(solution)/shard_map/ppermute | solution.py:190
  27.4 0.0 collective-permute-done.17.refs_6_
  27.4 1.3 %collective-permute-start.21 = (bf16[2,256,256]{2,1,0:T(8,128)(2,1)S(1)}, bf16[2,256,256]{2,1,0:T(8,128)(2,1)S(1)}, u32[]{:S(2)}, u32[]{:S(2)}) collective-permute-start(bf16[2,256,256]{2,1,0:T(8,128)(2,1)S(1)} %get-tuple-element.55), channel_id=1, source_target_pairs={{2,0},{3,1},{6,4},{7,5},{10,8},{11,9},{14,12},{15,13},{18,16},{19,... | collective-permute-start | bytes 786440 | tf_op jit(solution)/shard_map/ppermute | solution.py:196
  28.7 4.1 %collective-permute-done.18.refs_7_ = bf16[288,256]{1,0:T(8,128)(2,1)S(1)} collective-permute-done((bf16[288,256]{1,0:T(8,128)(2,1)S(1)}, bf16[288,256]{1,0:T(8,128)(2,1)S(1)}, u32[]{:S(2)}, u32[]{:S(2)}) %collective-permute-start.18) | collective-permute-done | bytes 147488 | tf_op jit(solution)/shard_map/ppermute | solution.py:190
  32.8 0.7 collective-permute-start.23
  33.5 0.0 collective-permute-done.3.refs_5_
  33.5 0.9 collective-permute-start.7
  34.4 4.1 %collective-permute-done.21.refs_12_ = bf16[2,256,256]{2,1,0:T(8,128)(2,1)S(1)} collective-permute-done((bf16[2,256,256]{2,1,0:T(8,128)(2,1)S(1)}, bf16[2,256,256]{2,1,0:T(8,128)(2,1)S(1)}, u32[]{:S(2)}, u32[]{:S(2)}) %collective-permute-start.21) | collective-permute-done | bytes 262176 | tf_op jit(solution)/shard_map/ppermute | solution.py:196
  38.5 1.3 %collective-permute-start.9 = (bf16[2,256,256]{2,1,0:T(8,128)(2,1)S(1)}, bf16[2,256,256]{2,1,0:T(8,128)(2,1)S(1)}, u32[]{:S(2)}, u32[]{:S(2)}) collective-permute-start(bf16[2,256,256]{2,1,0:T(8,128)(2,1)S(1)} %get-tuple-element.44), channel_id=1, source_target_pairs={{2,0},{3,1},{6,4},{7,5},{10,8},{11,9},{14,12},{15,13},{18,16},{19,... | collective-permute-start | bytes 786440 | tf_op jit(solution)/shard_map/ppermute | solution.py:196
  39.8 0.0 collective-permute-done.23.refs_14_
  39.8 0.7 collective-permute-start.11
  40.5 0.0 collective-permute-done.19.refs_10_
  40.5 1.8 %collective-permute-start.20 = (bf16[2,256,512]{2,1,0:T(8,128)(2,1)S(1)}, bf16[2,256,512]{2,1,0:T(8,128)(2,1)S(1)}, u32[]{:S(2)}, u32[]{:S(2)}) collective-permute-start(bf16[2,256,512]{2,1,0:T(8,128)(2,1)S(1)} %collective-permute-done.19.refs_10_), channel_id=1, source_target_pairs={{0,1},{1,0},{2,3},{3,2},{4,5},{5,4},{6,7},{7,6},{8,9},{9,8},{10,11... | collective-permute-start | bytes 1572872 | tf_op jit(solution)/shard_map/ppermute | solution.py:198
  42.3 13.1 %collective-permute-done.9.refs_12_ = bf16[2,256,256]{2,1,0:T(8,128)(2,1)S(1)} collective-permute-done((bf16[2,256,256]{2,1,0:T(8,128)(2,1)S(1)}, bf16[2,256,256]{2,1,0:T(8,128)(2,1)S(1)}, u32[]{:S(2)}, u32[]{:S(2)}) %collective-permute-start.9) | collective-permute-done | bytes 262176 | tf_op jit(solution)/shard_map/ppermute | solution.py:196
  55.4 1.0 collective-permute-start.22
  56.4 0.0 collective-permute-done.11.refs_14_
  56.4 2.8 %collective-permute-start.24 = (bf16[2,256,256]{2,1,0:T(8,128)(2,1)S(1)}, bf16[2,256,256]{2,1,0:T(8,128)(2,1)S(1)}, u32[]{:S(2)}, u32[]{:S(2)}) collective-permute-start(bf16[2,256,256]{2,1,0:T(8,128)(2,1)S(1)} %collective-permute-done.23.refs_14_), channel_id=1, source_target_pairs={{0,1},{1,0},{2,3},{3,2},{4,5},{5,4},{6,7},{7,6},{8,9},{9,8},{10,11... | collective-permute-start | bytes 786440 | tf_op jit(solution)/shard_map/ppermute | solution.py:198
  59.2 0.0 collective-permute-done.7.refs_10_
  59.2 0.0 collective-permute-start.8
  59.2 0.0 collective-permute-done.22.refs_13_
  59.2 3.2 %collective-permute-start.4 = (bf16[288,256]{1,0:T(8,128)(2,1)S(1)}, bf16[288,256]{1,0:T(8,128)(2,1)S(1)}, u32[]{:S(2)}, u32[]{:S(2)}) collective-permute-start(bf16[288,256]{1,0:T(8,128)(2,1)S(1)} %get-tuple-element.41), channel_id=1, source_target_pairs={{0,8},{4,12},{8,0},{12,4},{1,9},{5,13},{9,1},{13,5},{2,10},{6,14},... | collective-permute-start | bytes 442376 | tf_op jit(solution)/shard_map/ppermute | solution.py:190
  62.4 0.0 collective-permute-done.24.refs_15_
  62.4 0.2 collective-permute-start.10
  62.5 0.0 collective-permute-done.20.refs_11_
  62.5 0.3 collective-permute-start.12
  62.9 0.0 collective-permute-done.6.refs_9_
  62.9 3.9 %collective-permute-start.5 = (bf16[288,256]{1,0:T(8,128)(2,1)S(1)}, bf16[288,256]{1,0:T(8,128)(2,1)S(1)}, u32[]{:S(2)}, u32[]{:S(2)}) collective-permute-start(bf16[288,256]{1,0:T(8,128)(2,1)S(1)} %get-tuple-element.42), channel_id=1, source_target_pairs={{0,12},{4,8},{8,4},{12,0},{1,13},{5,9},{9,5},{13,1},{2,14},{6,10},... | collective-permute-start | bytes 442376 | tf_op jit(solution)/shard_map/ppermute | solution.py:190
  66.7 0.0 copy-done
  66.7 1.7 %shard_map.65 = (bf16[384,256]{1,0:T(8,128)(2,1)S(1)}, bf16[384,256]{1,0:T(8,128)(2,1)S(1)}, bf16[384,256]{1,0:T(8,128)(2,1)S(1)}, bf16[384,256]{1,0:T(8,128)(2,1)S(1)}) custom-call(bf16[96,512]{1,0:T(8,128)(2,1)S(1)} %get-tuple-element.33.refs_0_, bf16[96,512]{1,0:T(8,128)(2,1)S(1)} %collective-permute-done.refs_1_, ...), custom_call_target="tpu_custom_call" | custom-call | flops 805306368 | bytes 2097152 | tf_op jit(solution)/shard_map/pallas_call | solution.py:284
  68.5 4.9 %collective-permute-done.4.refs_6_ = bf16[288,256]{1,0:T(8,128)(2,1)S(1)} collective-permute-done((bf16[288,256]{1,0:T(8,128)(2,1)S(1)}, bf16[288,256]{1,0:T(8,128)(2,1)S(1)}, u32[]{:S(2)}, u32[]{:S(2)}) %collective-permute-start.4) | collective-permute-done | bytes 147488 | tf_op jit(solution)/shard_map/ppermute | solution.py:190
  73.4 0.5 collective-permute-start.25
  73.9 0.0 collective-permute-done.5.refs_7_
  73.9 5.0 %collective-permute-start.26 = (bf16[384,256]{1,0:T(8,128)(2,1)S(1)}, bf16[384,256]{1,0:T(8,128)(2,1)S(1)}, u32[]{:S(2)}, u32[]{:S(2)}) collective-permute-start(bf16[384,256]{1,0:T(8,128)(2,1)S(1)} %get-tuple-element.59), channel_id=1, source_target_pairs={{0,8},{4,12},{8,0},{12,4},{1,9},{5,13},{9,1},{13,5},{2,10},{6,14},... | collective-permute-start | bytes 589832 | tf_op jit(solution)/shard_map/ppermute | solution.py:190
  78.9 0.0 collective-permute-done.10.refs_13_
  78.9 0.5 collective-permute-start.27
  79.4 0.0 collective-permute-done.12.refs_15_
  79.4 0.0 collective-permute-done.8.refs_11_
  79.4 1.7 %shard_map.64 = (bf16[384,256]{1,0:T(8,128)(2,1)S(1)}, bf16[384,256]{1,0:T(8,128)(2,1)S(1)}, bf16[384,256]{1,0:T(8,128)(2,1)S(1)}, bf16[384,256]{1,0:T(8,128)(2,1)S(1)}) custom-call(bf16[96,512]{1,0:T(8,128)(2,1)S(1)} %get-tuple-element.33.refs_0_, bf16[96,512]{1,0:T(8,128)(2,1)S(1)} %collective-permute-done.refs_1_, ...), custom_call_target="tpu_custom_call" | custom-call | flops 805306368 | bytes 2097152 | tf_op jit(solution)/shard_map/pallas_call | solution.py:284
  81.1 0.2 collective-permute-start.14
  81.3 3.8 %collective-permute-start.15 = (bf16[384,256]{1,0:T(8,128)(2,1)S(1)}, bf16[384,256]{1,0:T(8,128)(2,1)S(1)}, u32[]{:S(2)}, u32[]{:S(2)}) collective-permute-start(bf16[384,256]{1,0:T(8,128)(2,1)S(1)} %get-tuple-element.49), channel_id=1, source_target_pairs={{0,8},{4,12},{8,0},{12,4},{1,9},{5,13},{9,1},{13,5},{2,10},{6,14},... | collective-permute-start | bytes 589832 | tf_op jit(solution)/shard_map/ppermute | solution.py:190
  85.1 0.0 collective-permute-done.25.refs_1_
  85.1 1.6 %collective-permute-start.13 = (bf16[384,256]{1,0:T(8,128)(2,1)S(1)}, bf16[384,256]{1,0:T(8,128)(2,1)S(1)}, u32[]{:S(2)}, u32[]{:S(2)}) collective-permute-start(bf16[384,256]{1,0:T(8,128)(2,1)S(1)} %get-tuple-element.46), channel_id=1, source_target_pairs={{0,12},{4,8},{8,4},{12,0},{1,13},{5,9},{9,5},{13,1},{2,14},{6,10},... | collective-permute-start | bytes 589832 | tf_op jit(solution)/shard_map/ppermute | solution.py:190
  86.7 6.4 %collective-permute-done.26.refs_2_ = bf16[384,256]{1,0:T(8,128)(2,1)S(1)} collective-permute-done((bf16[384,256]{1,0:T(8,128)(2,1)S(1)}, bf16[384,256]{1,0:T(8,128)(2,1)S(1)}, u32[]{:S(2)}, u32[]{:S(2)}) %collective-permute-start.26) | collective-permute-done | bytes 196640 | tf_op jit(solution)/shard_map/ppermute | solution.py:190
  93.2 0.0 collective-permute-done.27.refs_3_
  93.2 1.3 %shard_map.66.refs_3_ = bf16[384,2048]{1,0:T(8,128)(2,1)} custom-call(bf16[384,2048]{1,0:T(8,128)(2,1)S(1)} %bitcast.3, bf16[384,256]{1,0:T(8,128)(2,1)S(1)} %get-tuple-element.57.refs_0_, bf16[384,256]{1,0:T(8,128)(2,1)S(1)} %collective-permute-done.25.refs_1_, bf16[384,256]{1,0:T(8,128)(2,1)S(1)} %collective-permute-done.26.refs_2_, ...), custom_call_target="tpu_custom_call" | custom-call | flops 4718592 | bytes 2359296 | tf_op jit(solution)/shard_map/pallas_call | solution.py:304
  94.5 0.0 collective-permute-done.14.refs_1_
  94.5 15.5 %collective-permute-done.15.refs_2_ = bf16[384,256]{1,0:T(8,128)(2,1)S(1)} collective-permute-done((bf16[384,256]{1,0:T(8,128)(2,1)S(1)}, bf16[384,256]{1,0:T(8,128)(2,1)S(1)}, u32[]{:S(2)}, u32[]{:S(2)}) %collective-permute-start.15) | collective-permute-done | bytes 196640 | tf_op jit(solution)/shard_map/ppermute | solution.py:190
  110.0 1.2 %shard_map.67.refs_1_ = bf16[384,2048]{1,0:T(8,128)(2,1)} custom-call(bf16[384,2048]{1,0:T(8,128)(2,1)S(1)} %bitcast.4, bf16[384,256]{1,0:T(8,128)(2,1)S(1)} %get-tuple-element.47.refs_0_, bf16[384,256]{1,0:T(8,128)(2,1)S(1)} %collective-permute-done.14.refs_1_, ...), custom_call_target="tpu_custom_call", output_to_operand_aliasing={{}: (4, {})} | custom-call | flops 3538944 | bytes 1769472 | tf_op jit(solution)/shard_map/pallas_call | solution.py:304
  111.2 0.0 collective-permute-done.13.refs_0_
  111.2 0.8 shard_map.68
  (5 shorter events, 0.0 us)
Async XLA Ops:
  0.0 62.9 %collective-permute-start.6 = (bf16[4,256,1024]{2,1,0:T(8,128)(2,1)}, bf16[4,256,1024]{2,1,0:T(8,128)(2,1)S(1)}, u32[]{:S(2)}, u32[]{:S(2)}) collective-permute-start(bf16[4,256,1024]{2,1,0:T(8,128)(2,1)} %refs_8_.3), channel_id=1, source_target_pairs={{0,1},{1,0},{2,3},{3,2},{4,5},{5,4},{6,7},{7,6},{8,9},{9,8},{10,11... | collective-permute-start | bytes 6291464 | tf_op jit(solution)/shard_map/ppermute | solution.py:267
  2.0 10.0 %collective-permute-start = (bf16[96,512]{1,0:T(8,128)(2,1)S(1)}, bf16[96,512]{1,0:T(8,128)(2,1)S(1)}, u32[]{:S(2)}, u32[]{:S(2)}) collective-permute-start(bf16[96,512]{1,0:T(8,128)(2,1)S(1)} %get-tuple-element.34), channel_id=1, source_target_pairs={{0,4},{4,0},{8,12},{12,8},{1,5},{5,1},{9,13},{13,9},{2,6},{6,2},{1... | collective-permute-start | bytes 294920 | tf_op jit(solution)/shard_map/ppermute | solution.py:190
  4.7 62.1 %copy-start = (bf16[4,256,1024]{2,1,0:T(8,128)(2,1)S(1)}, bf16[4,256,1024]{2,1,0:T(8,128)(2,1)}, u32[]{:S(2)}) copy-start(bf16[4,256,1024]{2,1,0:T(8,128)(2,1)} %refs_8_.3) | copy-start | bytes 6291460
  4.7 62.1 %copy-start.2 = (bf16[4,1024]{1,0:T(4,128)(2,1)S(1)}, bf16[4,1024]{1,0:T(4,128)(2,1)}, u32[]{:S(2)}) copy-start(bf16[4,1024]{1,0:T(4,128)(2,1)} %refs_16_.3) | copy-start | bytes 24580
  7.4 18.2 %collective-permute-start.16 = (bf16[288,256]{1,0:T(8,128)(2,1)S(1)}, bf16[288,256]{1,0:T(8,128)(2,1)S(1)}, u32[]{:S(2)}, u32[]{:S(2)}) collective-permute-start(bf16[288,256]{1,0:T(8,128)(2,1)S(1)} %get-tuple-element.51), channel_id=1, source_target_pairs={{0,4},{4,0},{8,12},{12,8},{1,5},{5,1},{9,13},{13,9},{2,6},{6,2},{1... | collective-permute-start | bytes 442376 | tf_op jit(solution)/shard_map/ppermute | solution.py:190
  7.5 33.0 %collective-permute-start.19 = (bf16[2,256,512]{2,1,0:T(8,128)(2,1)S(1)}, bf16[2,256,512]{2,1,0:T(8,128)(2,1)S(1)}, u32[]{:S(2)}, u32[]{:S(2)}) collective-permute-start(bf16[2,256,512]{2,1,0:T(8,128)(2,1)S(1)} %get-tuple-element.54), channel_id=1, source_target_pairs={{0,2},{1,3},{2,0},{3,1},{4,6},{5,7},{6,4},{7,5},{8,10},{9,11},{10,... | collective-permute-start | bytes 1572872 | tf_op jit(solution)/shard_map/ppermute | solution.py:196
  9.4 5.8 %collective-permute-start.1 = (bf16[96,512]{1,0:T(8,128)(2,1)S(1)}, bf16[96,512]{1,0:T(8,128)(2,1)S(1)}, u32[]{:S(2)}, u32[]{:S(2)}) collective-permute-start(bf16[96,512]{1,0:T(8,128)(2,1)S(1)} %get-tuple-element.35), channel_id=1, source_target_pairs={{0,8},{4,12},{8,0},{12,4},{1,9},{5,13},{9,1},{13,5},{2,10},{6,14},... | collective-permute-start | bytes 294920 | tf_op jit(solution)/shard_map/ppermute | solution.py:190
  12.0 7.8 %collective-permute-start.2 = (bf16[96,512]{1,0:T(8,128)(2,1)S(1)}, bf16[96,512]{1,0:T(8,128)(2,1)S(1)}, u32[]{:S(2)}, u32[]{:S(2)}) collective-permute-start(bf16[96,512]{1,0:T(8,128)(2,1)S(1)} %get-tuple-element.36), channel_id=1, source_target_pairs={{0,12},{4,8},{8,4},{12,0},{1,13},{5,9},{9,5},{13,1},{2,14},{6,10},... | collective-permute-start | bytes 294920 | tf_op jit(solution)/shard_map/ppermute | solution.py:190
  15.2 12.2 %collective-permute-start.17 = (bf16[288,256]{1,0:T(8,128)(2,1)S(1)}, bf16[288,256]{1,0:T(8,128)(2,1)S(1)}, u32[]{:S(2)}, u32[]{:S(2)}) collective-permute-start(bf16[288,256]{1,0:T(8,128)(2,1)S(1)} %get-tuple-element.52), channel_id=1, source_target_pairs={{0,8},{4,12},{8,0},{12,4},{1,9},{5,13},{9,1},{13,5},{2,10},{6,14},... | collective-permute-start | bytes 442376 | tf_op jit(solution)/shard_map/ppermute | solution.py:190
  19.8 13.0 %collective-permute-start.18 = (bf16[288,256]{1,0:T(8,128)(2,1)S(1)}, bf16[288,256]{1,0:T(8,128)(2,1)S(1)}, u32[]{:S(2)}, u32[]{:S(2)}) collective-permute-start(bf16[288,256]{1,0:T(8,128)(2,1)S(1)} %get-tuple-element.53), channel_id=1, source_target_pairs={{0,12},{4,8},{8,4},{12,0},{1,13},{5,9},{9,5},{13,1},{2,14},{6,10},... | collective-permute-start | bytes 442376 | tf_op jit(solution)/shard_map/ppermute | solution.py:190
  25.6 7.9 %collective-permute-start.3 = (bf16[288,256]{1,0:T(8,128)(2,1)S(1)}, bf16[288,256]{1,0:T(8,128)(2,1)S(1)}, u32[]{:S(2)}, u32[]{:S(2)}) collective-permute-start(bf16[288,256]{1,0:T(8,128)(2,1)S(1)} %get-tuple-element.40), channel_id=1, source_target_pairs={{0,4},{4,0},{8,12},{12,8},{1,5},{5,1},{9,13},{13,9},{2,6},{6,2},{1... | collective-permute-start | bytes 442376 | tf_op jit(solution)/shard_map/ppermute | solution.py:190
  27.4 11.1 %collective-permute-start.21 = (bf16[2,256,256]{2,1,0:T(8,128)(2,1)S(1)}, bf16[2,256,256]{2,1,0:T(8,128)(2,1)S(1)}, u32[]{:S(2)}, u32[]{:S(2)}) collective-permute-start(bf16[2,256,256]{2,1,0:T(8,128)(2,1)S(1)} %get-tuple-element.55), channel_id=1, source_target_pairs={{2,0},{3,1},{6,4},{7,5},{10,8},{11,9},{14,12},{15,13},{18,16},{19,... | collective-permute-start | bytes 786440 | tf_op jit(solution)/shard_map/ppermute | solution.py:196
  32.8 7.0 %collective-permute-start.23 = (bf16[2,256,256]{2,1,0:T(8,128)(2,1)S(1)}, bf16[2,256,256]{2,1,0:T(8,128)(2,1)S(1)}, u32[]{:S(2)}, u32[]{:S(2)}) collective-permute-start(bf16[2,256,256]{2,1,0:T(8,128)(2,1)S(1)} %get-tuple-element.56), channel_id=1, source_target_pairs={{3,1},{7,5},{11,9},{15,13},{19,17},{23,21},{27,25},{31,29}} | collective-permute-start | bytes 786440 | tf_op jit(solution)/shard_map/ppermute | solution.py:196
  33.5 25.6 %collective-permute-start.7 = (bf16[2,256,512]{2,1,0:T(8,128)(2,1)S(1)}, bf16[2,256,512]{2,1,0:T(8,128)(2,1)S(1)}, u32[]{:S(2)}, u32[]{:S(2)}) collective-permute-start(bf16[2,256,512]{2,1,0:T(8,128)(2,1)S(1)} %get-tuple-element.43), channel_id=1, source_target_pairs={{0,2},{1,3},{2,0},{3,1},{4,6},{5,7},{6,4},{7,5},{8,10},{9,11},{10,... | collective-permute-start | bytes 1572872 | tf_op jit(solution)/shard_map/ppermute | solution.py:196
  38.5 16.9 %collective-permute-start.9 = (bf16[2,256,256]{2,1,0:T(8,128)(2,1)S(1)}, bf16[2,256,256]{2,1,0:T(8,128)(2,1)S(1)}, u32[]{:S(2)}, u32[]{:S(2)}) collective-permute-start(bf16[2,256,256]{2,1,0:T(8,128)(2,1)S(1)} %get-tuple-element.44), channel_id=1, source_target_pairs={{2,0},{3,1},{6,4},{7,5},{10,8},{11,9},{14,12},{15,13},{18,16},{19,... | collective-permute-start | bytes 786440 | tf_op jit(solution)/shard_map/ppermute | solution.py:196
  39.8 16.5 %collective-permute-start.11 = (bf16[2,256,256]{2,1,0:T(8,128)(2,1)S(1)}, bf16[2,256,256]{2,1,0:T(8,128)(2,1)S(1)}, u32[]{:S(2)}, u32[]{:S(2)}) collective-permute-start(bf16[2,256,256]{2,1,0:T(8,128)(2,1)S(1)} %get-tuple-element.45), channel_id=1, source_target_pairs={{3,1},{7,5},{11,9},{15,13},{19,17},{23,21},{27,25},{31,29}} | collective-permute-start | bytes 786440 | tf_op jit(solution)/shard_map/ppermute | solution.py:196
  40.5 22.0 %collective-permute-start.20 = (bf16[2,256,512]{2,1,0:T(8,128)(2,1)S(1)}, bf16[2,256,512]{2,1,0:T(8,128)(2,1)S(1)}, u32[]{:S(2)}, u32[]{:S(2)}) collective-permute-start(bf16[2,256,512]{2,1,0:T(8,128)(2,1)S(1)} %collective-permute-done.19.refs_10_), channel_id=1, source_target_pairs={{0,1},{1,0},{2,3},{3,2},{4,5},{5,4},{6,7},{7,6},{8,9},{9,8},{10,11... | collective-permute-start | bytes 1572872 | tf_op jit(solution)/shard_map/ppermute | solution.py:198
  55.4 3.8 %collective-permute-start.22 = (bf16[2,256,256]{2,1,0:T(8,128)(2,1)S(1)}, bf16[2,256,256]{2,1,0:T(8,128)(2,1)S(1)}, u32[]{:S(2)}, u32[]{:S(2)}) collective-permute-start(bf16[2,256,256]{2,1,0:T(8,128)(2,1)S(1)} %collective-permute-done.21.refs_12_), channel_id=1, source_target_pairs={{0,1},{1,0},{2,3},{3,2},{4,5},{5,4},{6,7},{7,6},{8,9},{9,8},{10,11... | collective-permute-start | bytes 786440 | tf_op jit(solution)/shard_map/ppermute | solution.py:198
  56.4 6.0 %collective-permute-start.24 = (bf16[2,256,256]{2,1,0:T(8,128)(2,1)S(1)}, bf16[2,256,256]{2,1,0:T(8,128)(2,1)S(1)}, u32[]{:S(2)}, u32[]{:S(2)}) collective-permute-start(bf16[2,256,256]{2,1,0:T(8,128)(2,1)S(1)} %collective-permute-done.23.refs_14_), channel_id=1, source_target_pairs={{0,1},{1,0},{2,3},{3,2},{4,5},{5,4},{6,7},{7,6},{8,9},{9,8},{10,11... | collective-permute-start | bytes 786440 | tf_op jit(solution)/shard_map/ppermute | solution.py:198
  59.2 20.2 %collective-permute-start.8 = (bf16[2,256,512]{2,1,0:T(8,128)(2,1)S(1)}, bf16[2,256,512]{2,1,0:T(8,128)(2,1)S(1)}, u32[]{:S(2)}, u32[]{:S(2)}) collective-permute-start(bf16[2,256,512]{2,1,0:T(8,128)(2,1)S(1)} %collective-permute-done.7.refs_10_), channel_id=1, source_target_pairs={{0,1},{1,0},{2,3},{3,2},{4,5},{5,4},{6,7},{7,6},{8,9},{9,8},{10,11... | collective-permute-start | bytes 1572872 | tf_op jit(solution)/shard_map/ppermute | solution.py:198
  59.2 14.2 %collective-permute-start.4 = (bf16[288,256]{1,0:T(8,128)(2,1)S(1)}, bf16[288,256]{1,0:T(8,128)(2,1)S(1)}, u32[]{:S(2)}, u32[]{:S(2)}) collective-permute-start(bf16[288,256]{1,0:T(8,128)(2,1)S(1)} %get-tuple-element.41), channel_id=1, source_target_pairs={{0,8},{4,12},{8,0},{12,4},{1,9},{5,13},{9,1},{13,5},{2,10},{6,14},... | collective-permute-start | bytes 442376 | tf_op jit(solution)/shard_map/ppermute | solution.py:190
  62.4 16.6 %collective-permute-start.10 = (bf16[2,256,256]{2,1,0:T(8,128)(2,1)S(1)}, bf16[2,256,256]{2,1,0:T(8,128)(2,1)S(1)}, u32[]{:S(2)}, u32[]{:S(2)}) collective-permute-start(bf16[2,256,256]{2,1,0:T(8,128)(2,1)S(1)} %collective-permute-done.9.refs_12_), channel_id=1, source_target_pairs={{0,1},{1,0},{2,3},{3,2},{4,5},{5,4},{6,7},{7,6},{8,9},{9,8},{10,11... | collective-permute-start | bytes 786440 | tf_op jit(solution)/shard_map/ppermute | solution.py:198
  62.5 16.9 %collective-permute-start.12 = (bf16[2,256,256]{2,1,0:T(8,128)(2,1)S(1)}, bf16[2,256,256]{2,1,0:T(8,128)(2,1)S(1)}, u32[]{:S(2)}, u32[]{:S(2)}) collective-permute-start(bf16[2,256,256]{2,1,0:T(8,128)(2,1)S(1)} %collective-permute-done.11.refs_14_), channel_id=1, source_target_pairs={{0,1},{1,0},{2,3},{3,2},{4,5},{5,4},{6,7},{7,6},{8,9},{9,8},{10,11... | collective-permute-start | bytes 786440 | tf_op jit(solution)/shard_map/ppermute | solution.py:198
  62.9 11.0 %collective-permute-start.5 = (bf16[288,256]{1,0:T(8,128)(2,1)S(1)}, bf16[288,256]{1,0:T(8,128)(2,1)S(1)}, u32[]{:S(2)}, u32[]{:S(2)}) collective-permute-start(bf16[288,256]{1,0:T(8,128)(2,1)S(1)} %get-tuple-element.42), channel_id=1, source_target_pairs={{0,12},{4,8},{8,4},{12,0},{1,13},{5,9},{9,5},{13,1},{2,14},{6,10},... | collective-permute-start | bytes 442376 | tf_op jit(solution)/shard_map/ppermute | solution.py:190
  73.4 11.7 %collective-permute-start.25 = (bf16[384,256]{1,0:T(8,128)(2,1)S(1)}, bf16[384,256]{1,0:T(8,128)(2,1)S(1)}, u32[]{:S(2)}, u32[]{:S(2)}) collective-permute-start(bf16[384,256]{1,0:T(8,128)(2,1)S(1)} %get-tuple-element.58), channel_id=1, source_target_pairs={{0,4},{4,0},{8,12},{12,8},{1,5},{5,1},{9,13},{13,9},{2,6},{6,2},{1... | collective-permute-start | bytes 589832 | tf_op jit(solution)/shard_map/ppermute | solution.py:190
  73.9 19.3 %collective-permute-start.26 = (bf16[384,256]{1,0:T(8,128)(2,1)S(1)}, bf16[384,256]{1,0:T(8,128)(2,1)S(1)}, u32[]{:S(2)}, u32[]{:S(2)}) collective-permute-start(bf16[384,256]{1,0:T(8,128)(2,1)S(1)} %get-tuple-element.59), channel_id=1, source_target_pairs={{0,8},{4,12},{8,0},{12,4},{1,9},{5,13},{9,1},{13,5},{2,10},{6,14},... | collective-permute-start | bytes 589832 | tf_op jit(solution)/shard_map/ppermute | solution.py:190
  78.9 14.2 %collective-permute-start.27 = (bf16[384,256]{1,0:T(8,128)(2,1)S(1)}, bf16[384,256]{1,0:T(8,128)(2,1)S(1)}, u32[]{:S(2)}, u32[]{:S(2)}) collective-permute-start(bf16[384,256]{1,0:T(8,128)(2,1)S(1)} %get-tuple-element.60), channel_id=1, source_target_pairs={{0,12},{4,8},{8,4},{12,0},{1,13},{5,9},{9,5},{13,1},{2,14},{6,10},... | collective-permute-start | bytes 589832 | tf_op jit(solution)/shard_map/ppermute | solution.py:190
  79.4 13.8 %copy-start.1 = (bf16[1,384,2048]{2,1,0:T(8,128)(2,1)S(1)}, bf16[1,384,2048]{2,1,0:T(8,128)(2,1)}, u32[]{:S(2)}) copy-start(bf16[1,384,2048]{2,1,0:T(8,128)(2,1)} %param.6) | copy-start | bytes 4718596
  81.1 13.4 %collective-permute-start.14 = (bf16[384,256]{1,0:T(8,128)(2,1)S(1)}, bf16[384,256]{1,0:T(8,128)(2,1)S(1)}, u32[]{:S(2)}, u32[]{:S(2)}) collective-permute-start(bf16[384,256]{1,0:T(8,128)(2,1)S(1)} %get-tuple-element.48), channel_id=1, source_target_pairs={{0,4},{4,0},{8,12},{12,8},{1,5},{5,1},{9,13},{13,9},{2,6},{6,2},{1... | collective-permute-start | bytes 589832 | tf_op jit(solution)/shard_map/ppermute | solution.py:190
  81.3 28.7 %collective-permute-start.15 = (bf16[384,256]{1,0:T(8,128)(2,1)S(1)}, bf16[384,256]{1,0:T(8,128)(2,1)S(1)}, u32[]{:S(2)}, u32[]{:S(2)}) collective-permute-start(bf16[384,256]{1,0:T(8,128)(2,1)S(1)} %get-tuple-element.49), channel_id=1, source_target_pairs={{0,8},{4,12},{8,0},{12,4},{1,9},{5,13},{9,1},{13,5},{2,10},{6,14},... | collective-permute-start | bytes 589832 | tf_op jit(solution)/shard_map/ppermute | solution.py:190
  85.1 26.1 %collective-permute-start.13 = (bf16[384,256]{1,0:T(8,128)(2,1)S(1)}, bf16[384,256]{1,0:T(8,128)(2,1)S(1)}, u32[]{:S(2)}, u32[]{:S(2)}) collective-permute-start(bf16[384,256]{1,0:T(8,128)(2,1)S(1)} %get-tuple-element.46), channel_id=1, source_target_pairs={{0,12},{4,8},{8,4},{12,0},{1,13},{5,9},{9,5},{13,1},{2,14},{6,10},... | collective-permute-start | bytes 589832 | tf_op jit(solution)/shard_map/ppermute | solution.py:190
